TPU v7x, 512 devices: a whole 4x4x16 slice. The times are simulated.
512 devices in a mesh: sp: 16 (over z), fs: 4 (over y), tp: 8 (over x, core).
Axes of the slice: x: 4, y: 4, z: 16, core: 2. Of those that a mesh axis runs over, the one named last changes fastest.
Arguments:
- inputs: bfloat16 [4, 2048, 2048], P('fs', 'sp'), may hold values from -6 to 6
- norm_gain: float32 [2048], replicated, may hold values from 0.1 to 1.9
- w_gate: bfloat16 [2048, 2048], P(('sp', 'fs'), 'tp'), may hold values from -0.125 to 0.125
- w_input: bfloat16 [2048, 2048], P(('sp', 'fs'), 'tp'), may hold values from -0.125 to 0.125
- w_bkey: bfloat16 [2048, 1024], P(('sp', 'fs'), 'tp'), may hold values from -0.125 to 0.125
- w_cquery: bfloat16 [2048, 1024], P(('sp', 'fs'), 'tp'), may hold values from -0.125 to 0.125
- w_step: bfloat16 [2048, 32], replicated, may hold values from -0.125 to 0.125
- conv_weight: float32 [4, 4096], replicated, may hold values from -2 to 2
- decay_rate: float32 [32], replicated, may hold values from 0 to 0.05, as said below
- decay_offset: float32 [4, 2048, 32], P('fs', 'sp', 'tp'), may hold values from -2 to 0
- ssd_gain: float32 [2048], replicated, may hold values from 0.1 to 1.9
- w_query: bfloat16 [2048, 2048], P(('sp', 'fs'), 'tp'), may hold values from -0.125 to 0.125
- w_key: bfloat16 [2048, 2048], P(('sp', 'fs'), 'tp'), may hold values from -0.125 to 0.125
- w_value: bfloat16 [2048, 2048], P(('sp', 'fs'), 'tp'), may hold values from -0.125 to 0.125
- stick_bias: float32 [16], replicated, may hold values from -12 to 0
- out_mixer: bfloat16 [2048, 2048], P('tp', ('sp', 'fs')), may hold values from -0.125 to 0.125
- out_attend: bfloat16 [2048, 2048], P('tp', ('sp', 'fs')), may hold values from -3.59375 to 3.59375
Outputs:
- mixed: bfloat16 [4, 2048, 2048], P('fs', ('sp', 'tp'))
Inputs may be any that keep to these rules, and one draw needn't show every extreme that they name: `decay_rate`: one positive rate for each head.
All inputs are finite; a program needn't handle non-finite values.
Results may differ from a plain program's by a relative error of at most 0.015.
Values may be sent and summed in bfloat16 or wider, within the bound.
No kernel may reach another device: no remote copies, remote signals or barrier semaphores. Data moves between devices by JAX's collectives and lax.ppermute only.
A program may use at most 64 MiB of HBM per device.

v0:
```python
import jax
import jax.numpy as jnp
from jax import lax
from jax.sharding import PartitionSpec as P

HEAD_DIM = 64
STATE = 128
CONV = 4
BLOCK = 128
SB_DIM = 128
SSD_INNER = 2048
GROUP_WIDTH = 1024


EPS = 1e-06


def side_by_side(arrays, axis, dim, along):
    ends, at = ([], 0)
    for a in arrays[:-1]:
        at += a.shape[along]
        ends.append(at)
    both = jnp.concatenate(arrays, axis=along)
    return tuple(jnp.split(lax.all_gather(both, axis, axis=dim, tiled=True), ends, axis=along))


def turned_gather(arrays, axis, dims):
    turned = [jnp.moveaxis(a, dim, 0) for a, dim in zip(arrays, dims)]
    both = jnp.concatenate([t.reshape(len(t), -1) for t in turned], axis=1)
    filled, at, finished = (lax.all_gather(both, axis, axis=0, tiled=True), 0, [])
    for t, dim in zip(turned, dims):
        section = filled[:, at : at + t[0].size].reshape(-1, *t.shape[1:])
        finished.append(jnp.moveaxis(section, 0, dim))
        at += t[0].size
    return tuple(finished)


def passed_along(shard, axis, by):
    length = lax.axis_size(axis)
    pairs = [(i, i + by) for i in range(length) if 0 <= i + by < length]
    return lax.ppermute(shard, axis, pairs)


def copy_for_each(shard, axis):
    length = lax.axis_size(axis)
    return lax.all_to_all(
        jnp.broadcast_to(shard[None], (length, *shard.shape)), axis, 0, 0, tiled=True
    )


def joined_by_halves(pieces, combine):
    while len(jax.tree.leaves(pieces)[0]) > 1:
        pieces = jax.vmap(combine)(
            *(jax.tree.map(lambda part: part[side::2], pieces) for side in (0, 1))
        )
    return jax.tree.map(lambda part: part[0], pieces)


def prefix(shard, axis, combine, identity):
    length, here = (lax.axis_size(axis), lax.axis_index(axis))
    passed = jnp.arange(length) < here

    def kept(part, zero, own):
        part = jnp.where(
            passed.reshape(-1, *(1 for _ in own.shape)),
            part.astype(own.dtype),
            jnp.asarray(zero, own.dtype),
        )
        return part

    pieces = jax.tree.map(
        lambda part: copy_for_each(part, axis),
        jax.tree.map(lambda part, kind: part.astype(kind), shard, (jnp.bfloat16, jnp.bfloat16)),
    )
    return joined_by_halves(jax.tree.map(kept, pieces, identity, shard), combine)


def cut_along(shard, dim, length):
    dims = shard.shape
    parts = shard.reshape(*dims[:dim], length, dims[dim] // length, *dims[dim + 1 :])
    return jnp.moveaxis(parts, dim, 0)


def summed_on_arrival(shard, axis, dim):
    length = lax.axis_size(axis)
    parts = lax.all_to_all(cut_along(shard, dim, length), axis, 0, 0, tiled=True)
    return jnp.sum(parts.astype(jnp.float32), axis=0)


def short_conv(rim_rows, current, weights):
    padded = jnp.concatenate([rim_rows, current], axis=0).astype(jnp.float32)
    length = current.shape[0]
    summed = weights[0] * padded[0:length]
    for tap_index in range(1, weights.shape[0]):
        summed = summed + weights[tap_index] * padded[tap_index : tap_index + length]
    return jax.nn.silu(summed).astype(jnp.bfloat16)


def block_terms(input_blocks, bkey_blocks, cquery_blocks, step_blocks, decay_blocks):
    cumulative = jnp.cumsum(decay_blocks, axis=1)
    cum_turned = jnp.transpose(cumulative, (0, 2, 3, 1))
    step_turned = jnp.transpose(step_blocks, (0, 2, 3, 1))
    length = input_blocks.shape[1]
    row_index = lax.broadcasted_iota(jnp.int32, (length, length), 0)
    col_index = lax.broadcasted_iota(jnp.int32, (length, length), 1)
    lower_mask = row_index >= col_index
    spread = cum_turned[..., :, None] - cum_turned[..., None, :]
    inner_prod = jnp.einsum(
        "blgn,bsgn->bgls", cquery_blocks, bkey_blocks, preferred_element_type=jnp.float32
    )
    mixing = jnp.where(
        lower_mask,
        inner_prod[:, :, None]
        * jnp.exp(jnp.where(lower_mask, spread, 0.0))
        * step_turned[..., None, :],
        0.0,
    )
    y_inner = jnp.einsum(
        "bgrls,bsgrp->blgrp",
        mixing.astype(jnp.bfloat16),
        input_blocks,
        preferred_element_type=jnp.float32,
    )
    to_end = jnp.exp(cumulative[:, -1:] - cumulative) * step_blocks
    weighted = (bkey_blocks.astype(jnp.float32)[:, :, :, None, :] * to_end[..., None]).astype(
        jnp.bfloat16
    )
    states = jnp.einsum(
        "blgrp,blgrn->bgrpn", input_blocks, weighted, preferred_element_type=jnp.float32
    )
    return (cumulative, y_inner, states)


def chain_blocks(states, totals):

    def advance(held_state, block_item):
        block_state, block_log = block_item
        return (held_state * jnp.exp(block_log)[..., None, None] + block_state, held_state)

    return lax.scan(advance, jnp.zeros_like(states[0]), (states, totals))


def carried_output(cquery_blocks, entering, cumulative):
    return (
        jnp.einsum(
            "blgn,bgrpn->blgrp",
            cquery_blocks.astype(jnp.float32),
            entering,
            precision=lax.Precision.HIGHEST,
        )
        * jnp.exp(cumulative)[..., None]
    )


def gating_rescaled_output(y_total, gate_act, gain_slice, groups):
    length = y_total.shape[0]
    group_width = y_total.shape[2] * y_total.shape[3]
    gated_out = y_total.reshape(length, groups, group_width) * jax.nn.silu(
        gate_act.astype(jnp.float32)
    ).reshape(length, groups, group_width)
    scaled = gated_out * lax.rsqrt(jnp.mean(gated_out * gated_out, axis=-1, keepdims=True) + EPS)
    return (scaled.reshape(length, groups * group_width) * gain_slice).astype(jnp.bfloat16)


def join_states(earlier, following):
    return (
        earlier[0] * jnp.exp(following[1])[..., None, None] + following[0],
        earlier[1] + following[1],
    )


def stick_piece(carried, query_heads, key_heads, value_heads, bias_heads, causal):
    summed, later_log = carried
    length = query_heads.shape[0]
    key_count = key_heads.shape[0]
    logits = (
        jnp.einsum("thd,shd->hts", query_heads, key_heads, preferred_element_type=jnp.float32)
        * query_heads.shape[2] ** (-0.5)
        + bias_heads[:, None, None]
    )
    log_keep = jax.nn.log_sigmoid(logits)
    log_pass = jax.nn.log_sigmoid(-logits)
    if causal:
        query_pos = lax.broadcasted_iota(jnp.int32, (length, key_count), 0)
        key_pos = lax.broadcasted_iota(jnp.int32, (length, key_count), 1)
        before = key_pos < query_pos
        log_pass = jnp.where(before, log_pass, 0.0)
    tail_sum = lax.cumsum(log_pass, axis=2, reverse=True) - log_pass
    weights = jnp.exp(log_keep + tail_sum + later_log[:, :, None])
    if causal:
        weights = jnp.where(before, weights, 0.0)
    summed = summed + jnp.einsum(
        "hts,shd->thd",
        weights.astype(jnp.bfloat16),
        value_heads,
        preferred_element_type=jnp.float32,
    )
    return (summed, later_log + jnp.sum(log_pass, axis=2))


def body(
    inputs,
    norm_gain,
    w_gate,
    w_input,
    w_bkey,
    w_cquery,
    w_step,
    conv_weight,
    decay_rate,
    decay_offset,
    ssd_gain,
    w_query,
    w_key,
    w_value,
    stick_bias,
    out_mixer,
    out_attend,
):
    tensor_index = lax.axis_index("tp")
    seq_index = lax.axis_index("sp")
    seq_count = lax.axis_size("sp")
    tokens = inputs[0]
    row_count = tokens.shape[0]
    widened = tokens.astype(jnp.float32)
    normed = (
        widened * lax.rsqrt(jnp.mean(widened * widened, axis=-1, keepdims=True) + EPS) * norm_gain
    ).astype(jnp.bfloat16)
    gate_near, input_near, bkey_near, cquery_near, query_near, local_window_lookup, value_near = (
        side_by_side((w_gate, w_input, w_bkey, w_cquery, w_query, w_key, w_value), "fs", 0, 1)
    )
    pieces = side_by_side(
        (
            gate_near,
            input_near,
            bkey_near,
            cquery_near,
            query_near,
            local_window_lookup,
            value_near,
        ),
        "sp",
        0,
        1,
    )
    projected = tuple(
        (jnp.dot(normed, piece_rows, preferred_element_type=jnp.float32) for piece_rows in pieces)
    )
    gate_act, input_act, input_projection_after_silu, cquery_act, queries, key_act, value_act = (
        tuple((summed.astype(jnp.bfloat16) for summed in projected))
    )
    mixer_full, attend_full = turned_gather((out_mixer, out_attend), ("sp", "fs"), (1, 1))
    input_width = input_act.shape[1]
    group_cols = input_projection_after_silu.shape[1]
    heads_local = input_width // HEAD_DIM
    groups_local = group_cols // STATE
    head_ratio = heads_local // groups_local
    blocks_local = row_count // BLOCK
    rim_input, rim_bkey, rim_cquery = passed_along(
        (
            input_act[row_count - CONV + 1 :],
            input_projection_after_silu[row_count - CONV + 1 :],
            cquery_act[row_count - CONV + 1 :],
        ),
        "sp",
        1,
    )
    conv_input = lax.dynamic_slice_in_dim(conv_weight, tensor_index * input_width, input_width, 1)
    conv_bkey = lax.dynamic_slice_in_dim(
        conv_weight, SSD_INNER + tensor_index * group_cols, group_cols, 1
    )
    conv_cquery = lax.dynamic_slice_in_dim(
        conv_weight, SSD_INNER + GROUP_WIDTH + tensor_index * group_cols, group_cols, 1
    )
    input_conv = short_conv(rim_input, input_act, conv_input)
    bkey_conv = short_conv(rim_bkey, input_projection_after_silu, conv_bkey)
    cquery_conv = short_conv(rim_cquery, cquery_act, conv_cquery)
    step_cols = lax.dynamic_slice_in_dim(w_step, tensor_index * heads_local, heads_local, 1)
    step_size = jax.nn.softplus(jnp.dot(normed, step_cols, preferred_element_type=jnp.float32))
    rate_slice = lax.dynamic_slice_in_dim(decay_rate, tensor_index * heads_local, heads_local, 0)
    log_decay = decay_offset[0] - rate_slice * step_size
    input_blocks = input_conv.reshape(blocks_local, BLOCK, groups_local, head_ratio, HEAD_DIM)
    bkey_blocks = bkey_conv.reshape(blocks_local, BLOCK, groups_local, STATE)
    cquery_blocks = cquery_conv.reshape(blocks_local, BLOCK, groups_local, STATE)
    step_blocks = step_size.reshape(blocks_local, BLOCK, groups_local, head_ratio)
    decay_blocks = log_decay.reshape(blocks_local, BLOCK, groups_local, head_ratio)
    cumulative, y_inner, states = block_terms(
        input_blocks, bkey_blocks, cquery_blocks, step_blocks, decay_blocks
    )
    totals = cumulative[:, -1]
    local_end, local_entering = chain_blocks(states, totals)
    device_log = jnp.sum(totals, axis=0)
    carried_state, carried_log = prefix(
        (local_end, device_log),
        "sp",
        join_states,
        (jnp.zeros_like(local_end), jnp.zeros_like(device_log)),
    )
    before_log = jnp.cumsum(totals, axis=0) - totals
    entering = local_entering + jnp.exp(before_log)[..., None, None] * carried_state[None]
    y_total = y_inner + carried_output(cquery_blocks, entering, cumulative)
    gain_slice = lax.dynamic_slice_in_dim(ssd_gain, tensor_index * input_width, input_width, 0)
    y_mixer = gating_rescaled_output(
        y_total.reshape(row_count, groups_local, head_ratio, HEAD_DIM),
        gate_act,
        gain_slice,
        groups_local,
    )
    heads_stick = queries.shape[1] // SB_DIM
    query_heads = queries.reshape(row_count, heads_stick, SB_DIM)
    key_heads = key_act.reshape(row_count, heads_stick, SB_DIM)
    value_heads = value_act.reshape(row_count, heads_stick, SB_DIM)
    bias_heads = lax.dynamic_slice_in_dim(stick_bias, tensor_index * heads_stick, heads_stick, 0)
    carried = (
        jnp.zeros((row_count, heads_stick, SB_DIM), jnp.float32),
        jnp.zeros((heads_stick, row_count), jnp.float32),
    )
    carried = stick_piece(carried, query_heads, key_heads, value_heads, bias_heads, True)

    def relay(turn_index, held_four):
        summed, later_log, key_here, value_here = held_four
        key_here, value_here = passed_along((key_here, value_here), "sp", 1)

        def take_piece(retained_couple):
            return stick_piece(
                retained_couple, query_heads, key_here, value_here, bias_heads, False
            )

        def skip_piece(retained_couple):
            return retained_couple

        summed, later_log = lax.cond(
            turn_index < seq_index, take_piece, skip_piece, (summed, later_log)
        )
        return (summed, later_log, key_here, value_here)

    outcome = lax.fori_loop(
        0, seq_count - 1, relay, (carried[0], carried[1], key_heads, value_heads)
    )
    carried = (outcome[0], outcome[1])
    y_attend = carried[0].astype(jnp.bfloat16).reshape(row_count, heads_stick * SB_DIM)
    mixed = summed_on_arrival(
        (
            jnp.dot(y_mixer, mixer_full, preferred_element_type=jnp.float32)
            + jnp.dot(y_attend, attend_full, preferred_element_type=jnp.float32)
        ).astype(jnp.bfloat16),
        "tp",
        0,
    )
    return mixed.astype(jnp.bfloat16)[None]


def solution(mesh):
    return jax.shard_map(
        body,
        mesh=mesh,
        in_specs=(
            P("fs", "sp", None),
            P(),
            P(("sp", "fs"), "tp"),
            P(("sp", "fs"), "tp"),
            P(("sp", "fs"), "tp"),
            P(("sp", "fs"), "tp"),
            P(),
            P(),
            P(),
            P("fs", "sp", "tp"),
            P(),
            P(("sp", "fs"), "tp"),
            P(("sp", "fs"), "tp"),
            P(("sp", "fs"), "tp"),
            P(),
            P("tp", ("sp", "fs")),
            P("tp", ("sp", "fs")),
        ),
        out_specs=P("fs", ("sp", "tp"), None),
        check_vma=False,
    )
```

profile of v0, /device:TPU:1, one launch (start us, length us, event | category | flops | bytes accessed | tf_op | source)
XLA Modules:
  0.0 379.1 jit_solution(12561317519375032750)
XLA Ops:
  11.6 12.0 %all_gather.9 = bf16[128,1536]{1,0:T(8,128)(2,1)} all-gather(bf16[32,1536]{1,0:T(8,128)(2,1)S(1)} %constant_dynamic-update-slice_fusion), channel_id=1, replica_groups=mesh['sp'=16,'fs'=4,'tp'=8] {'fs'}, dimensions={0}, use_global_device_ids=true | all-gather | bytes 491520 | tf_op jit(solution)/shard_map/all_gather | solution.py:24
  28.7 15.3 %all-to-all-start.1 = ((bf16[16,1,4]{2,1,0:T(2,128)(2,1)}), bf16[16,1,4]{2,1,0:T(2,128)(2,1)S(1)}, u32[]{:S(2)}, u32[]{:S(2)}) async-start(bf16[16,1,4]{2,1,0:T(2,128)(2,1)} %broadcast_in_dim.93), calls=%async_computation.1 | async-start | bytes 16384 | tf_op jit(solution)/shard_map/all_to_all | solution.py:46
  48.7 65.2 %all-gather.3.cloned.1.call-done = bf16[2048,1536]{1,0:T(8,128)(2,1)} async-done(((bf16[128,1536]{1,0:T(8,128)(2,1)}), bf16[2048,1536]{1,0:T(8,128)(2,1)}) %all-gather.3.cloned.1.call-update) | async-done | bytes 6291472 | tf_op jit(solution)/shard_map/all_gather | solution.py:24
  118.8 3.7 collective-permute-start.2
  125.1 12.6 %all-to-all-start = ((bf16[16,1,4,64,128]{4,3,2,1,0:T(8,128)(2,1)}), bf16[16,1,4,64,128]{4,3,2,1,0:T(8,128)(2,1)S(1)}, u32[]{:S(2)}, u32[]{:S(2)}) async-start(bf16[16,1,4,64,128]{4,3,2,1,0:T(8,128)(2,1)} %broadcast_in_dim.90), calls=%async_computation | async-start | bytes 2097152 | tf_op jit(solution)/shard_map/all_to_all | solution.py:46
  151.5 184.8 %while.5 = (s32[]{:T(128)}, f32[128,2,128]{2,0,1:T(8,128)S(1)}, f32[2,128]{1,0:T(2,128)S(1)}, bf16[128,2,128]{2,0,1:T(8,128)(2,1)S(1)}, bf16[128,2,128]{2,0,1:T(...) while((s32[]{:T(128)}, f32[128,2,128]{2,0,1:T(8,128)S(1)}, ...), condition=%wide.region_10.11_spmd, body=%wide.region_5.10_spmd.sunk | while | flops 22266116 | bytes 2217247 | solution.py:337
  157.7 16.8 %collective-permute-done = bf16[128,2,128]{2,0,1:T(8,128)(2,1)S(1)} collective-permute-done((bf16[128,2,128]{2,0,1:T(8,128)(2,1)S(1)}, bf16[128,2,128]{2,0,1:T(8,128)(2,1)S(1)}, u32[]{:S(2)}, u32[]{:S(2)}) %collective-permute-start) | collective-permute-done | bytes 65568 | tf_op jit(solution)/shard_map/while/body/eval_jaxpr/ppermute | solution.py:41
  174.5 5.9 %collective-permute-done.1 = bf16[128,2,128]{2,0,1:T(8,128)(2,1)S(1)} collective-permute-done((bf16[128,2,128]{2,0,1:T(8,128)(2,1)S(1)}, bf16[128,2,128]{2,0,1:T(8,128)(2,1)S(1)}, u32[]{:S(2)}, u32[]{:S(2)}) %collective-permute-start.1) | collective-permute-done | bytes 65568 | tf_op jit(solution)/shard_map/while/body/eval_jaxpr/ppermute | solution.py:41
  180.4 13.5 %collective-permute-start = (bf16[128,2,128]{2,0,1:T(8,128)(2,1)S(1)}, bf16[128,2,128]{2,0,1:T(8,128)(2,1)S(1)}, u32[]{:S(2)}, u32[]{:S(2)}) collective-permute-start(bf16[128,2,128]{2,0,1:T(8,128)(2,1)S(1)} %get-tuple-element.351), channel_id=1, source_target_pairs={{0,32},{32,64},{64,96},{96,128},{128,160},{160,192},{192,224},{224... | collective-permute-start | bytes 196616 | tf_op jit(solution)/shard_map/while/body/eval_jaxpr/ppermute | solution.py:41
  193.9 4.4 %collective-permute-start.1 = (bf16[128,2,128]{2,0,1:T(8,128)(2,1)S(1)}, bf16[128,2,128]{2,0,1:T(8,128)(2,1)S(1)}, u32[]{:S(2)}, u32[]{:S(2)}) collective-permute-start(bf16[128,2,128]{2,0,1:T(8,128)(2,1)S(1)} %get-tuple-element.352), channel_id=1, source_target_pairs={{0,32},{32,64},{64,96},{96,128},{128,160},{160,192},{192,224},{224... | collective-permute-start | bytes 196616 | tf_op jit(solution)/shard_map/while/body/eval_jaxpr/ppermute | solution.py:41
  203.3 6.2 %collective-permute-start.1 = (bf16[128,2,128]{2,0,1:T(8,128)(2,1)S(1)}, bf16[128,2,128]{2,0,1:T(8,128)(2,1)S(1)}, u32[]{:S(2)}, u32[]{:S(2)}) collective-permute-start(bf16[128,2,128]{2,0,1:T(8,128)(2,1)S(1)} %get-tuple-element.352), channel_id=1, source_target_pairs={{0,32},{32,64},{64,96},{96,128},{128,160},{160,192},{192,224},{224... | collective-permute-start | bytes 196616 | tf_op jit(solution)/shard_map/while/body/eval_jaxpr/ppermute | solution.py:41
  214.6 5.0 %collective-permute-start.1 = (bf16[128,2,128]{2,0,1:T(8,128)(2,1)S(1)}, bf16[128,2,128]{2,0,1:T(8,128)(2,1)S(1)}, u32[]{:S(2)}, u32[]{:S(2)}) collective-permute-start(bf16[128,2,128]{2,0,1:T(8,128)(2,1)S(1)} %get-tuple-element.352), channel_id=1, source_target_pairs={{0,32},{32,64},{64,96},{96,128},{128,160},{160,192},{192,224},{224... | collective-permute-start | bytes 196616 | tf_op jit(solution)/shard_map/while/body/eval_jaxpr/ppermute | solution.py:41
  220.9 7.2 %collective-permute-start = (bf16[128,2,128]{2,0,1:T(8,128)(2,1)S(1)}, bf16[128,2,128]{2,0,1:T(8,128)(2,1)S(1)}, u32[]{:S(2)}, u32[]{:S(2)}) collective-permute-start(bf16[128,2,128]{2,0,1:T(8,128)(2,1)S(1)} %get-tuple-element.351), channel_id=1, source_target_pairs={{0,32},{32,64},{64,96},{96,128},{128,160},{160,192},{192,224},{224... | collective-permute-start | bytes 196616 | tf_op jit(solution)/shard_map/while/body/eval_jaxpr/ppermute | solution.py:41
  228.1 4.2 %collective-permute-start.1 = (bf16[128,2,128]{2,0,1:T(8,128)(2,1)S(1)}, bf16[128,2,128]{2,0,1:T(8,128)(2,1)S(1)}, u32[]{:S(2)}, u32[]{:S(2)}) collective-permute-start(bf16[128,2,128]{2,0,1:T(8,128)(2,1)S(1)} %get-tuple-element.352), channel_id=1, source_target_pairs={{0,32},{32,64},{64,96},{96,128},{128,160},{160,192},{192,224},{224... | collective-permute-start | bytes 196616 | tf_op jit(solution)/shard_map/while/body/eval_jaxpr/ppermute | solution.py:41
  234.1 4.2 %collective-permute-start = (bf16[128,2,128]{2,0,1:T(8,128)(2,1)S(1)}, bf16[128,2,128]{2,0,1:T(8,128)(2,1)S(1)}, u32[]{:S(2)}, u32[]{:S(2)}) collective-permute-start(bf16[128,2,128]{2,0,1:T(8,128)(2,1)S(1)} %get-tuple-element.351), channel_id=1, source_target_pairs={{0,32},{32,64},{64,96},{96,128},{128,160},{160,192},{192,224},{224... | collective-permute-start | bytes 196616 | tf_op jit(solution)/shard_map/while/body/eval_jaxpr/ppermute | solution.py:41
  238.4 4.3 %collective-permute-start.1 = (bf16[128,2,128]{2,0,1:T(8,128)(2,1)S(1)}, bf16[128,2,128]{2,0,1:T(8,128)(2,1)S(1)}, u32[]{:S(2)}, u32[]{:S(2)}) collective-permute-start(bf16[128,2,128]{2,0,1:T(8,128)(2,1)S(1)} %get-tuple-element.352), channel_id=1, source_target_pairs={{0,32},{32,64},{64,96},{96,128},{128,160},{160,192},{192,224},{224... | collective-permute-start | bytes 196616 | tf_op jit(solution)/shard_map/while/body/eval_jaxpr/ppermute | solution.py:41
  244.2 4.2 %collective-permute-start = (bf16[128,2,128]{2,0,1:T(8,128)(2,1)S(1)}, bf16[128,2,128]{2,0,1:T(8,128)(2,1)S(1)}, u32[]{:S(2)}, u32[]{:S(2)}) collective-permute-start(bf16[128,2,128]{2,0,1:T(8,128)(2,1)S(1)} %get-tuple-element.351), channel_id=1, source_target_pairs={{0,32},{32,64},{64,96},{96,128},{128,160},{160,192},{192,224},{224... | collective-permute-start | bytes 196616 | tf_op jit(solution)/shard_map/while/body/eval_jaxpr/ppermute | solution.py:41
  248.4 4.0 %collective-permute-start.1 = (bf16[128,2,128]{2,0,1:T(8,128)(2,1)S(1)}, bf16[128,2,128]{2,0,1:T(8,128)(2,1)S(1)}, u32[]{:S(2)}, u32[]{:S(2)}) collective-permute-start(bf16[128,2,128]{2,0,1:T(8,128)(2,1)S(1)} %get-tuple-element.352), channel_id=1, source_target_pairs={{0,32},{32,64},{64,96},{96,128},{128,160},{160,192},{192,224},{224... | collective-permute-start | bytes 196616 | tf_op jit(solution)/shard_map/while/body/eval_jaxpr/ppermute | solution.py:41
  253.8 5.7 %collective-permute-start = (bf16[128,2,128]{2,0,1:T(8,128)(2,1)S(1)}, bf16[128,2,128]{2,0,1:T(8,128)(2,1)S(1)}, u32[]{:S(2)}, u32[]{:S(2)}) collective-permute-start(bf16[128,2,128]{2,0,1:T(8,128)(2,1)S(1)} %get-tuple-element.351), channel_id=1, source_target_pairs={{0,32},{32,64},{64,96},{96,128},{128,160},{160,192},{192,224},{224... | collective-permute-start | bytes 196616 | tf_op jit(solution)/shard_map/while/body/eval_jaxpr/ppermute | solution.py:41
  259.5 5.3 %collective-permute-start.1 = (bf16[128,2,128]{2,0,1:T(8,128)(2,1)S(1)}, bf16[128,2,128]{2,0,1:T(8,128)(2,1)S(1)}, u32[]{:S(2)}, u32[]{:S(2)}) collective-permute-start(bf16[128,2,128]{2,0,1:T(8,128)(2,1)S(1)} %get-tuple-element.352), channel_id=1, source_target_pairs={{0,32},{32,64},{64,96},{96,128},{128,160},{160,192},{192,224},{224... | collective-permute-start | bytes 196616 | tf_op jit(solution)/shard_map/while/body/eval_jaxpr/ppermute | solution.py:41
  266.3 4.1 %collective-permute-start = (bf16[128,2,128]{2,0,1:T(8,128)(2,1)S(1)}, bf16[128,2,128]{2,0,1:T(8,128)(2,1)S(1)}, u32[]{:S(2)}, u32[]{:S(2)}) collective-permute-start(bf16[128,2,128]{2,0,1:T(8,128)(2,1)S(1)} %get-tuple-element.351), channel_id=1, source_target_pairs={{0,32},{32,64},{64,96},{96,128},{128,160},{160,192},{192,224},{224... | collective-permute-start | bytes 196616 | tf_op jit(solution)/shard_map/while/body/eval_jaxpr/ppermute | solution.py:41
  275.3 3.9 %collective-permute-start = (bf16[128,2,128]{2,0,1:T(8,128)(2,1)S(1)}, bf16[128,2,128]{2,0,1:T(8,128)(2,1)S(1)}, u32[]{:S(2)}, u32[]{:S(2)}) collective-permute-start(bf16[128,2,128]{2,0,1:T(8,128)(2,1)S(1)} %get-tuple-element.351), channel_id=1, source_target_pairs={{0,32},{32,64},{64,96},{96,128},{128,160},{160,192},{192,224},{224... | collective-permute-start | bytes 196616 | tf_op jit(solution)/shard_map/while/body/eval_jaxpr/ppermute | solution.py:41
  279.2 4.6 %collective-permute-start.1 = (bf16[128,2,128]{2,0,1:T(8,128)(2,1)S(1)}, bf16[128,2,128]{2,0,1:T(8,128)(2,1)S(1)}, u32[]{:S(2)}, u32[]{:S(2)}) collective-permute-start(bf16[128,2,128]{2,0,1:T(8,128)(2,1)S(1)} %get-tuple-element.352), channel_id=1, source_target_pairs={{0,32},{32,64},{64,96},{96,128},{128,160},{160,192},{192,224},{224... | collective-permute-start | bytes 196616 | tf_op jit(solution)/shard_map/while/body/eval_jaxpr/ppermute | solution.py:41
  285.1 5.0 %collective-permute-start = (bf16[128,2,128]{2,0,1:T(8,128)(2,1)S(1)}, bf16[128,2,128]{2,0,1:T(8,128)(2,1)S(1)}, u32[]{:S(2)}, u32[]{:S(2)}) collective-permute-start(bf16[128,2,128]{2,0,1:T(8,128)(2,1)S(1)} %get-tuple-element.351), channel_id=1, source_target_pairs={{0,32},{32,64},{64,96},{96,128},{128,160},{160,192},{192,224},{224... | collective-permute-start | bytes 196616 | tf_op jit(solution)/shard_map/while/body/eval_jaxpr/ppermute | solution.py:41
  290.2 4.9 %collective-permute-start.1 = (bf16[128,2,128]{2,0,1:T(8,128)(2,1)S(1)}, bf16[128,2,128]{2,0,1:T(8,128)(2,1)S(1)}, u32[]{:S(2)}, u32[]{:S(2)}) collective-permute-start(bf16[128,2,128]{2,0,1:T(8,128)(2,1)S(1)} %get-tuple-element.352), channel_id=1, source_target_pairs={{0,32},{32,64},{64,96},{96,128},{128,160},{160,192},{192,224},{224... | collective-permute-start | bytes 196616 | tf_op jit(solution)/shard_map/while/body/eval_jaxpr/ppermute | solution.py:41
  296.4 4.1 %collective-permute-start = (bf16[128,2,128]{2,0,1:T(8,128)(2,1)S(1)}, bf16[128,2,128]{2,0,1:T(8,128)(2,1)S(1)}, u32[]{:S(2)}, u32[]{:S(2)}) collective-permute-start(bf16[128,2,128]{2,0,1:T(8,128)(2,1)S(1)} %get-tuple-element.351), channel_id=1, source_target_pairs={{0,32},{32,64},{64,96},{96,128},{128,160},{160,192},{192,224},{224... | collective-permute-start | bytes 196616 | tf_op jit(solution)/shard_map/while/body/eval_jaxpr/ppermute | solution.py:41
  300.6 5.7 %collective-permute-start.1 = (bf16[128,2,128]{2,0,1:T(8,128)(2,1)S(1)}, bf16[128,2,128]{2,0,1:T(8,128)(2,1)S(1)}, u32[]{:S(2)}, u32[]{:S(2)}) collective-permute-start(bf16[128,2,128]{2,0,1:T(8,128)(2,1)S(1)} %get-tuple-element.352), channel_id=1, source_target_pairs={{0,32},{32,64},{64,96},{96,128},{128,160},{160,192},{192,224},{224... | collective-permute-start | bytes 196616 | tf_op jit(solution)/shard_map/while/body/eval_jaxpr/ppermute | solution.py:41
  307.6 4.1 %collective-permute-start = (bf16[128,2,128]{2,0,1:T(8,128)(2,1)S(1)}, bf16[128,2,128]{2,0,1:T(8,128)(2,1)S(1)}, u32[]{:S(2)}, u32[]{:S(2)}) collective-permute-start(bf16[128,2,128]{2,0,1:T(8,128)(2,1)S(1)} %get-tuple-element.351), channel_id=1, source_target_pairs={{0,32},{32,64},{64,96},{96,128},{128,160},{160,192},{192,224},{224... | collective-permute-start | bytes 196616 | tf_op jit(solution)/shard_map/while/body/eval_jaxpr/ppermute | solution.py:41
  311.7 4.6 %collective-permute-start.1 = (bf16[128,2,128]{2,0,1:T(8,128)(2,1)S(1)}, bf16[128,2,128]{2,0,1:T(8,128)(2,1)S(1)}, u32[]{:S(2)}, u32[]{:S(2)}) collective-permute-start(bf16[128,2,128]{2,0,1:T(8,128)(2,1)S(1)} %get-tuple-element.352), channel_id=1, source_target_pairs={{0,32},{32,64},{64,96},{96,128},{128,160},{160,192},{192,224},{224... | collective-permute-start | bytes 196616 | tf_op jit(solution)/shard_map/while/body/eval_jaxpr/ppermute | solution.py:41
  317.7 4.1 %collective-permute-start = (bf16[128,2,128]{2,0,1:T(8,128)(2,1)S(1)}, bf16[128,2,128]{2,0,1:T(8,128)(2,1)S(1)}, u32[]{:S(2)}, u32[]{:S(2)}) collective-permute-start(bf16[128,2,128]{2,0,1:T(8,128)(2,1)S(1)} %get-tuple-element.351), channel_id=1, source_target_pairs={{0,32},{32,64},{64,96},{96,128},{128,160},{160,192},{192,224},{224... | collective-permute-start | bytes 196616 | tf_op jit(solution)/shard_map/while/body/eval_jaxpr/ppermute | solution.py:41
  330.5 3.9 %collective-permute-start.1 = (bf16[128,2,128]{2,0,1:T(8,128)(2,1)S(1)}, bf16[128,2,128]{2,0,1:T(8,128)(2,1)S(1)}, u32[]{:S(2)}, u32[]{:S(2)}) collective-permute-start(bf16[128,2,128]{2,0,1:T(8,128)(2,1)S(1)} %get-tuple-element.352), channel_id=1, source_target_pairs={{0,32},{32,64},{64,96},{96,128},{128,160},{160,192},{192,224},{224... | collective-permute-start | bytes 196616 | tf_op jit(solution)/shard_map/while/body/eval_jaxpr/ppermute | solution.py:41
  343.2 28.3 %all_to_all.15 = bf16[8,16,2048]{2,1,0:T(8,128)(2,1)S(1)} all-to-all(bf16[8,16,2048]{2,1,0:T(8,128)(2,1)S(1)} %bitcast.127), channel_id=1, replica_groups=mesh['sp'=16,'fs'=4,'tp'=8] {'tp'}, dimensions={0} | all-to-all | bytes 1048576 | tf_op jit(solution)/shard_map/all_to_all | solution.py:86
  (183 shorter events, 87.4 us)
Async XLA Ops:
  6.5 107.4 %all-gather.3.cloned.1.call-start = ((), (), s32[]{:S(2)}) async-start(), calls=%async_computation.3 | async-start | bytes 6684672 | tf_op jit(solution)/shard_map/all_gather | solution.py:24
  28.7 95.1 %all-to-all-start.1 = ((bf16[16,1,4]{2,1,0:T(2,128)(2,1)}), bf16[16,1,4]{2,1,0:T(2,128)(2,1)S(1)}, u32[]{:S(2)}, u32[]{:S(2)}) async-start(bf16[16,1,4]{2,1,0:T(2,128)(2,1)} %broadcast_in_dim.93), calls=%async_computation.1 | async-start | bytes 16384 | tf_op jit(solution)/shard_map/all_to_all | solution.py:46
  43.9 295.9 %all-gather.5.cloned.1.call-start = ((), (), s32[]{:S(2)}) async-start(), calls=%async_computation.4 | async-start | bytes 2129920 | tf_op jit(solution)/shard_map/all_gather | solution.py:30
  115.5 7.1 %collective-permute-start.4 = (bf16[3,128]{1,0:T(4,128)(2,1)S(1)}, bf16[3,128]{1,0:T(4,128)(2,1)S(1)}, u32[]{:S(2)}, u32[]{:S(2)}) collective-permute-start(bf16[3,128]{1,0:T(4,128)(2,1)S(1)} %slice.195), channel_id=1, source_target_pairs={{0,32},{32,64},{64,96},{96,128},{128,160},{160,192},{192,224},{224... | collective-permute-start | bytes 2312 | tf_op jit(solution)/shard_map/ppermute | solution.py:41
  125.1 211.6 %all-to-all-start = ((bf16[16,1,4,64,128]{4,3,2,1,0:T(8,128)(2,1)}), bf16[16,1,4,64,128]{4,3,2,1,0:T(8,128)(2,1)S(1)}, u32[]{:S(2)}, u32[]{:S(2)}) async-start(bf16[16,1,4,64,128]{4,3,2,1,0:T(8,128)(2,1)} %broadcast_in_dim.90), calls=%async_computation | async-start | bytes 2097152 | tf_op jit(solution)/shard_map/all_to_all | solution.py:46
  148.2 188.3 %collective-permute-start.3 = (bf16[3,128]{1,0:T(4,128)(2,1)S(1)}, bf16[3,128]{1,0:T(4,128)(2,1)S(1)}, u32[]{:S(2)}, u32[]{:S(2)}) collective-permute-start(bf16[3,128]{1,0:T(4,128)(2,1)S(1)} %slice.190), channel_id=1, source_target_pairs={{0,32},{32,64},{64,96},{96,128},{128,160},{160,192},{192,224},{224... | collective-permute-start | bytes 2312 | tf_op jit(solution)/shard_map/ppermute | solution.py:41
  151.5 23.0 %collective-permute-start = (bf16[128,2,128]{2,0,1:T(8,128)(2,1)S(1)}, bf16[128,2,128]{2,0,1:T(8,128)(2,1)S(1)}, u32[]{:S(2)}, u32[]{:S(2)}) collective-permute-start(bf16[128,2,128]{2,0,1:T(8,128)(2,1)S(1)} %get-tuple-element.351), channel_id=1, source_target_pairs={{0,32},{32,64},{64,96},{96,128},{128,160},{160,192},{192,224},{224... | collective-permute-start | bytes 196616 | tf_op jit(solution)/shard_map/while/body/eval_jaxpr/ppermute | solution.py:41
  154.6 25.8 %collective-permute-start.1 = (bf16[128,2,128]{2,0,1:T(8,128)(2,1)S(1)}, bf16[128,2,128]{2,0,1:T(8,128)(2,1)S(1)}, u32[]{:S(2)}, u32[]{:S(2)}) collective-permute-start(bf16[128,2,128]{2,0,1:T(8,128)(2,1)S(1)} %get-tuple-element.352), channel_id=1, source_target_pairs={{0,32},{32,64},{64,96},{96,128},{128,160},{160,192},{192,224},{224... | collective-permute-start | bytes 196616 | tf_op jit(solution)/shard_map/while/body/eval_jaxpr/ppermute | solution.py:41
  180.4 17.9 %collective-permute-start = (bf16[128,2,128]{2,0,1:T(8,128)(2,1)S(1)}, bf16[128,2,128]{2,0,1:T(8,128)(2,1)S(1)}, u32[]{:S(2)}, u32[]{:S(2)}) collective-permute-start(bf16[128,2,128]{2,0,1:T(8,128)(2,1)S(1)} %get-tuple-element.351), channel_id=1, source_target_pairs={{0,32},{32,64},{64,96},{96,128},{128,160},{160,192},{192,224},{224... | collective-permute-start | bytes 196616 | tf_op jit(solution)/shard_map/while/body/eval_jaxpr/ppermute | solution.py:41
  199.6 9.9 %collective-permute-start = (bf16[128,2,128]{2,0,1:T(8,128)(2,1)S(1)}, bf16[128,2,128]{2,0,1:T(8,128)(2,1)S(1)}, u32[]{:S(2)}, u32[]{:S(2)}) collective-permute-start(bf16[128,2,128]{2,0,1:T(8,128)(2,1)S(1)} %get-tuple-element.351), channel_id=1, source_target_pairs={{0,32},{32,64},{64,96},{96,128},{128,160},{160,192},{192,224},{224... | collective-permute-start | bytes 196616 | tf_op jit(solution)/shard_map/while/body/eval_jaxpr/ppermute | solution.py:41
  203.3 7.5 %collective-permute-start.1 = (bf16[128,2,128]{2,0,1:T(8,128)(2,1)S(1)}, bf16[128,2,128]{2,0,1:T(8,128)(2,1)S(1)}, u32[]{:S(2)}, u32[]{:S(2)}) collective-permute-start(bf16[128,2,128]{2,0,1:T(8,128)(2,1)S(1)} %get-tuple-element.352), channel_id=1, source_target_pairs={{0,32},{32,64},{64,96},{96,128},{128,160},{160,192},{192,224},{224... | collective-permute-start | bytes 196616 | tf_op jit(solution)/shard_map/while/body/eval_jaxpr/ppermute | solution.py:41
  210.9 8.7 %collective-permute-start = (bf16[128,2,128]{2,0,1:T(8,128)(2,1)S(1)}, bf16[128,2,128]{2,0,1:T(8,128)(2,1)S(1)}, u32[]{:S(2)}, u32[]{:S(2)}) collective-permute-start(bf16[128,2,128]{2,0,1:T(8,128)(2,1)S(1)} %get-tuple-element.351), channel_id=1, source_target_pairs={{0,32},{32,64},{64,96},{96,128},{128,160},{160,192},{192,224},{224... | collective-permute-start | bytes 196616 | tf_op jit(solution)/shard_map/while/body/eval_jaxpr/ppermute | solution.py:41
  214.6 6.3 %collective-permute-start.1 = (bf16[128,2,128]{2,0,1:T(8,128)(2,1)S(1)}, bf16[128,2,128]{2,0,1:T(8,128)(2,1)S(1)}, u32[]{:S(2)}, u32[]{:S(2)}) collective-permute-start(bf16[128,2,128]{2,0,1:T(8,128)(2,1)S(1)} %get-tuple-element.352), channel_id=1, source_target_pairs={{0,32},{32,64},{64,96},{96,128},{128,160},{160,192},{192,224},{224... | collective-permute-start | bytes 196616 | tf_op jit(solution)/shard_map/while/body/eval_jaxpr/ppermute | solution.py:41
  220.9 11.5 %collective-permute-start = (bf16[128,2,128]{2,0,1:T(8,128)(2,1)S(1)}, bf16[128,2,128]{2,0,1:T(8,128)(2,1)S(1)}, u32[]{:S(2)}, u32[]{:S(2)}) collective-permute-start(bf16[128,2,128]{2,0,1:T(8,128)(2,1)S(1)} %get-tuple-element.351), channel_id=1, source_target_pairs={{0,32},{32,64},{64,96},{96,128},{128,160},{160,192},{192,224},{224... | collective-permute-start | bytes 196616 | tf_op jit(solution)/shard_map/while/body/eval_jaxpr/ppermute | solution.py:41
  228.1 6.0 %collective-permute-start.1 = (bf16[128,2,128]{2,0,1:T(8,128)(2,1)S(1)}, bf16[128,2,128]{2,0,1:T(8,128)(2,1)S(1)}, u32[]{:S(2)}, u32[]{:S(2)}) collective-permute-start(bf16[128,2,128]{2,0,1:T(8,128)(2,1)S(1)} %get-tuple-element.352), channel_id=1, source_target_pairs={{0,32},{32,64},{64,96},{96,128},{128,160},{160,192},{192,224},{224... | collective-permute-start | bytes 196616 | tf_op jit(solution)/shard_map/while/body/eval_jaxpr/ppermute | solution.py:41
  234.1 8.6 %collective-permute-start = (bf16[128,2,128]{2,0,1:T(8,128)(2,1)S(1)}, bf16[128,2,128]{2,0,1:T(8,128)(2,1)S(1)}, u32[]{:S(2)}, u32[]{:S(2)}) collective-permute-start(bf16[128,2,128]{2,0,1:T(8,128)(2,1)S(1)} %get-tuple-element.351), channel_id=1, source_target_pairs={{0,32},{32,64},{64,96},{96,128},{128,160},{160,192},{192,224},{224... | collective-permute-start | bytes 196616 | tf_op jit(solution)/shard_map/while/body/eval_jaxpr/ppermute | solution.py:41
  238.4 5.8 %collective-permute-start.1 = (bf16[128,2,128]{2,0,1:T(8,128)(2,1)S(1)}, bf16[128,2,128]{2,0,1:T(8,128)(2,1)S(1)}, u32[]{:S(2)}, u32[]{:S(2)}) collective-permute-start(bf16[128,2,128]{2,0,1:T(8,128)(2,1)S(1)} %get-tuple-element.352), channel_id=1, source_target_pairs={{0,32},{32,64},{64,96},{96,128},{128,160},{160,192},{192,224},{224... | collective-permute-start | bytes 196616 | tf_op jit(solution)/shard_map/while/body/eval_jaxpr/ppermute | solution.py:41
  244.2 8.3 %collective-permute-start = (bf16[128,2,128]{2,0,1:T(8,128)(2,1)S(1)}, bf16[128,2,128]{2,0,1:T(8,128)(2,1)S(1)}, u32[]{:S(2)}, u32[]{:S(2)}) collective-permute-start(bf16[128,2,128]{2,0,1:T(8,128)(2,1)S(1)} %get-tuple-element.351), channel_id=1, source_target_pairs={{0,32},{32,64},{64,96},{96,128},{128,160},{160,192},{192,224},{224... | collective-permute-start | bytes 196616 | tf_op jit(solution)/shard_map/while/body/eval_jaxpr/ppermute | solution.py:41
  253.8 11.0 %collective-permute-start = (bf16[128,2,128]{2,0,1:T(8,128)(2,1)S(1)}, bf16[128,2,128]{2,0,1:T(8,128)(2,1)S(1)}, u32[]{:S(2)}, u32[]{:S(2)}) collective-permute-start(bf16[128,2,128]{2,0,1:T(8,128)(2,1)S(1)} %get-tuple-element.351), channel_id=1, source_target_pairs={{0,32},{32,64},{64,96},{96,128},{128,160},{160,192},{192,224},{224... | collective-permute-start | bytes 196616 | tf_op jit(solution)/shard_map/while/body/eval_jaxpr/ppermute | solution.py:41
  259.5 6.8 %collective-permute-start.1 = (bf16[128,2,128]{2,0,1:T(8,128)(2,1)S(1)}, bf16[128,2,128]{2,0,1:T(8,128)(2,1)S(1)}, u32[]{:S(2)}, u32[]{:S(2)}) collective-permute-start(bf16[128,2,128]{2,0,1:T(8,128)(2,1)S(1)} %get-tuple-element.352), channel_id=1, source_target_pairs={{0,32},{32,64},{64,96},{96,128},{128,160},{160,192},{192,224},{224... | collective-permute-start | bytes 196616 | tf_op jit(solution)/shard_map/while/body/eval_jaxpr/ppermute | solution.py:41
  266.3 7.7 %collective-permute-start = (bf16[128,2,128]{2,0,1:T(8,128)(2,1)S(1)}, bf16[128,2,128]{2,0,1:T(8,128)(2,1)S(1)}, u32[]{:S(2)}, u32[]{:S(2)}) collective-permute-start(bf16[128,2,128]{2,0,1:T(8,128)(2,1)S(1)} %get-tuple-element.351), channel_id=1, source_target_pairs={{0,32},{32,64},{64,96},{96,128},{128,160},{160,192},{192,224},{224... | collective-permute-start | bytes 196616 | tf_op jit(solution)/shard_map/while/body/eval_jaxpr/ppermute | solution.py:41
  275.3 8.5 %collective-permute-start = (bf16[128,2,128]{2,0,1:T(8,128)(2,1)S(1)}, bf16[128,2,128]{2,0,1:T(8,128)(2,1)S(1)}, u32[]{:S(2)}, u32[]{:S(2)}) collective-permute-start(bf16[128,2,128]{2,0,1:T(8,128)(2,1)S(1)} %get-tuple-element.351), channel_id=1, source_target_pairs={{0,32},{32,64},{64,96},{96,128},{128,160},{160,192},{192,224},{224... | collective-permute-start | bytes 196616 | tf_op jit(solution)/shard_map/while/body/eval_jaxpr/ppermute | solution.py:41
  279.2 5.9 %collective-permute-start.1 = (bf16[128,2,128]{2,0,1:T(8,128)(2,1)S(1)}, bf16[128,2,128]{2,0,1:T(8,128)(2,1)S(1)}, u32[]{:S(2)}, u32[]{:S(2)}) collective-permute-start(bf16[128,2,128]{2,0,1:T(8,128)(2,1)S(1)} %get-tuple-element.352), channel_id=1, source_target_pairs={{0,32},{32,64},{64,96},{96,128},{128,160},{160,192},{192,224},{224... | collective-permute-start | bytes 196616 | tf_op jit(solution)/shard_map/while/body/eval_jaxpr/ppermute | solution.py:41
  285.1 10.0 %collective-permute-start = (bf16[128,2,128]{2,0,1:T(8,128)(2,1)S(1)}, bf16[128,2,128]{2,0,1:T(8,128)(2,1)S(1)}, u32[]{:S(2)}, u32[]{:S(2)}) collective-permute-start(bf16[128,2,128]{2,0,1:T(8,128)(2,1)S(1)} %get-tuple-element.351), channel_id=1, source_target_pairs={{0,32},{32,64},{64,96},{96,128},{128,160},{160,192},{192,224},{224... | collective-permute-start | bytes 196616 | tf_op jit(solution)/shard_map/while/body/eval_jaxpr/ppermute | solution.py:41
  290.2 6.3 %collective-permute-start.1 = (bf16[128,2,128]{2,0,1:T(8,128)(2,1)S(1)}, bf16[128,2,128]{2,0,1:T(8,128)(2,1)S(1)}, u32[]{:S(2)}, u32[]{:S(2)}) collective-permute-start(bf16[128,2,128]{2,0,1:T(8,128)(2,1)S(1)} %get-tuple-element.352), channel_id=1, source_target_pairs={{0,32},{32,64},{64,96},{96,128},{128,160},{160,192},{192,224},{224... | collective-permute-start | bytes 196616 | tf_op jit(solution)/shard_map/while/body/eval_jaxpr/ppermute | solution.py:41
  296.4 9.8 %collective-permute-start = (bf16[128,2,128]{2,0,1:T(8,128)(2,1)S(1)}, bf16[128,2,128]{2,0,1:T(8,128)(2,1)S(1)}, u32[]{:S(2)}, u32[]{:S(2)}) collective-permute-start(bf16[128,2,128]{2,0,1:T(8,128)(2,1)S(1)} %get-tuple-element.351), channel_id=1, source_target_pairs={{0,32},{32,64},{64,96},{96,128},{128,160},{160,192},{192,224},{224... | collective-permute-start | bytes 196616 | tf_op jit(solution)/shard_map/while/body/eval_jaxpr/ppermute | solution.py:41
  300.6 7.0 %collective-permute-start.1 = (bf16[128,2,128]{2,0,1:T(8,128)(2,1)S(1)}, bf16[128,2,128]{2,0,1:T(8,128)(2,1)S(1)}, u32[]{:S(2)}, u32[]{:S(2)}) collective-permute-start(bf16[128,2,128]{2,0,1:T(8,128)(2,1)S(1)} %get-tuple-element.352), channel_id=1, source_target_pairs={{0,32},{32,64},{64,96},{96,128},{128,160},{160,192},{192,224},{224... | collective-permute-start | bytes 196616 | tf_op jit(solution)/shard_map/while/body/eval_jaxpr/ppermute | solution.py:41
  307.6 8.8 %collective-permute-start = (bf16[128,2,128]{2,0,1:T(8,128)(2,1)S(1)}, bf16[128,2,128]{2,0,1:T(8,128)(2,1)S(1)}, u32[]{:S(2)}, u32[]{:S(2)}) collective-permute-start(bf16[128,2,128]{2,0,1:T(8,128)(2,1)S(1)} %get-tuple-element.351), channel_id=1, source_target_pairs={{0,32},{32,64},{64,96},{96,128},{128,160},{160,192},{192,224},{224... | collective-permute-start | bytes 196616 | tf_op jit(solution)/shard_map/while/body/eval_jaxpr/ppermute | solution.py:41
  311.7 5.9 %collective-permute-start.1 = (bf16[128,2,128]{2,0,1:T(8,128)(2,1)S(1)}, bf16[128,2,128]{2,0,1:T(8,128)(2,1)S(1)}, u32[]{:S(2)}, u32[]{:S(2)}) collective-permute-start(bf16[128,2,128]{2,0,1:T(8,128)(2,1)S(1)} %get-tuple-element.352), channel_id=1, source_target_pairs={{0,32},{32,64},{64,96},{96,128},{128,160},{160,192},{192,224},{224... | collective-permute-start | bytes 196616 | tf_op jit(solution)/shard_map/while/body/eval_jaxpr/ppermute | solution.py:41
  317.7 7.8 %collective-permute-start = (bf16[128,2,128]{2,0,1:T(8,128)(2,1)S(1)}, bf16[128,2,128]{2,0,1:T(8,128)(2,1)S(1)}, u32[]{:S(2)}, u32[]{:S(2)}) collective-permute-start(bf16[128,2,128]{2,0,1:T(8,128)(2,1)S(1)} %get-tuple-element.351), channel_id=1, source_target_pairs={{0,32},{32,64},{64,96},{96,128},{128,160},{160,192},{192,224},{224... | collective-permute-start | bytes 196616 | tf_op jit(solution)/shard_map/while/body/eval_jaxpr/ppermute | solution.py:41
  326.8 7.6 %collective-permute-start = (bf16[128,2,128]{2,0,1:T(8,128)(2,1)S(1)}, bf16[128,2,128]{2,0,1:T(8,128)(2,1)S(1)}, u32[]{:S(2)}, u32[]{:S(2)}) collective-permute-start(bf16[128,2,128]{2,0,1:T(8,128)(2,1)S(1)} %get-tuple-element.351), channel_id=1, source_target_pairs={{0,32},{32,64},{64,96},{96,128},{128,160},{160,192},{192,224},{224... | collective-permute-start | bytes 196616 | tf_op jit(solution)/shard_map/while/body/eval_jaxpr/ppermute | solution.py:41
  330.5 5.7 %collective-permute-start.1 = (bf16[128,2,128]{2,0,1:T(8,128)(2,1)S(1)}, bf16[128,2,128]{2,0,1:T(8,128)(2,1)S(1)}, u32[]{:S(2)}, u32[]{:S(2)}) collective-permute-start(bf16[128,2,128]{2,0,1:T(8,128)(2,1)S(1)} %get-tuple-element.352), channel_id=1, source_target_pairs={{0,32},{32,64},{64,96},{96,128},{128,160},{160,192},{192,224},{224... | collective-permute-start | bytes 196616 | tf_op jit(solution)/shard_map/while/body/eval_jaxpr/ppermute | solution.py:41
  (8 other events, 309.3 us)
Sparse Core Ops, SparseCore 0:
  23.8 90.0 all-gather.2
  116.8 142.3 all-gather.4
where the time goes:
time: 386 us; the launch traced here: 379 us
  starting transfers between devices  178 us (46%)
  waiting for transfers between devices  108 us (28%)
  blocking collectives  40.3 us (10%)
  matrix products  17.4 us (5%)
  between operations  13.8 us (4%)
  local copies, waits for them, and re-layouts  12.9 us (3%)
  other arithmetic  7.7 us (2%)
    ppermute x33, starting transfers between devices, passed_along(): return lax.ppermute(shard, axis, pairs)  150 us
    all_gather x1, waiting for transfers between devices, side_by_side(): lax.all_gather(both, axis, axis=dim, tiled=True)  65.2 us
    ppermute x33, waiting for transfers between devices, passed_along(): return lax.ppermute(shard, axis, pairs)  42.7 us
    all_to_all x1, blocking collectives, summed_on_arrival(): lax.all_to_all(cut_along(shard, dim, length), axis, 0, 0, tiled=True)  28.3 us
    all_to_all x2, starting transfers between devices, copy_for_each(): lax.all_to_all(jnp.broadcast_to(shard[None], (length, *shard.shape)), axi...  27.9 us
    all_gather x1, blocking collectives, side_by_side(): lax.all_gather(both, axis, axis=dim, tiled=True)  12 us
    dot_general x7, matrix products, body(): jnp.dot(normed, piece_rows, preferred_element_type=jnp.float32)  11.2 us
  transfers between devices with their start and end apart: 37, of which 18 were waited for; matrix products, arithmetic and copies ran while one was open for 8% of the time, Pallas kernels for 0%

commit v1 on v0

v1 whole, which is shorter than its diff:
```python
import jax
import jax.numpy as jnp
from jax import lax
from jax.experimental import pallas as pl
from jax.experimental.pallas import tpu as pltpu
from jax.sharding import PartitionSpec as P

BLOCK = 128
CONV = 4
EPS = 1e-06
HALO = 16
F32 = jnp.float32
BF16 = jnp.bfloat16
HIGH = lax.Precision.HIGHEST
NT = (((1,), (1,)), ((), ()))
TN = (((0,), (0,)), ((), ()))


def vmem(limit=48):
    return pltpu.CompilerParams(vmem_limit_bytes=limit * 1024 * 1024)


def iota(shape, dim):
    return lax.broadcasted_iota(jnp.int32, shape, dim)


def softplus(x):
    return jnp.maximum(x, 0.0) + jnp.log1p(jnp.exp(-jnp.abs(x)))


def silu(x):
    return x / (1.0 + jnp.exp(-x))


def norm_kernel(x_ref, gain_ref, ws_ref, xs_ref, step_ref):
    x = x_ref[0].astype(F32)
    scale = lax.rsqrt(jnp.mean(x * x, axis=-1, keepdims=True) + EPS)
    normed = (x * scale * gain_ref[...]).astype(BF16)
    step_ref[...] = softplus(lax.dot_general(ws_ref[...], normed, NT, preferred_element_type=F32))
    wide = normed.astype(F32)
    lane = iota((x.shape[0], 128), 1) // 32
    for f in range(4):
        for g in range(4):
            out = None
            for k in range(4):
                at = (4 * g + k) * 128
                piece = wide[:, at : at + 128]
                shift = ((k - f) * 32) % 128
                if shift:
                    piece = pltpu.roll(piece, shift, 1)
                out = piece if out is None else jnp.where(lane == k, piece, out)
            xs_ref[f, :, g * 128 : (g + 1) * 128] = out.astype(BF16)


def norm_call(inputs, gain, w_step_t):
    rows, width = inputs.shape[1:]
    return pl.pallas_call(
        norm_kernel,
        out_shape=(
            jax.ShapeDtypeStruct((4, rows, width // 4), BF16),
            jax.ShapeDtypeStruct((w_step_t.shape[0], rows), F32),
        ),
        compiler_params=vmem(),
        name="norm",
    )(inputs, gain.reshape(1, -1), w_step_t)


def pack_kernel(g, i, b, c, q, k, v, om, oa, first, second):
    at = 0
    for r in (k, v):
        first[:, at : at + r.shape[1]] = r[...]
        at += r.shape[1]
    at = 0
    for r in (g, i, b, c, q, om, oa):
        second[:, at : at + r.shape[1]] = r[...]
        at += r.shape[1]


def pack_call(g, i, b, c, q, k, v, om, oa):
    rows = g.shape[0]
    w1 = k.shape[1] + v.shape[1]
    w2 = sum(a.shape[1] for a in (g, i, b, c, q, om, oa))
    return pl.pallas_call(
        pack_kernel,
        out_shape=(
            jax.ShapeDtypeStruct((rows, w1), BF16),
            jax.ShapeDtypeStruct((rows, w2), BF16),
        ),
        compiler_params=vmem(),
        name="pack",
    )(g, i, b, c, q, k, v, om, oa)


def local_kernel(
    ids, rate, act_ref, step_ref, off_ref, ci_ref, cb_ref, cc_ref,
    yin_ref, gate_ref, cq_ref, cum_ref, send_ref, wide_ref,
):
    tensor = ids[1]
    total = act_ref[0, :, 0:768].astype(F32)
    for j in range(1, 4):
        total = total + act_ref[j, :, 0:768].astype(F32)
    act = total.astype(BF16).astype(F32)
    gate_ref[...] = act[HALO:, 0:256]
    wide_ref[...] = act[:, 256:768]
    taps = jnp.concatenate([ci_ref[...], cb_ref[...], cc_ref[...]], axis=1)
    summed = None
    for i in range(CONV):
        part = taps[i : i + 1] * wide_ref[HALO - CONV + 1 + i : HALO - CONV + 1 + i + BLOCK, :]
        summed = part if summed is None else summed + part
    conv = silu(summed).astype(BF16)
    xin, bkey, cquery = conv[:, 0:256], conv[:, 256:384], conv[:, 384:512]
    cq_ref[...] = cquery
    row = iota((BLOCK, BLOCK), 0)
    col = iota((BLOCK, BLOCK), 1)
    lower = row >= col
    step = jnp.concatenate(
        [step_ref[pl.ds(4 * tensor + h, 1), :] for h in range(4)], axis=0
    )
    rates = jnp.concatenate(
        [jnp.full((1, BLOCK), rate[4 * tensor + h], F32) for h in range(4)], axis=0
    )
    decay = off_ref[...] - rates * step
    pad = jnp.zeros((4, BLOCK), F32)
    decay8 = jnp.concatenate([decay, pad], axis=0)
    upper = (row <= col).astype(F32)
    cum = jnp.dot(decay8, upper, precision=HIGH, preferred_element_type=F32)
    last = jnp.sum(decay, axis=1, keepdims=True)
    to_end = jnp.exp(last - cum[0:4]) * step
    eye = (row == col).astype(F32)
    rows = jnp.concatenate([cum[0:4], to_end], axis=0)
    cols = lax.dot_general(eye, rows, NT, precision=HIGH, preferred_element_type=F32)
    cum_ref[...] = cols
    inner = lax.dot_general(cquery, bkey, NT, preferred_element_type=F32)
    wide_key = bkey.astype(F32)
    ys = []
    for h in range(4):
        spread = cols[:, h : h + 1] - cum[h : h + 1]
        decayed = jnp.exp(jnp.where(lower, spread, 0.0))
        mix = jnp.where(lower, inner * decayed * step[h : h + 1], 0.0).astype(BF16)
        xh = xin[:, h * 64 : (h + 1) * 64]
        ys.append(jnp.dot(mix, xh, preferred_element_type=F32))
        wk = (wide_key * cols[:, 4 + h : 5 + h]).astype(BF16)
        state = lax.dot_general(xh, wk, TN, preferred_element_type=F32).astype(BF16)
        log = jnp.broadcast_to(last[h : h + 1], (8, BLOCK))
        high = log.astype(BF16).astype(F32)
        logs = jnp.concatenate([high, log - high], axis=0).astype(BF16)
        for j in range(4):
            send_ref[4 * h + j, 0:16, :] = state[16 * j : 16 * (j + 1), :]
            send_ref[4 * h + j, 16:32, :] = logs
    yin_ref[...] = jnp.concatenate(ys, axis=1)


def local_call(ids, rate, act, step, offset, conv_weight):
    full = lambda *shape: pl.BlockSpec(shape, lambda i, ids, rate: (0,) * len(shape))
    return pl.pallas_call(
        local_kernel,
        grid_spec=pltpu.PrefetchScalarGridSpec(
            num_scalar_prefetch=2,
            grid=(1,),
            in_specs=[
                full(*act.shape),
                full(*step.shape),
                full(*offset.shape),
                pl.BlockSpec((CONV, 256), lambda i, ids, rate: (0, ids[1])),
                pl.BlockSpec((CONV, 128), lambda i, ids, rate: (0, 16 + ids[1])),
                pl.BlockSpec((CONV, 128), lambda i, ids, rate: (0, 24 + ids[1])),
            ],
            out_specs=[
                full(BLOCK, 256), full(BLOCK, 256), full(BLOCK, 128), full(BLOCK, 8),
                full(16, 32, 128),
            ],
            scratch_shapes=[pltpu.VMEM((BLOCK + HALO, 512), F32)],
        ),
        out_shape=(
            jax.ShapeDtypeStruct((BLOCK, 256), F32),
            jax.ShapeDtypeStruct((BLOCK, 256), F32),
            jax.ShapeDtypeStruct((BLOCK, 128), BF16),
            jax.ShapeDtypeStruct((BLOCK, 8), F32),
            jax.ShapeDtypeStruct((16, 32, 128), BF16),
        ),
        compiler_params=vmem(),
        name="ssd_local",
    )(ids, rate, act, step, offset, conv_weight, conv_weight, conv_weight)


def scan_kernel(got_ref, out_ref):
    held = jnp.zeros((16, 128), F32)
    for k in range(16):
        out_ref[k] = held.astype(BF16)
        logs = got_ref[k, 16:32, :].astype(F32)
        decay = jnp.exp(logs[0:8] + logs[8:16])
        held = held * jnp.concatenate([decay, decay], axis=0) + got_ref[k, 0:16, :].astype(F32)


def scan_call(got):
    return pl.pallas_call(
        scan_kernel,
        out_shape=jax.ShapeDtypeStruct((16, 16, 128), BF16),
        name="state_scan",
    )(got)


def carry_kernel(ids, enter_ref, yin_ref, gate_ref, cq_ref, cum_ref, gain_ref, out_ref):
    cquery = cq_ref[...]
    ys = []
    for h in range(4):
        enter = enter_ref[64 * h : 64 * (h + 1), :]
        moved = lax.dot_general(cquery, enter, NT, preferred_element_type=F32)
        ys.append(moved * jnp.exp(cum_ref[:, h : h + 1]))
    total = yin_ref[...] + jnp.concatenate(ys, axis=1)
    gated = total * silu(gate_ref[...])
    scale = lax.rsqrt(jnp.mean(gated * gated, axis=-1, keepdims=True) + EPS)
    out_ref[...] = (gated * scale * gain_ref[...]).astype(BF16)


def carry_call(ids, enter, yin, gate, cq, cum, gain):
    full = lambda *shape: pl.BlockSpec(shape, lambda i, ids: (0,) * len(shape))
    return pl.pallas_call(
        carry_kernel,
        grid_spec=pltpu.PrefetchScalarGridSpec(
            num_scalar_prefetch=1,
            grid=(1,),
            in_specs=[
                full(256, 128), full(BLOCK, 256), full(BLOCK, 256), full(BLOCK, 128),
                full(BLOCK, 8), pl.BlockSpec((1, 256), lambda i, ids: (0, ids[1])),
            ],
            out_specs=full(BLOCK, 256),
        ),
        out_shape=jax.ShapeDtypeStruct((BLOCK, 256), BF16),
        compiler_params=vmem(),
        name="ssd_carry",
    )(ids, enter, yin, gate, cq, cum, gain.reshape(1, -1))


KEYS = 256


def attend_kernel(ids, bias, qp_ref, kv_ref, mix_ref, w0, w1, w2, w3, out_ref, w_ref, acc_ref, late_ref, sems):
    block = ids[0]
    mine = ids[2]
    copies = [
        pltpu.make_async_copy(w, w_ref.at[(mine + 4 - r) % 4], sems.at[r])
        for r, w in enumerate((w0, w1, w2, w3))
    ]
    for copy in copies:
        copy.start()
    queries = qp_ref[0, HALO:, :].astype(F32)
    for j in range(1, 4):
        queries = queries + qp_ref[j, HALO:, :].astype(F32)
    queries = queries.astype(BF16)
    acc_ref[...] = jnp.zeros_like(acc_ref)
    late_ref[...] = jnp.zeros_like(late_ref)
    after = (iota((KEYS, KEYS), 0) > iota((KEYS, KEYS), 1)).astype(BF16)
    ones = jnp.ones((KEYS, 128), BF16)
    spot = block * BLOCK + iota((BLOCK, KEYS), 0)
    for at in range(kv_ref.shape[0] - KEYS, -1, -KEYS):

        @pl.when(at <= block * BLOCK)
        def _(at=at):
            before = (at + iota((BLOCK, KEYS), 1)) < spot
            for h in range(2):
                key = kv_ref[at : at + KEYS, h * 128 : (h + 1) * 128]
                value = kv_ref[at : at + KEYS, 256 + h * 128 : 256 + (h + 1) * 128]
                query = queries[:, h * 128 : (h + 1) * 128]
                logits = lax.dot_general(query, key, NT, preferred_element_type=F32)
                logits = logits * (128 ** -0.5) + bias[2 * ids[1] + h]
                soft = jnp.maximum(logits, 0.0) + jnp.log1p(jnp.exp(-jnp.abs(logits)))
                passed = jnp.where(before, -soft, 0.0)
                high = passed.astype(BF16)
                low = (passed - high.astype(F32)).astype(BF16)
                tail = jnp.dot(high, after, preferred_element_type=F32) + jnp.dot(
                    low, after, preferred_element_type=F32
                )
                whole = jnp.dot(high, ones, preferred_element_type=F32) + jnp.dot(
                    low, ones, preferred_element_type=F32
                )
                late = late_ref[h]
                late2 = jnp.concatenate([late] * (KEYS // 128), axis=1)
                weight = jnp.where(before, jnp.exp(logits - soft + tail + late2), 0.0)
                acc_ref[h] += jnp.dot(weight.astype(BF16), value, preferred_element_type=F32)
                late_ref[h] = late + whole

    both = jnp.concatenate(
        [mix_ref[...], acc_ref[0].astype(BF16), acc_ref[1].astype(BF16)], axis=1
    )
    for copy in copies:
        copy.wait()
    for s in range(16):
        piece = jnp.concatenate([w_ref[f, 32 * s : 32 * (s + 1), :] for f in range(4)], axis=0)
        out_ref[:, 128 * s : 128 * (s + 1)] = lax.dot_general(
            both, piece, NT, preferred_element_type=F32
        ).astype(BF16)


def attend_call(ids, bias, act, kv, mix, w):
    full = lambda *shape: pl.BlockSpec(shape, lambda i, ids, bias: (0,) * len(shape))
    hbm = pl.BlockSpec(memory_space=pl.ANY)
    return pl.pallas_call(
        attend_kernel,
        grid_spec=pltpu.PrefetchScalarGridSpec(
            num_scalar_prefetch=2,
            grid=(1,),
            in_specs=[
                pl.BlockSpec((4, BLOCK + HALO, 256), lambda i, ids, bias: (0, 0, 3)),
                full(*kv.shape), full(BLOCK, 256), hbm, hbm, hbm, hbm,
            ],
            out_specs=full(BLOCK, 2048),
            scratch_shapes=[
                pltpu.VMEM((4, 512, 512), BF16),
                pltpu.VMEM((2, BLOCK, 128), F32),
                pltpu.VMEM((2, BLOCK, 128), F32),
                pltpu.SemaphoreType.DMA((4,)),
            ],
        ),
        out_shape=jax.ShapeDtypeStruct((BLOCK, 2048), BF16),
        compiler_params=vmem(),
        name="attend",
    )(ids, bias, act, kv, mix, *w)


def rotated(shard, axis, by):
    length = lax.axis_size(axis)
    return lax.ppermute(shard, axis, [(i, (i + by) % length) for i in range(length)])


def body(
    inputs, norm_gain, w_gate, w_input, w_bkey, w_cquery, w_step, conv_weight, decay_rate,
    decay_offset, ssd_gain, w_query, w_key, w_value, stick_bias, out_mixer, out_attend,
):
    tensor = lax.axis_index("tp")
    seq = lax.axis_index("sp")
    part = lax.axis_index("fs")
    ids = jnp.stack([seq, tensor, part]).astype(jnp.int32)
    first, second = pack_call(
        w_gate, w_input, w_bkey, w_cquery, w_query, w_key, w_value, out_mixer.T, out_attend.T
    )
    rest = lax.all_gather(second, "sp", axis=0, tiled=True)
    split, step = norm_call(inputs, norm_gain, w_step.T)
    length = lax.axis_size("sp")
    halo = lax.ppermute(
        split[:, BLOCK - HALO :], "sp", [(i, i + 1) for i in range(length - 1)]
    )
    tokens = lax.all_to_all(jnp.concatenate([halo, split], axis=1), "fs", 0, 0, tiled=True)
    flat = tokens.reshape(-1, 512)
    w_kv = lax.all_gather(first, "sp", axis=0, tiled=True)
    kv_part = jnp.dot(flat, w_kv, preferred_element_type=F32).astype(BF16)
    kv_part = lax.all_to_all(kv_part.reshape(4, -1, 512), "fs", 0, 0, tiled=True)
    kv_own = jnp.sum(kv_part[:, HALO:].astype(F32), axis=0).astype(BF16)
    kv = lax.all_gather(kv_own, "sp", axis=0, tiled=True)
    w_out = rest[:, 1024:]
    outs = [w_out] + [rotated(w_out, "fs", by) for by in (1, 2, 3)]
    act = jnp.dot(flat, rest[:, :1024], preferred_element_type=F32).astype(BF16)
    act = lax.all_to_all(act.reshape(4, -1, 1024), "fs", 0, 0, tiled=True)
    yin, gate, cq, cum, send = local_call(
        ids, decay_rate, act, step, decay_offset[0].T, conv_weight
    )
    got = lax.all_to_all(send, "sp", 0, 0, tiled=True)
    enter = lax.all_to_all(scan_call(got), "sp", 0, 0, tiled=True).reshape(256, 128)
    mix = carry_call(ids, enter, yin, gate, cq, cum, ssd_gain)
    partial = attend_call(ids, stick_bias, act, kv, mix, outs)
    parts = lax.all_to_all(partial.reshape(8, 16, 2048), "tp", 0, 0, tiled=True)
    return jnp.sum(parts.astype(F32), axis=0).astype(BF16)[None]


def solution(mesh):
    shard = P(("sp", "fs"), "tp")
    return jax.shard_map(
        body,
        mesh=mesh,
        in_specs=(
            P("fs", "sp", None), P(), shard, shard, shard, shard, P(), P(), P(),
            P("fs", "sp", "tp"), P(), shard, shard, shard, P(),
            P("tp", ("sp", "fs")), P("tp", ("sp", "fs")),
        ),
        out_specs=P("fs", ("sp", "tp"), None),
        check_vma=False,
    )
```

time: 386 us -> 193 us (0.50); the launches traced: 379 us -> 192 us
  starting transfers between devices: 178 us -> 28 us
  waiting for transfers between devices: 108 us -> 29.8 us
  blocking collectives: 40.3 us -> 91.7 us
  matrix products: 17.4 us -> 3.48 us
  Pallas kernels: 0 us -> 8.43 us
  other arithmetic: 7.7 us -> 2.36 us
    ppermute x33 -> x4, starting transfers between devices: 150 us -> 12.8 us  [the longest x3 8.42 us: rotated(): lax.ppermute(shard, axis, [(i, (i + by) % length) for i in range(length)])]
    all_gather x2, waiting for transfers between devices: 65.2 us -> 15.2 us  [the longest x1 9.8 us: body(): kv = lax.all_gather(kv_own, 'sp', axis=0, tiled=True)]
    ppermute x33 -> x4, waiting for transfers between devices: 42.7 us -> 1.32 us  [the longest x1 1.31 us: body(): lax.ppermute(split[:, BLOCK - HALO:], 'sp', [(i, i + 1) for i in range(le...]
    all_to_all x1 -> x3, blocking collectives: 28.3 us -> 57.2 us  [the longest x1 23.5 us: body(): parts = lax.all_to_all(partial.reshape(8, 16, 2048), 'tp', 0, 0, tiled=True)]
    all_gather x1, blocking collectives: 12 us -> 34.5 us  [body(): w_kv = lax.all_gather(first, 'sp', axis=0, tiled=True)]
    dot_general x16 -> x2, matrix products: 17.4 us -> 3.48 us  [the longest x1 3.01 us: body(): act = jnp.dot(flat, rest[:, :1024], preferred_element_type=F32).astype(BF16)]
    all_to_all x2 -> x3, waiting for transfers between devices: 0.01 us -> 13.3 us  [the longest x1 10.4 us: body(): act = lax.all_to_all(act.reshape(4, -1, 1024), 'fs', 0, 0, tiled=True)]
    all_to_all x2 -> x3, starting transfers between devices: 27.9 us -> 15.2 us  [the longest x1 6.53 us: body(): got = lax.all_to_all(send, 'sp', 0, 0, tiled=True)]
  transfers between devices with their start and end apart: 37 -> 9, of which waited for: 18 -> 5; matrix products, arithmetic and copies ran while one was open for 8% -> 3% of each run, Pallas kernels for 0% -> 3%
where the time goes in v1:
time: 193 us; the launch traced here: 192 us
  blocking collectives  91.7 us (48%)
  waiting for transfers between devices  29.8 us (15%)
  starting transfers between devices  28 us (15%)
  local copies, waits for them, and re-layouts  14.7 us (8%)
  between operations  13.5 us (7%)
  Pallas kernels  8.43 us (4%)
  matrix products  3.48 us (2%)
  other arithmetic  2.36 us (1%)
    all_gather x1, blocking collectives, body(): w_kv = lax.all_gather(first, 'sp', axis=0, tiled=True)  34.5 us
    all_to_all x1, blocking collectives, body(): parts = lax.all_to_all(partial.reshape(8, 16, 2048), 'tp', 0, 0, tiled=True)  23.5 us
    all_to_all x1, blocking collectives, body(): lax.all_to_all(scan_call(got), 'sp', 0, 0, tiled=True).reshape(256, 128)  20.3 us
    unnamed x44, local copies, waits for them, and re-layouts  13.6 us
    all_to_all x1, blocking collectives, body(): lax.all_to_all(kv_part.reshape(4, -1, 512), 'fs', 0, 0, tiled=True)  13.3 us
    all_to_all x1, waiting for transfers between devices, body(): act = lax.all_to_all(act.reshape(4, -1, 1024), 'fs', 0, 0, tiled=True)  10.4 us
    all_gather x1, waiting for transfers between devices, body(): kv = lax.all_gather(kv_own, 'sp', axis=0, tiled=True)  9.8 us
    ppermute x3, starting transfers between devices, rotated(): lax.ppermute(shard, axis, [(i, (i + by) % length) for i in range(length)])  8.42 us
  transfers between devices with their start and end apart: 9, of which 5 were waited for; matrix products, arithmetic and copies ran while one was open for 3% of the time, Pallas kernels for 3%

profile of v1, /device:TPU:1, one launch (start us, length us, event | category | flops | bytes accessed | tf_op | source)
XLA Modules:
  0.0 191.9 jit_solution(10924667684639230538)
XLA Ops:
  6.5 0.7 copy-done.8
  7.3 0.7 copy-done.9
  8.7 0.7 copy-done.11
  13.6 1.0 copy-done.2
  14.7 0.9 copy-done.5
  17.0 4.4 %collective-permute-start = (bf16[4,16,512]{2,1,0:T(8,128)(2,1)S(1)}, bf16[4,16,512]{2,1,0:T(8,128)(2,1)S(1)}, u32[]{:S(2)}, u32[]{:S(2)}) collective-permute-start(bf16[4,16,512]{2,1,0:T(8,128)(2,1)S(1)} %slice.12), channel_id=1, source_target_pairs={{0,32},{32,64},{64,96},{96,128},{128,160},{160,192},{192,224},{224... | collective-permute-start | bytes 196616 | tf_op jit(solution)/shard_map/ppermute | solution.py:340
  21.4 1.3 collective-permute-done
  22.7 0.9 pad_maximum_fusion
  23.5 4.2 %all-to-all-start = ((bf16[4,144,512]{2,1,0:T(8,128)(2,1)}), bf16[4,144,512]{2,1,0:T(8,128)(2,1)S(1)}, u32[]{:S(2)}, u32[]{:S(2)}) async-start(bf16[4,144,512]{2,1,0:T(8,128)(2,1)} %pad_maximum_fusion), calls=%async_computation | async-start | bytes 1179648 | tf_op jit(solution)/shard_map/all_to_all | solution.py:343
  27.7 34.5 %all_gather.10 = bf16[512,512]{1,0:T(8,128)(2,1)S(1)} all-gather(bf16[32,512]{1,0:T(8,128)(2,1)S(1)} %get-tuple-element.16), channel_id=1, replica_groups=mesh['sp'=16,'fs'=4,'tp'=8] {'sp'}, dimensions={0}, use_global_device_ids=true | all-gather | bytes 557056 | tf_op jit(solution)/shard_map/all_gather | solution.py:345
  62.7 13.3 %all_to_all.30 = bf16[4,144,512]{2,1,0:T(8,128)(2,1)S(1)} all-to-all(bf16[4,144,512]{2,1,0:T(8,128)(2,1)S(1)} %bitcast.30), channel_id=1, replica_groups=mesh['sp'=16,'fs'=4,'tp'=8] {'fs'}, dimensions={0} | all-to-all | bytes 1179648 | tf_op jit(solution)/shard_map/all_to_all | solution.py:347
  76.0 0.7 slice_reduce_fusion
  76.8 5.4 %all-gather.3.cloned.1.call-done = bf16[512,1536]{1,0:T(8,128)(2,1)} async-done(((bf16[32,1536]{1,0:T(8,128)(2,1)}), bf16[512,1536]{1,0:T(8,128)(2,1)}) %all-gather.3.cloned.1.call-update) | async-done | bytes 1572880 | tf_op jit(solution)/shard_map/all_gather | solution.py:337
  82.1 3.0 %convolution_convert_fusion = bf16[576,1024]{1,0:T(8,128)(2,1)} fusion(bf16[576,512]{1,0:T(8,128)(2,1)S(1)} %bitcast.29, bf16[512,1536]{1,0:T(8,128)(2,1)} %all-gather.3.cloned.1.call-done), kind=kOutput, calls=%fused_computation | convolution fusion | flops 604569600 | bytes 2818048 | tf_op jit(solution)/shard_map/dot_general | solution.py:352
  85.1 4.5 %all-to-all-start.1 = ((bf16[4,144,1024]{2,1,0:T(8,128)(2,1)}), bf16[4,144,1024]{2,1,0:T(8,128)(2,1)S(1)}, u32[]{:S(2)}, u32[]{:S(2)}) async-start(bf16[4,144,1024]{2,1,0:T(8,128)(2,1)} %bitcast.8), calls=%async_computation.1 | async-start | bytes 2359296 | tf_op jit(solution)/shard_map/all_to_all | solution.py:353
  89.7 10.4 %all-to-all-done.1.act_ref.qp_ref = bf16[4,144,1024]{2,1,0:T(8,128)(2,1)S(1)} async-done(((bf16[4,144,1024]{2,1,0:T(8,128)(2,1)}), bf16[4,144,1024]{2,1,0:T(8,128)(2,1)S(1)}, u32[]{:S(2)}, u32[]{:S(2)}) %all-to-all-start.1) | async-done | bytes 1179680 | tf_op jit(solution)/shard_map/all_to_all | solution.py:353
  100.1 2.2 %ssd_local.1 = (f32[128,256]{1,0:T(8,128)S(1)}, f32[128,256]{1,0:T(8,128)S(1)}, bf16[128,128]{1,0:T(8,128)(2,1)S(1)}, f32[128,8]{1,0:T(8,128)S(1)}, bf16[16,32,128]{2,1,0:T(8,128)(2,1)}) custom-call(s32[3]{0:T(128)S(1)} %pad_add_fusion.ids, f32[32]{0:T(128)S(1)} %copy-done.20, bf16[4,144,1024]{2,1,0:T(8,128)(2,1)S(1)} %all-to-all-done.1.act_ref.qp_ref, ...), custom_call_target="tpu_custom_call" | custom-call | tf_op jit(solution)/shard_map/ssd_local/pallas_call | solution.py:155
  103.6 6.5 %all-to-all-start.3 = ((bf16[16,32,128]{2,1,0:T(8,128)(2,1)}), bf16[16,32,128]{2,1,0:T(8,128)(2,1)}, u32[]{:S(2)}, u32[]{:S(2)}) async-start(bf16[16,32,128]{2,1,0:T(8,128)(2,1)} %get-tuple-element.18), calls=%async_computation.3 | async-start | bytes 262144 | tf_op jit(solution)/shard_map/all_to_all | solution.py:357
  110.1 1.1 slice.18.w0
  111.2 2.2 %collective-permute-start.1 = (bf16[512,512]{1,0:T(8,128)(2,1)S(1)}, bf16[512,512]{1,0:T(8,128)(2,1)S(1)}, u32[]{:S(2)}, u32[]{:S(2)}) collective-permute-start(bf16[512,512]{1,0:T(8,128)(2,1)S(1)} %slice.18.w0), channel_id=1, source_target_pairs={{0,8},{8,16},{16,24},{24,0},{1,9},{9,17},{17,25},{25,1},{2,10},{10... | collective-permute-start | bytes 1572872 | tf_op jit(solution)/shard_map/ppermute | solution.py:323
  113.4 3.7 %collective-permute-start.2 = (bf16[512,512]{1,0:T(8,128)(2,1)S(1)}, bf16[512,512]{1,0:T(8,128)(2,1)S(1)}, u32[]{:S(2)}, u32[]{:S(2)}) collective-permute-start(bf16[512,512]{1,0:T(8,128)(2,1)S(1)} %slice.18.w0), channel_id=1, source_target_pairs={{0,16},{8,24},{16,0},{24,8},{1,17},{9,25},{17,1},{25,9},{2,18},{10... | collective-permute-start | bytes 1572872 | tf_op jit(solution)/shard_map/ppermute | solution.py:323
  117.1 2.5 %collective-permute-start.3 = (bf16[512,512]{1,0:T(8,128)(2,1)S(1)}, bf16[512,512]{1,0:T(8,128)(2,1)S(1)}, u32[]{:S(2)}, u32[]{:S(2)}) collective-permute-start(bf16[512,512]{1,0:T(8,128)(2,1)S(1)} %slice.18.w0), channel_id=1, source_target_pairs={{0,24},{8,0},{16,8},{24,16},{1,25},{9,1},{17,9},{25,17},{2,26},{10... | collective-permute-start | bytes 1572872 | tf_op jit(solution)/shard_map/ppermute | solution.py:323
  119.6 2.9 %all-to-all-done.3.got_ref = bf16[16,32,128]{2,1,0:T(8,128)(2,1)} async-done(((bf16[16,32,128]{2,1,0:T(8,128)(2,1)}), bf16[16,32,128]{2,1,0:T(8,128)(2,1)}, u32[]{:S(2)}, u32[]{:S(2)}) %all-to-all-start.3) | async-done | bytes 131104 | tf_op jit(solution)/shard_map/all_to_all | solution.py:357
  122.5 1.6 state_scan.1
  124.1 20.3 %all_to_all.31 = bf16[16,16,128]{2,1,0:T(8,128)(2,1)S(1)} all-to-all(bf16[16,16,128]{2,1,0:T(8,128)(2,1)} %state_scan.1), channel_id=1, replica_groups=mesh['sp'=16,'fs'=4,'tp'=8] {'sp'}, dimensions={0} | all-to-all | bytes 131072 | tf_op jit(solution)/shard_map/all_to_all | solution.py:358
  144.5 0.9 copy-done.4
  145.4 0.8 copy-done.7
  146.1 0.9 ssd_carry.1.mix_ref
  147.1 9.8 %all-gather.5.cloned.1.call-done.kv_ref = bf16[2048,512]{1,0:T(8,128)(2,1)} async-done(((bf16[128,512]{1,0:T(8,128)(2,1)}), bf16[2048,512]{1,0:T(8,128)(2,1)}) %all-gather.5.cloned.1.call-update) | async-done | bytes 2097168 | tf_op jit(solution)/shard_map/all_gather | solution.py:349
  156.9 1.6 copy-done
  158.4 2.4 %attend.1 = bf16[128,2048]{1,0:T(8,128)(2,1)S(1)} custom-call(s32[3]{0:T(128)S(1)} %pad_add_fusion.ids, f32[16]{0:T(128)S(1)} %copy-done.21, bf16[4,144,1024]{2,1,0:T(8,128)(2,1)S(1)} %all-to-all-done.1.act_ref.qp_ref, bf16[2048,512]{1,0:T(8,128)(2,1)S(1)} %copy-done, bf16[128,256]{1,0:T(8,128)(2,1)S(1)} %ssd_carry.1.mix_ref, ...), custom_call_target="tpu_custom_call" | custom-call | tf_op jit(solution)/shard_map/attend/pallas_call | solution.py:298
  160.9 23.5 %all_to_all.32 = bf16[8,16,2048]{2,1,0:T(8,128)(2,1)S(1)} all-to-all(bf16[8,16,2048]{2,1,0:T(8,128)(2,1)S(1)} %bitcast.20), channel_id=1, replica_groups=mesh['sp'=16,'fs'=4,'tp'=8] {'tp'}, dimensions={0} | all-to-all | bytes 1048576 | tf_op jit(solution)/shard_map/all_to_all | solution.py:361
  (50 shorter events, 8.9 us)
Async XLA Ops:
  6.5 75.6 %all-gather.3.cloned.1.call-start = ((), (), s32[]{:S(2)}) async-start(), calls=%async_computation.6 | async-start | bytes 1671168 | tf_op jit(solution)/shard_map/all_gather | solution.py:337
  6.5 0.7 copy-start.8
  7.3 0.7 copy-start.9
  8.0 0.7 copy-start.10
  8.7 0.7 copy-start.11
  9.4 0.7 copy-start.12
  10.1 0.7 copy-start.13
  10.8 0.7 copy-start.14
  11.6 0.7 copy-start.16
  12.3 0.7 copy-start.17
  13.6 1.0 copy-start.2
  14.7 0.9 copy-start.5
  15.6 0.7 copy-start.18
  17.0 5.7 %collective-permute-start = (bf16[4,16,512]{2,1,0:T(8,128)(2,1)S(1)}, bf16[4,16,512]{2,1,0:T(8,128)(2,1)S(1)}, u32[]{:S(2)}, u32[]{:S(2)}) collective-permute-start(bf16[4,16,512]{2,1,0:T(8,128)(2,1)S(1)} %slice.12), channel_id=1, source_target_pairs={{0,32},{32,64},{64,96},{96,128},{128,160},{160,192},{192,224},{224... | collective-permute-start | bytes 196616 | tf_op jit(solution)/shard_map/ppermute | solution.py:340
  23.5 38.7 %all-to-all-start = ((bf16[4,144,512]{2,1,0:T(8,128)(2,1)}), bf16[4,144,512]{2,1,0:T(8,128)(2,1)S(1)}, u32[]{:S(2)}, u32[]{:S(2)}) async-start(bf16[4,144,512]{2,1,0:T(8,128)(2,1)} %pad_maximum_fusion), calls=%async_computation | async-start | bytes 1179648 | tf_op jit(solution)/shard_map/all_to_all | solution.py:343
  27.7 129.1 %all-gather.5.cloned.1.call-start = ((), (), s32[]{:S(2)}) async-start(), calls=%async_computation.7 | async-start | bytes 2228224 | tf_op jit(solution)/shard_map/all_gather | solution.py:349
  85.1 15.0 %copy-start.1 = (f32[4,4096]{1,0:T(4,128)S(1)}, f32[4,4096]{1,0:T(4,128)}, u32[]{:S(2)}) copy-start(f32[4,4096]{1,0:T(4,128)} %cc_ref.1) | copy-start | bytes 196612
  85.1 15.0 %copy-start.19 = (f32[1,128,4]{1,2,0:T(4,128)S(1)}, f32[1,128,4]{1,2,0:T(4,128)}, u32[]{:S(2)}) copy-start(f32[1,128,4]{1,2,0:T(4,128)} %param.26) | copy-start | bytes 6148
  85.1 15.0 %copy-start.20 = (f32[32]{0:T(128)S(1)}, f32[32]{0:T(128)}, u32[]{:S(2)}) copy-start(f32[32]{0:T(128)} %rate.1) | copy-start | bytes 388
  85.1 14.9 %all-to-all-start.1 = ((bf16[4,144,1024]{2,1,0:T(8,128)(2,1)}), bf16[4,144,1024]{2,1,0:T(8,128)(2,1)S(1)}, u32[]{:S(2)}, u32[]{:S(2)}) async-start(bf16[4,144,1024]{2,1,0:T(8,128)(2,1)} %bitcast.8), calls=%async_computation.1 | async-start | bytes 2359296 | tf_op jit(solution)/shard_map/all_to_all | solution.py:353
  100.1 44.4 %copy-start.15 = (f32[2048]{0:T(1024)S(1)}, f32[2048]{0:T(1024)}, u32[]{:S(2)}) copy-start(f32[2048]{0:T(1024)} %param.27) | copy-start | bytes 24580
  102.3 0.6 copy-start.3
  103.0 0.6 copy-start.6
  103.6 53.3 %copy-start.21 = (f32[16]{0:T(128)S(1)}, f32[16]{0:T(128)}, u32[]{:S(2)}) copy-start(f32[16]{0:T(128)} %bias.1) | copy-start | bytes 196
  103.6 19.0 %all-to-all-start.3 = ((bf16[16,32,128]{2,1,0:T(8,128)(2,1)}), bf16[16,32,128]{2,1,0:T(8,128)(2,1)}, u32[]{:S(2)}, u32[]{:S(2)}) async-start(bf16[16,32,128]{2,1,0:T(8,128)(2,1)} %get-tuple-element.18), calls=%async_computation.3 | async-start | bytes 262144 | tf_op jit(solution)/shard_map/all_to_all | solution.py:357
  111.2 35.8 %collective-permute-start.1 = (bf16[512,512]{1,0:T(8,128)(2,1)S(1)}, bf16[512,512]{1,0:T(8,128)(2,1)S(1)}, u32[]{:S(2)}, u32[]{:S(2)}) collective-permute-start(bf16[512,512]{1,0:T(8,128)(2,1)S(1)} %slice.18.w0), channel_id=1, source_target_pairs={{0,8},{8,16},{16,24},{24,0},{1,9},{9,17},{17,25},{25,1},{2,10},{10... | collective-permute-start | bytes 1572872 | tf_op jit(solution)/shard_map/ppermute | solution.py:323
  113.4 33.6 %collective-permute-start.2 = (bf16[512,512]{1,0:T(8,128)(2,1)S(1)}, bf16[512,512]{1,0:T(8,128)(2,1)S(1)}, u32[]{:S(2)}, u32[]{:S(2)}) collective-permute-start(bf16[512,512]{1,0:T(8,128)(2,1)S(1)} %slice.18.w0), channel_id=1, source_target_pairs={{0,16},{8,24},{16,0},{24,8},{1,17},{9,25},{17,1},{25,9},{2,18},{10... | collective-permute-start | bytes 1572872 | tf_op jit(solution)/shard_map/ppermute | solution.py:323
  117.1 30.0 %collective-permute-start.3 = (bf16[512,512]{1,0:T(8,128)(2,1)S(1)}, bf16[512,512]{1,0:T(8,128)(2,1)S(1)}, u32[]{:S(2)}, u32[]{:S(2)}) collective-permute-start(bf16[512,512]{1,0:T(8,128)(2,1)S(1)} %slice.18.w0), channel_id=1, source_target_pairs={{0,24},{8,0},{16,8},{24,16},{1,25},{9,1},{17,9},{25,17},{2,26},{10... | collective-permute-start | bytes 1572872 | tf_op jit(solution)/shard_map/ppermute | solution.py:323
  144.5 0.9 copy-start.4
  145.4 0.8 copy-start.7
  156.9 1.6 copy-start
Sparse Core Ops, SparseCore 0:
  13.7 68.3 all-gather.2
  84.2 72.6 all-gather.4

commit v2 on v1

v2 whole, which is shorter than its diff:
```python
import jax
import jax.numpy as jnp
from jax import lax
from jax.experimental import pallas as pl
from jax.experimental.pallas import tpu as pltpu
from jax.sharding import PartitionSpec as P

BLOCK = 128
CONV = 4
EPS = 1e-06
HALO = 16
F32 = jnp.float32
BF16 = jnp.bfloat16
HIGH = lax.Precision.HIGHEST
NT = (((1,), (1,)), ((), ()))
TN = (((0,), (0,)), ((), ()))


def vmem(limit=48):
    return pltpu.CompilerParams(vmem_limit_bytes=limit * 1024 * 1024)


def iota(shape, dim):
    return lax.broadcasted_iota(jnp.int32, shape, dim)


def softplus(x):
    return jnp.maximum(x, 0.0) + jnp.log1p(jnp.exp(-jnp.abs(x)))


def silu(x):
    return x / (1.0 + jnp.exp(-x))


def pull(pairs, sems):
    copies = [pltpu.make_async_copy(src, dst, sems.at[i]) for i, (src, dst) in enumerate(pairs)]
    for copy in copies:
        copy.start()
    return copies


def norm_kernel(x_hbm, halo_hbm, gain_hbm, ws_hbm, xs_ref, step_ref, x_ref, gain_ref, ws_ref, sems):
    copies = pull(
        (
            (x_hbm.at[0], x_ref.at[pl.ds(HALO, BLOCK)]),
            (halo_hbm, x_ref.at[pl.ds(0, HALO)]),
            (gain_hbm, gain_ref),
            (ws_hbm, ws_ref),
        ),
        sems,
    )
    for copy in copies:
        copy.wait()
    x = x_ref[...].astype(F32)
    scale = lax.rsqrt(jnp.mean(x * x, axis=-1, keepdims=True) + EPS)
    normed = (x * scale * gain_ref[...]).astype(BF16)
    step_ref[...] = softplus(
        lax.dot_general(ws_ref[...], normed[HALO:], NT, preferred_element_type=F32)
    )
    wide = normed.astype(F32)
    lane = iota((x.shape[0], 128), 1) // 32
    for f in range(4):
        for g in range(4):
            out = None
            for k in range(4):
                at = (4 * g + k) * 128
                piece = wide[:, at : at + 128]
                shift = ((k - f) * 32) % 128
                if shift:
                    piece = pltpu.roll(piece, shift, 1)
                out = piece if out is None else jnp.where(lane == k, piece, out)
            xs_ref[f, :, g * 128 : (g + 1) * 128] = out.astype(BF16)


def norm_call(inputs, halo, gain, w_step_t):
    rows, width = inputs.shape[1:]
    heads = w_step_t.shape[0]
    hbm = pl.BlockSpec(memory_space=pltpu.HBM)
    return pl.pallas_call(
        norm_kernel,
        in_specs=[hbm] * 4,
        out_shape=(
            jax.ShapeDtypeStruct((4, rows + HALO, width // 4), BF16),
            jax.ShapeDtypeStruct((heads, rows), F32),
        ),
        scratch_shapes=[
            pltpu.VMEM((rows + HALO, width), BF16),
            pltpu.VMEM((1, width), F32),
            pltpu.VMEM((heads, width), BF16),
            pltpu.SemaphoreType.DMA((4,)),
        ],
        compiler_params=vmem(),
        name="norm",
    )(inputs, halo, gain.reshape(1, -1), w_step_t)


def pack_kernel(*refs):
    sources, outs, sems = refs[:9], refs[9:12], refs[12]
    pairs = []
    at, which = 0, 0
    for n, src in enumerate(sources):
        if n in (4, 7):
            at, which = 0, which + 1
        width = src.shape[1]
        pairs.append((src, outs[which].at[:, pl.ds(at, width)]))
        at += width
    for copy in pull(pairs, sems):
        copy.wait()


def pack_call(*arrays):
    rows = arrays[0].shape[0]
    widths = [sum(a.shape[1] for a in group) for group in (arrays[:4], arrays[4:7], arrays[7:])]
    hbm = pl.BlockSpec(memory_space=pltpu.HBM)
    return pl.pallas_call(
        pack_kernel,
        in_specs=[hbm] * len(arrays),
        out_specs=[hbm] * 3,
        out_shape=[jax.ShapeDtypeStruct((rows, w), BF16) for w in widths],
        scratch_shapes=[pltpu.SemaphoreType.DMA((len(arrays),))],
        name="pack",
    )(*arrays)


def added(ref, at, width):
    total = ref[0, :, at : at + width].astype(F32)
    for j in range(1, 4):
        total = total + ref[j, :, at : at + width].astype(F32)
    return total.astype(BF16)


def convolved(wide_ref, taps):
    summed = None
    for i in range(CONV):
        at = HALO - CONV + 1 + i
        part = taps[i : i + 1] * wide_ref[at : at + BLOCK, :]
        summed = part if summed is None else summed + part
    return silu(summed).astype(BF16)


def local_kernel(
    ids, rate, act_ref, step_ref, off_ref, ci_ref, cb_ref,
    send_ref, xin_ref, bkey_ref, rows_ref, cols_ref, wide_ref,
):
    tensor = ids[1]
    send_ref[0:BLOCK, :] = added(act_ref, 0, 512)[HALO:]
    wide_ref[...] = added(act_ref, 512, 384).astype(F32)
    conv = convolved(wide_ref, jnp.concatenate([ci_ref[...], cb_ref[...]], axis=1))
    xin, bkey = conv[:, 0:256], conv[:, 256:384]
    xin_ref[...] = xin
    bkey_ref[...] = bkey
    row = iota((BLOCK, BLOCK), 0)
    col = iota((BLOCK, BLOCK), 1)
    step = jnp.concatenate([step_ref[pl.ds(4 * tensor + h, 1), :] for h in range(4)], axis=0)
    rates = jnp.concatenate(
        [jnp.full((1, BLOCK), rate[4 * tensor + h], F32) for h in range(4)], axis=0
    )
    decay = off_ref[...] - rates * step
    decay8 = jnp.concatenate([decay, jnp.zeros((4, BLOCK), F32)], axis=0)
    upper = (row <= col).astype(F32)
    cum = jnp.dot(decay8, upper, precision=HIGH, preferred_element_type=F32)
    last = jnp.sum(decay, axis=1, keepdims=True)
    to_end = jnp.exp(last - cum[0:4]) * step
    eye = (row == col).astype(F32)
    cols = lax.dot_general(
        eye, jnp.concatenate([cum[0:4], to_end], axis=0), NT, precision=HIGH,
        preferred_element_type=F32,
    )
    rows_ref[...] = jnp.concatenate([cum[0:4], step], axis=0)
    cols_ref[...] = cols
    wide_key = bkey.astype(F32)
    for h in range(4):
        wk = (wide_key * cols[:, 4 + h : 5 + h]).astype(BF16)
        state = lax.dot_general(
            xin[:, h * 64 : (h + 1) * 64], wk, TN, preferred_element_type=F32
        )
        log = jnp.broadcast_to(last[h : h + 1], (8, BLOCK))
        high = log.astype(BF16).astype(F32)
        logs = jnp.concatenate([high, log - high], axis=0).astype(BF16)
        send_ref[BLOCK : BLOCK + 64, h * 128 : (h + 1) * 128] = state.astype(BF16)
        send_ref[BLOCK + 64 : BLOCK + 80, h * 128 : (h + 1) * 128] = logs


def local_call(ids, rate, act, step, offset, conv_weight):
    full = lambda *shape: pl.BlockSpec(shape, lambda i, ids, rate: (0,) * len(shape))
    return pl.pallas_call(
        local_kernel,
        grid_spec=pltpu.PrefetchScalarGridSpec(
            num_scalar_prefetch=2,
            grid=(1,),
            in_specs=[
                full(*act.shape),
                full(*step.shape),
                full(*offset.shape),
                pl.BlockSpec((CONV, 256), lambda i, ids, rate: (0, ids[1])),
                pl.BlockSpec((CONV, 128), lambda i, ids, rate: (0, 16 + ids[1])),
            ],
            out_specs=[
                full(SENT, 512), full(BLOCK, 256), full(BLOCK, 128), full(8, BLOCK),
                full(BLOCK, 8),
            ],
            scratch_shapes=[pltpu.VMEM((BLOCK + HALO, 384), F32)],
        ),
        out_shape=(
            jax.ShapeDtypeStruct((SENT, 512), BF16),
            jax.ShapeDtypeStruct((BLOCK, 256), BF16),
            jax.ShapeDtypeStruct((BLOCK, 128), BF16),
            jax.ShapeDtypeStruct((8, BLOCK), F32),
            jax.ShapeDtypeStruct((BLOCK, 8), F32),
        ),
        compiler_params=vmem(),
        name="ssd_local",
    )(ids, rate, act, step, offset, conv_weight, conv_weight)


def inner_kernel(
    ids, act_ref, cc_ref, xin_ref, bkey_ref, rows_ref, cols_ref,
    yin_ref, gate_ref, cq_ref, q_ref, wide_ref,
):
    gate_ref[...] = silu(added(act_ref, 0, 256)[HALO:].astype(F32))
    q_ref[...] = added(act_ref, 384, 256)[HALO:]
    wide_ref[...] = added(act_ref, 256, 128).astype(F32)
    cquery = convolved(wide_ref, cc_ref[...])
    cq_ref[...] = cquery
    lower = iota((BLOCK, BLOCK), 0) >= iota((BLOCK, BLOCK), 1)
    inner = lax.dot_general(cquery, bkey_ref[...], NT, preferred_element_type=F32)
    for h in range(4):
        spread = cols_ref[:, h : h + 1] - rows_ref[h : h + 1, :]
        decayed = jnp.exp(jnp.where(lower, spread, 0.0))
        mix = jnp.where(lower, inner * decayed * rows_ref[4 + h : 5 + h, :], 0.0).astype(BF16)
        yin_ref[:, h * 64 : (h + 1) * 64] = jnp.dot(
            mix, xin_ref[:, h * 64 : (h + 1) * 64], preferred_element_type=F32
        )


def inner_call(ids, act, conv_weight, xin, bkey, rows, cols):
    full = lambda *shape: pl.BlockSpec(shape, lambda i, ids: (0,) * len(shape))
    return pl.pallas_call(
        inner_kernel,
        grid_spec=pltpu.PrefetchScalarGridSpec(
            num_scalar_prefetch=1,
            grid=(1,),
            in_specs=[
                full(*act.shape),
                pl.BlockSpec((CONV, 128), lambda i, ids: (0, 24 + ids[1])),
                full(BLOCK, 256), full(BLOCK, 128), full(8, BLOCK), full(BLOCK, 8),
            ],
            out_specs=[full(BLOCK, 256), full(BLOCK, 256), full(BLOCK, 128), full(BLOCK, 256)],
            scratch_shapes=[pltpu.VMEM((BLOCK + HALO, 128), F32)],
        ),
        out_shape=(
            jax.ShapeDtypeStruct((BLOCK, 256), F32),
            jax.ShapeDtypeStruct((BLOCK, 256), F32),
            jax.ShapeDtypeStruct((BLOCK, 128), BF16),
            jax.ShapeDtypeStruct((BLOCK, 256), BF16),
        ),
        compiler_params=vmem(),
        name="ssd_inner",
    )(ids, act, conv_weight, xin, bkey, rows, cols)


SUB = 256
KEYS = 512
SENT = BLOCK + 80


def attend_kernel(
    ids, bias, q_ref, yin_ref, gate_ref, cq_ref, cols_ref, gain_ref, all_hbm, w0, w1, w2, w3,
    out_ref, kv_ref, st_ref, w_ref, acc_ref, late_ref, hold_ref, sems, wsems,
):
    block, tensor, mine = ids[0], ids[1], ids[2]
    per = KEYS // BLOCK

    def move(k):
        return pltpu.make_async_copy(
            all_hbm.at[k, pl.ds(0, BLOCK)], kv_ref.at[pl.ds(k * BLOCK, BLOCK)], sems.at[0, k]
        )

    def state_move(k):
        return pltpu.make_async_copy(
            all_hbm.at[k, pl.ds(BLOCK, SENT - BLOCK)], st_ref.at[k], sems.at[1, k]
        )

    count = all_hbm.shape[0]
    for chunk in range(count // per - 1, -1, -1):

        @pl.when(chunk * per <= block)
        def _(chunk=chunk):
            for k in range(chunk * per, (chunk + 1) * per):
                move(k).start()

    for k in range(count - 1):
        state_move(k).start()
    weights = [
        pltpu.make_async_copy(w, w_ref.at[(mine + 4 - r) % 4], wsems.at[r])
        for r, w in enumerate((w0, w1, w2, w3))
    ]
    for copy in weights:
        copy.start()
    acc_ref[...] = jnp.zeros_like(acc_ref)
    late_ref[...] = jnp.zeros_like(late_ref)
    hold_ref[...] = jnp.zeros_like(hold_ref)
    after = (iota((SUB, SUB), 0) > iota((SUB, SUB), 1)).astype(BF16)
    ones = jnp.ones((SUB, 128), BF16)
    for chunk in range(count // per - 1, -1, -1):

        @pl.when(chunk * per <= block)
        def _(chunk=chunk):
            for k in range(chunk * per, (chunk + 1) * per):
                move(k).wait()
            for h in range(2):
                late = late_ref[h]
                gained = acc_ref[h]
                query = q_ref[:, h * 128 : (h + 1) * 128]
                for sub in range(KEYS // SUB - 1, -1, -1):
                    at = chunk * KEYS + sub * SUB
                    before = at + iota((BLOCK, SUB), 1) < block * BLOCK + iota((BLOCK, SUB), 0)
                    key = kv_ref[at : at + SUB, h * 128 : (h + 1) * 128]
                    value = kv_ref[at : at + SUB, 256 + h * 128 : 256 + (h + 1) * 128]
                    logits = lax.dot_general(query, key, NT, preferred_element_type=F32)
                    logits = logits * (128 ** -0.5) + bias[2 * tensor + h]
                    soft = jnp.maximum(logits, 0.0) + jnp.log(1.0 + jnp.exp(-jnp.abs(logits)))
                    passed = jnp.where(before, -soft, 0.0)
                    high = passed.astype(BF16)
                    low = (passed - high.astype(F32)).astype(BF16)
                    tail = jnp.dot(high, after, preferred_element_type=F32) + jnp.dot(
                        low, after, preferred_element_type=F32
                    )
                    whole = jnp.dot(high, ones, preferred_element_type=F32) + jnp.dot(
                        low, ones, preferred_element_type=F32
                    )
                    later = jnp.concatenate([late] * (SUB // 128), axis=1)
                    weight = jnp.where(before, jnp.exp(logits - soft + (tail + later)), 0.0)
                    gained = gained + jnp.dot(
                        weight.astype(BF16), value, preferred_element_type=F32
                    )
                    late = late + whole
                late_ref[h] = late
                acc_ref[h] = gained

    for k in range(count - 1):
        state_move(k).wait()

        @pl.when(k < block)
        def _(k=k):
            logs = st_ref[k, 64:80, :].astype(F32)
            decay = jnp.exp(logs[0:8] + logs[8:16])
            hold_ref[...] = hold_ref[...] * jnp.concatenate([decay] * 8, axis=0) + st_ref[
                k, 0:64, :
            ].astype(F32)

    cquery = cq_ref[...]
    ys = []
    for h in range(4):
        enter = hold_ref[:, h * 128 : (h + 1) * 128].astype(BF16)
        moved = lax.dot_general(cquery, enter, NT, preferred_element_type=F32)
        ys.append(moved * jnp.exp(cols_ref[:, h : h + 1]))
    gated = (yin_ref[...] + jnp.concatenate(ys, axis=1)) * gate_ref[...]
    scale = lax.rsqrt(jnp.mean(gated * gated, axis=-1, keepdims=True) + EPS)
    mixed = (gated * scale * gain_ref[...]).astype(BF16)
    both = jnp.concatenate([mixed, acc_ref[0].astype(BF16), acc_ref[1].astype(BF16)], axis=1)
    for copy in weights:
        copy.wait()
    for s in range(16):
        piece = jnp.concatenate([w_ref[f, 32 * s : 32 * (s + 1), :] for f in range(4)], axis=0)
        out_ref[:, 128 * s : 128 * (s + 1)] = lax.dot_general(
            both, piece, NT, preferred_element_type=F32
        ).astype(BF16)


def attend_call(ids, bias, q, yin, gate, cq, cols, gain, gathered, w):
    full = lambda *shape: pl.BlockSpec(shape, lambda i, ids, bias: (0,) * len(shape))
    hbm = pl.BlockSpec(memory_space=pltpu.HBM)
    count = gathered.shape[0]
    return pl.pallas_call(
        attend_kernel,
        grid_spec=pltpu.PrefetchScalarGridSpec(
            num_scalar_prefetch=2,
            grid=(1,),
            in_specs=[
                full(BLOCK, 256), full(BLOCK, 256), full(BLOCK, 256), full(BLOCK, 128),
                full(BLOCK, 8), pl.BlockSpec((1, 256), lambda i, ids, bias: (0, ids[1])),
                hbm, hbm, hbm, hbm, hbm,
            ],
            out_specs=full(BLOCK, 2048),
            scratch_shapes=[
                pltpu.VMEM((count * BLOCK, 512), BF16),
                pltpu.VMEM((count, SENT - BLOCK, 512), BF16),
                pltpu.VMEM((4, 512, 512), BF16),
                pltpu.VMEM((2, BLOCK, 128), F32),
                pltpu.VMEM((2, BLOCK, 128), F32),
                pltpu.VMEM((64, 512), F32),
                pltpu.SemaphoreType.DMA((2, count)),
                pltpu.SemaphoreType.DMA((4,)),
            ],
        ),
        out_shape=jax.ShapeDtypeStruct((BLOCK, 2048), BF16),
        compiler_params=vmem(),
        name="attend",
    )(ids, bias, q, yin, gate, cq, cols, gain.reshape(1, -1), gathered, *w)


def rotated(shard, axis, by):
    length = lax.axis_size(axis)
    return lax.ppermute(shard, axis, [(i, (i + by) % length) for i in range(length)])


def body(
    inputs, norm_gain, w_gate, w_input, w_bkey, w_cquery, w_step, conv_weight, decay_rate,
    decay_offset, ssd_gain, w_query, w_key, w_value, stick_bias, out_mixer, out_attend,
):
    tensor = lax.axis_index("tp")
    seq = lax.axis_index("sp")
    part = lax.axis_index("fs")
    length = lax.axis_size("sp")
    ids = jnp.stack([seq, tensor, part]).astype(jnp.int32)
    halo = lax.ppermute(
        inputs[0, BLOCK - HALO :], "sp", [(i, i + 1) for i in range(length - 1)]
    )
    first, second, third = pack_call(
        w_key, w_value, w_input, w_bkey, w_gate, w_cquery, w_query, out_mixer.T, out_attend.T
    )
    split, step = norm_call(inputs, halo, norm_gain, w_step.T)
    tokens = lax.all_to_all(split, "fs", 0, 0, tiled=True).reshape(-1, 512)
    rows = BLOCK + HALO

    def projected(weights):
        whole = lax.all_gather(weights, "sp", axis=0, tiled=True)
        act = jnp.dot(tokens, whole, preferred_element_type=F32).astype(BF16)
        return lax.all_to_all(act.reshape(4, rows, -1), "fs", 0, 0, tiled=True)

    send, xin, bkey, srows, scols = local_call(
        ids, decay_rate, projected(first), step, decay_offset[0].T, conv_weight
    )
    gathered = lax.all_gather(send, "sp", axis=0)
    out_w = lax.all_to_all(
        jnp.broadcast_to(third[None], (length, *third.shape)), "sp", 0, 0, tiled=True
    ).reshape(-1, 512)
    outs = [out_w] + [rotated(out_w, "fs", by) for by in (1, 2, 3)]
    yin, gate, cq, q = inner_call(ids, projected(second), conv_weight, xin, bkey, srows, scols)
    partial = attend_call(ids, stick_bias, q, yin, gate, cq, scols, ssd_gain, gathered, outs)
    parts = lax.all_to_all(partial.reshape(8, 16, 2048), "tp", 0, 0, tiled=True)
    return jnp.sum(parts.astype(F32), axis=0).astype(BF16)[None]


def solution(mesh):
    shard = P(("sp", "fs"), "tp")
    return jax.shard_map(
        body,
        mesh=mesh,
        in_specs=(
            P("fs", "sp", None), P(), shard, shard, shard, shard, P(), P(), P(),
            P("fs", "sp", "tp"), P(), shard, shard, shard, P(),
            P("tp", ("sp", "fs")), P("tp", ("sp", "fs")),
        ),
        out_specs=P("fs", ("sp", "tp"), None),
        check_vma=False,
    )
```

time: 193 us -> 209 us (1.083)
  blocking collectives: 91.7 us -> 113 us
  local copies, waits for them, and re-layouts: 14.7 us -> 4.37 us
  Pallas kernels: 8.43 us -> 14.7 us
  starting transfers between devices: 28 us -> 33.3 us
  waiting for transfers between devices: 29.8 us -> 25.5 us
    all_gather x1 -> x2, blocking collectives: 34.5 us -> 86.6 us  [projected(): whole = lax.all_gather(weights, 'sp', axis=0, tiled=True)]
    all_to_all x2 -> x0, blocking collectives: 33.7 us -> none  [the longest x1 20.3 us: body(): lax.all_to_all(scan_call(got), 'sp', 0, 0, tiled=True).reshape(256, 128)]
    all_gather x2 -> x1, waiting for transfers between devices: 15.2 us -> 0.01 us  [body(): gathered = lax.all_gather(send, 'sp', axis=0)]
    ppermute x3, waiting for transfers between devices: 0.01 us -> 14.5 us  [rotated(): lax.ppermute(shard, axis, [(i, (i + by) % length) for i in range(length)])]
    unnamed x44 -> x20, local copies, waits for them, and re-layouts: 13.6 us -> 2.67 us
    pallas_call x4 -> x3, Pallas kernels: 3.79 us -> 8.19 us  [the longest x1 5.15 us: pack_call(): pl.pallas_call(pack_kernel, in_specs=[hbm] * len(arrays), out_specs=[hbm]...]
    all_to_all x3 -> x4, starting transfers between devices: 15.2 us -> 19.4 us  [the longest x2 8.08 us: projected(): return lax.all_to_all(act.reshape(4, rows, -1), 'fs', 0, 0, tiled=True)]
    all_to_all x3 -> x4, waiting for transfers between devices: 13.3 us -> 9.58 us  [the longest x2 9.58 us: projected(): return lax.all_to_all(act.reshape(4, rows, -1), 'fs', 0, 0, tiled=True)]
  transfers between devices with their start and end apart: 9 -> 9, of which waited for: 5 -> 5; matrix products, arithmetic and copies ran while one was open for 3% -> 1% of each run, Pallas kernels for 3% -> 3%
where the time goes in v2:
time: 209 us; the launch traced here: 208 us
  blocking collectives  113 us (54%)
  starting transfers between devices  33.3 us (16%)
  waiting for transfers between devices  25.5 us (12%)
  Pallas kernels  14.7 us (7%)
  between operations  13.5 us (6%)
  local copies, waits for them, and re-layouts  4.37 us (2%)
  matrix products  3.28 us (2%)
    all_gather x2, blocking collectives, projected(): whole = lax.all_gather(weights, 'sp', axis=0, tiled=True)  86.6 us
    all_to_all x1, blocking collectives, body(): parts = lax.all_to_all(partial.reshape(8, 16, 2048), 'tp', 0, 0, tiled=True)  26.1 us
    ppermute x3, waiting for transfers between devices, rotated(): lax.ppermute(shard, axis, [(i, (i + by) % length) for i in range(length)])  14.5 us
    all_to_all x2, waiting for transfers between devices, projected(): return lax.all_to_all(act.reshape(4, rows, -1), 'fs', 0, 0, tiled=True)  9.58 us
    ppermute x3, starting transfers between devices, rotated(): lax.ppermute(shard, axis, [(i, (i + by) % length) for i in range(length)])  9.51 us
    all_to_all x2, starting transfers between devices, projected(): return lax.all_to_all(act.reshape(4, rows, -1), 'fs', 0, 0, tiled=True)  8.08 us
    all_to_all x1, starting transfers between devices, body(): lax.all_to_all(jnp.broadcast_to(third[None], (length, *third.shape)), 'sp...  7.13 us
    pallas_call x1, Pallas kernels, pack_call(): pl.pallas_call(pack_kernel, in_specs=[hbm] * len(arrays), out_specs=[hbm]...  5.15 us
  transfers between devices with their start and end apart: 9, of which 5 were waited for; matrix products, arithmetic and copies ran while one was open for 1% of the time, Pallas kernels for 3%

profile of v2, /device:TPU:1, one launch (start us, length us, event | category | flops | bytes accessed | tf_op | source)
XLA Modules:
  0.0 208.0 jit_solution(17618523601575213896)
XLA Ops:
  6.5 0.8 slice_bitcast_fusion
  7.4 4.4 %collective-permute-start = (bf16[16,2048]{1,0:T(8,128)(2,1)S(1)}, bf16[16,2048]{1,0:T(8,128)(2,1)S(1)}, u32[]{:S(2)}, u32[]{:S(2)}) collective-permute-start(bf16[16,2048]{1,0:T(8,128)(2,1)S(1)} %slice_bitcast_fusion), channel_id=1, source_target_pairs={{0,32},{32,64},{64,96},{96,128},{128,160},{160,192},{192,224},{224... | collective-permute-start | bytes 196616 | tf_op jit(solution)/shard_map/ppermute | solution.py:417
  11.7 1.3 collective-permute-done.halo_hbm
  13.1 1.0 copy-done
  14.1 0.9 copy-done.2
  15.0 0.7 copy-done.3
  15.7 2.0 norm.1
  17.7 4.2 %all-to-all-start = ((bf16[4,144,512]{2,1,0:T(8,128)(2,1)}), bf16[4,144,512]{2,1,0:T(8,128)(2,1)S(1)}, u32[]{:S(2)}, u32[]{:S(2)}) async-start(bf16[4,144,512]{2,1,0:T(8,128)(2,1)} %get-tuple-element.19), calls=%async_computation | async-start | bytes 1179648 | tf_op jit(solution)/shard_map/all_to_all | solution.py:424
  21.9 5.2 %pack.1 = (bf16[32,896]{1,0:T(8,128)(2,1)}, bf16[32,640]{1,0:T(8,128)(2,1)}, bf16[32,512]{1,0:T(8,128)(2,1)}) custom-call(bf16[32,256]{1,0:T(8,128)(2,1)} %refs_0_.1, bf16[32,256]{1,0:T(8,128)(2,1)} %refs_1_.1, bf16[32,256]{1,0:T(8,128)(2,1)} %refs_2_.1, bf16[32,128]{1,0:T(8,128)(2,1)} %refs_3_.1, bf16[32,256]{1,0:T(8,128)(2,1)} %refs_4_.1, ...), custom_call_target="tpu_custom_call" | custom-call | tf_op jit(solution)/shard_map/pack/pallas_call | solution.py:115
  27.0 34.8 %all_gather.13 = bf16[512,896]{1,0:T(8,128)(2,1)S(1)} all-gather(bf16[32,896]{1,0:T(8,128)(2,1)} %get-tuple-element.21), channel_id=1, replica_groups=mesh['sp'=16,'fs'=4,'tp'=8] {'sp'}, dimensions={0}, use_global_device_ids=true | all-gather | bytes 974848 | tf_op jit(solution)/shard_map/all_gather | solution.py:428
  61.8 0.0 copy-start.6
  61.9 1.8 convolution_convert_fusion
  63.6 4.6 %all-to-all-start.2 = ((bf16[4,144,896]{2,1,0:T(8,128)(2,1)}), bf16[4,144,896]{2,1,0:T(8,128)(2,1)S(1)}, u32[]{:S(2)}, u32[]{:S(2)}) async-start(bf16[4,144,896]{2,1,0:T(8,128)(2,1)} %bitcast.10), calls=%async_computation.2 | async-start | bytes 2064384 | tf_op jit(solution)/shard_map/all_to_all | solution.py:430
  68.2 0.1 pad_add_fusion.ids
  68.3 9.6 %all-to-all-done.2.act_ref = bf16[4,144,896]{2,1,0:T(8,128)(2,1)S(1)} async-done(((bf16[4,144,896]{2,1,0:T(8,128)(2,1)}), bf16[4,144,896]{2,1,0:T(8,128)(2,1)S(1)}, u32[]{:S(2)}, u32[]{:S(2)}) %all-to-all-start.2) | async-done | bytes 1032224 | tf_op jit(solution)/shard_map/all_to_all | solution.py:430
  77.9 2.1 ssd_local.1
  80.0 0.0 all-gather.3.cloned.1.call-update
  80.0 0.9 broadcast_in_dim.4
  80.9 7.1 %all-to-all-start.3 = ((bf16[16,32,512]{2,1,0:T(8,128)(2,1)}), bf16[16,32,512]{2,1,0:T(8,128)(2,1)S(1)}, u32[]{:S(2)}, u32[]{:S(2)}) async-start(bf16[16,32,512]{2,1,0:T(8,128)(2,1)} %broadcast_in_dim.4), calls=%async_computation.3 | async-start | bytes 1048576 | tf_op jit(solution)/shard_map/all_to_all | solution.py:436
  88.0 51.8 %all_gather.12 = bf16[512,640]{1,0:T(8,128)(2,1)S(1)} all-gather(bf16[32,640]{1,0:T(8,128)(2,1)S(1)} %copy-done.8), channel_id=1, replica_groups=mesh['sp'=16,'fs'=4,'tp'=8] {'sp'}, dimensions={0}, use_global_device_ids=true | all-gather | bytes 696320 | tf_op jit(solution)/shard_map/all_gather | solution.py:428
  139.8 1.5 convolution_convert_fusion.1
  141.3 3.5 %all-to-all-start.1 = ((bf16[4,144,640]{2,1,0:T(8,128)(2,1)}), bf16[4,144,640]{2,1,0:T(8,128)(2,1)S(1)}, u32[]{:S(2)}, u32[]{:S(2)}) async-start(bf16[4,144,640]{2,1,0:T(8,128)(2,1)} %bitcast.9), calls=%async_computation.1 | async-start | bytes 1474560 | tf_op jit(solution)/shard_map/all_to_all | solution.py:430
  144.8 4.5 %collective-permute-start.3 = (bf16[512,512]{1,0:T(8,128)(2,1)S(1)}, bf16[512,512]{1,0:T(8,128)(2,1)S(1)}, u32[]{:S(2)}, u32[]{:S(2)}) collective-permute-start(bf16[512,512]{1,0:T(8,128)(2,1)S(1)} %bitcast.24), channel_id=1, source_target_pairs={{0,24},{8,0},{16,8},{24,16},{1,25},{9,1},{17,9},{25,17},{2,26},{10... | collective-permute-start | bytes 1572872 | tf_op jit(solution)/shard_map/ppermute | solution.py:405
  149.3 2.5 %collective-permute-start.2 = (bf16[512,512]{1,0:T(8,128)(2,1)S(1)}, bf16[512,512]{1,0:T(8,128)(2,1)S(1)}, u32[]{:S(2)}, u32[]{:S(2)}) collective-permute-start(bf16[512,512]{1,0:T(8,128)(2,1)S(1)} %bitcast.25), channel_id=1, source_target_pairs={{0,16},{8,24},{16,0},{24,8},{1,17},{9,25},{17,1},{25,9},{2,18},{10... | collective-permute-start | bytes 1572872 | tf_op jit(solution)/shard_map/ppermute | solution.py:405
  151.8 2.5 %collective-permute-start.1 = (bf16[512,512]{1,0:T(8,128)(2,1)S(1)}, bf16[512,512]{1,0:T(8,128)(2,1)S(1)}, u32[]{:S(2)}, u32[]{:S(2)}) collective-permute-start(bf16[512,512]{1,0:T(8,128)(2,1)S(1)} %bitcast.26), channel_id=1, source_target_pairs={{0,8},{8,16},{16,24},{24,0},{1,9},{9,17},{17,25},{25,1},{2,10},{10... | collective-permute-start | bytes 1572872 | tf_op jit(solution)/shard_map/ppermute | solution.py:405
  154.3 1.1 ssd_inner.1
  155.4 1.7 collective-permute-done.3.w3
  157.1 3.7 %collective-permute-done.2.w2 = bf16[512,512]{1,0:T(8,128)(2,1)S(1)} collective-permute-done((bf16[512,512]{1,0:T(8,128)(2,1)S(1)}, bf16[512,512]{1,0:T(8,128)(2,1)S(1)}, u32[]{:S(2)}, u32[]{:S(2)}) %collective-permute-start.2) | collective-permute-done | bytes 524320 | tf_op jit(solution)/shard_map/ppermute | solution.py:405
  160.8 9.1 %collective-permute-done.1.w1 = bf16[512,512]{1,0:T(8,128)(2,1)S(1)} collective-permute-done((bf16[512,512]{1,0:T(8,128)(2,1)S(1)}, bf16[512,512]{1,0:T(8,128)(2,1)S(1)}, u32[]{:S(2)}, u32[]{:S(2)}) %collective-permute-start.1) | collective-permute-done | bytes 524320 | tf_op jit(solution)/shard_map/ppermute | solution.py:405
  169.9 4.4 %attend.1 = bf16[128,2048]{1,0:T(8,128)(2,1)S(1)} custom-call(s32[3]{0:T(128)S(1)} %pad_add_fusion.ids, f32[16]{0:T(128)S(1)} %copy-done.7, bf16[128,256]{1,0:T(8,128)(2,1)S(1)} %get-tuple-element.27.q_ref, f32[128,256]{1,0:T(8,128)S(1)} %get-tuple-element.28.yin_ref, f32[128,256]{1,0:T(8,128)S(1)} %get-tuple-element.29.gate_ref, ...), custom_call_target="tpu_custom_call" | custom-call | tf_op jit(solution)/shard_map/attend/pallas_call | solution.py:375
  174.3 26.1 %all_to_all.25 = bf16[8,16,2048]{2,1,0:T(8,128)(2,1)S(1)} all-to-all(bf16[8,16,2048]{2,1,0:T(8,128)(2,1)S(1)} %bitcast.28), channel_id=1, replica_groups=mesh['sp'=16,'fs'=4,'tp'=8] {'tp'}, dimensions={0} | all-to-all | bytes 1048576 | tf_op jit(solution)/shard_map/all_to_all | solution.py:442
  200.4 0.7 reduce_sum.12
  (21 shorter events, 0.0 us)
Async XLA Ops:
  7.4 5.7 %collective-permute-start = (bf16[16,2048]{1,0:T(8,128)(2,1)S(1)}, bf16[16,2048]{1,0:T(8,128)(2,1)S(1)}, u32[]{:S(2)}, u32[]{:S(2)}) collective-permute-start(bf16[16,2048]{1,0:T(8,128)(2,1)S(1)} %slice_bitcast_fusion), channel_id=1, source_target_pairs={{0,32},{32,64},{64,96},{96,128},{128,160},{160,192},{192,224},{224... | collective-permute-start | bytes 196616 | tf_op jit(solution)/shard_map/ppermute | solution.py:417
  13.0 1.0 copy-start
  14.1 0.9 copy-start.2
  15.0 0.7 copy-start.3
  17.7 44.2 %all-to-all-start = ((bf16[4,144,512]{2,1,0:T(8,128)(2,1)}), bf16[4,144,512]{2,1,0:T(8,128)(2,1)S(1)}, u32[]{:S(2)}, u32[]{:S(2)}) async-start(bf16[4,144,512]{2,1,0:T(8,128)(2,1)} %get-tuple-element.19), calls=%async_computation | async-start | bytes 1179648 | tf_op jit(solution)/shard_map/all_to_all | solution.py:424
  61.8 16.1 %copy-start.1 = (f32[4,4096]{1,0:T(4,128)S(1)}, f32[4,4096]{1,0:T(4,128)}, u32[]{:S(2)}) copy-start(f32[4,4096]{1,0:T(4,128)} %cc_ref.1) | copy-start | bytes 196612
  61.8 16.1 %copy-start.5 = (f32[1,128,4]{1,2,0:T(4,128)S(1)}, f32[1,128,4]{1,2,0:T(4,128)}, u32[]{:S(2)}) copy-start(f32[1,128,4]{1,2,0:T(4,128)} %param.26) | copy-start | bytes 6148
  61.8 16.1 %copy-start.6 = (f32[32]{0:T(128)S(1)}, f32[32]{0:T(128)}, u32[]{:S(2)}) copy-start(f32[32]{0:T(128)} %rate.1) | copy-start | bytes 388
  63.6 16.4 %copy-start.9 = (bf16[32,512]{1,0:T(8,128)(2,1)S(1)}, bf16[32,512]{1,0:T(8,128)(2,1)}, u32[]{:S(2)}) copy-start(bf16[32,512]{1,0:T(8,128)(2,1)} %get-tuple-element.32) | copy-start | bytes 98308
  63.6 24.4 %copy-start.8 = (bf16[32,640]{1,0:T(8,128)(2,1)S(1)}, bf16[32,640]{1,0:T(8,128)(2,1)}, u32[]{:S(2)}) copy-start(bf16[32,640]{1,0:T(8,128)(2,1)} %get-tuple-element.20) | copy-start | bytes 122884
  63.6 14.2 %all-to-all-start.2 = ((bf16[4,144,896]{2,1,0:T(8,128)(2,1)}), bf16[4,144,896]{2,1,0:T(8,128)(2,1)S(1)}, u32[]{:S(2)}, u32[]{:S(2)}) async-start(bf16[4,144,896]{2,1,0:T(8,128)(2,1)} %bitcast.10), calls=%async_computation.2 | async-start | bytes 2064384 | tf_op jit(solution)/shard_map/all_to_all | solution.py:430
  68.2 101.7 %all-gather.3.cloned.1.call-start = ((), (), s32[]{:S(2)}) async-start(), calls=%async_computation.5 | async-start | bytes 3620864 | tf_op jit(solution)/shard_map/all_gather | solution.py:435
  80.9 60.4 %all-to-all-start.3 = ((bf16[16,32,512]{2,1,0:T(8,128)(2,1)}), bf16[16,32,512]{2,1,0:T(8,128)(2,1)S(1)}, u32[]{:S(2)}, u32[]{:S(2)}) async-start(bf16[16,32,512]{2,1,0:T(8,128)(2,1)} %broadcast_in_dim.4), calls=%async_computation.3 | async-start | bytes 1048576 | tf_op jit(solution)/shard_map/all_to_all | solution.py:436
  139.8 30.2 %copy-start.4 = (f32[2048]{0:T(1024)S(1)}, f32[2048]{0:T(1024)}, u32[]{:S(2)}) copy-start(f32[2048]{0:T(1024)} %param.27) | copy-start | bytes 24580
  139.8 30.2 %copy-start.7 = (f32[16]{0:T(128)S(1)}, f32[16]{0:T(128)}, u32[]{:S(2)}) copy-start(f32[16]{0:T(128)} %bias.1) | copy-start | bytes 196
  141.3 13.0 %all-to-all-start.1 = ((bf16[4,144,640]{2,1,0:T(8,128)(2,1)}), bf16[4,144,640]{2,1,0:T(8,128)(2,1)S(1)}, u32[]{:S(2)}, u32[]{:S(2)}) async-start(bf16[4,144,640]{2,1,0:T(8,128)(2,1)} %bitcast.9), calls=%async_computation.1 | async-start | bytes 1474560 | tf_op jit(solution)/shard_map/all_to_all | solution.py:430
  144.8 12.3 %collective-permute-start.3 = (bf16[512,512]{1,0:T(8,128)(2,1)S(1)}, bf16[512,512]{1,0:T(8,128)(2,1)S(1)}, u32[]{:S(2)}, u32[]{:S(2)}) collective-permute-start(bf16[512,512]{1,0:T(8,128)(2,1)S(1)} %bitcast.24), channel_id=1, source_target_pairs={{0,24},{8,0},{16,8},{24,16},{1,25},{9,1},{17,9},{25,17},{2,26},{10... | collective-permute-start | bytes 1572872 | tf_op jit(solution)/shard_map/ppermute | solution.py:405
  149.3 11.5 %collective-permute-start.2 = (bf16[512,512]{1,0:T(8,128)(2,1)S(1)}, bf16[512,512]{1,0:T(8,128)(2,1)S(1)}, u32[]{:S(2)}, u32[]{:S(2)}) collective-permute-start(bf16[512,512]{1,0:T(8,128)(2,1)S(1)} %bitcast.25), channel_id=1, source_target_pairs={{0,16},{8,24},{16,0},{24,8},{1,17},{9,25},{17,1},{25,9},{2,18},{10... | collective-permute-start | bytes 1572872 | tf_op jit(solution)/shard_map/ppermute | solution.py:405
  151.8 18.1 %collective-permute-start.1 = (bf16[512,512]{1,0:T(8,128)(2,1)S(1)}, bf16[512,512]{1,0:T(8,128)(2,1)S(1)}, u32[]{:S(2)}, u32[]{:S(2)}) collective-permute-start(bf16[512,512]{1,0:T(8,128)(2,1)S(1)} %bitcast.26), channel_id=1, source_target_pairs={{0,8},{8,16},{16,24},{24,0},{1,9},{9,17},{17,25},{25,1},{2,10},{10... | collective-permute-start | bytes 1572872 | tf_op jit(solution)/shard_map/ppermute | solution.py:405
Sparse Core Ops, SparseCore 0:
  80.1 84.3 all-gather.2

commit v3 on v2

v3 whole, which is shorter than its diff:
```python
import jax
import jax.numpy as jnp
from jax import lax
from jax.experimental import pallas as pl
from jax.experimental.pallas import tpu as pltpu
from jax.sharding import PartitionSpec as P

BLOCK = 128
CONV = 4
EPS = 1e-06
HALO = 16
ROWS = BLOCK + HALO
F32 = jnp.float32
BF16 = jnp.bfloat16
HIGH = lax.Precision.HIGHEST
NT = (((1,), (1,)), ((), ()))
TN = (((0,), (0,)), ((), ()))


def vmem(limit=48):
    return pltpu.CompilerParams(vmem_limit_bytes=limit * 1024 * 1024)


def iota(shape, dim):
    return lax.broadcasted_iota(jnp.int32, shape, dim)


def softplus(x):
    return jnp.maximum(x, 0.0) + jnp.log1p(jnp.exp(-jnp.abs(x)))


def silu(x):
    return x / (1.0 + jnp.exp(-x))


def pull(pairs, sems):
    copies = [pltpu.make_async_copy(src, dst, sems.at[i]) for i, (src, dst) in enumerate(pairs)]
    for copy in copies:
        copy.start()
    return copies


def shuffled(normed, f, g):
    lane = iota((normed.shape[0], 128), 1) // 32
    out = None
    for k in range(4):
        at = (4 * g + k) * 128
        piece = normed[:, at : at + 128]
        shift = ((k - f) * 32) % 128
        if shift:
            piece = pltpu.roll(piece, shift, 1)
        out = piece if out is None else jnp.where(lane == k, piece, out)
    return out.astype(BF16)


def normalised(x, gain):
    wide = x.astype(F32)
    scale = lax.rsqrt(jnp.mean(wide * wide, axis=-1, keepdims=True) + EPS)
    return (wide * scale * gain).astype(BF16)


def prep_kernel(*refs):
    x_hbm, gain_hbm, ws_hbm = refs[:3]
    sources = refs[3:12]
    xs_ref, step_ref, first_ref, second_ref = refs[12:16]
    x_ref, gain_ref, ws_ref, third_ref, sems, wsems = refs[16:]
    early = pull(((x_hbm.at[0], x_ref), (gain_hbm, gain_ref), (ws_hbm, ws_ref)), sems)
    pairs = []
    outs = (first_ref, second_ref, third_ref)
    at, which = 0, 0
    for n, src in enumerate(sources):
        if n in (4, 7):
            at, which = 0, which + 1
        pairs.append((src, outs[which].at[:, pl.ds(at, src.shape[1])]))
        at += src.shape[1]
    later = pull(pairs, wsems)
    for copy in early:
        copy.wait()
    normed = normalised(x_ref[...], gain_ref[...])
    step_ref[...] = softplus(
        lax.dot_general(ws_ref[...], normed, NT, preferred_element_type=F32)
    )
    wide = normed.astype(F32)
    for f in range(4):
        for g in range(4):
            xs_ref[f, HALO:ROWS, g * 128 : (g + 1) * 128] = shuffled(wide, f, g)
    for copy in later:
        copy.wait()
    for f in range(4):
        xs_ref[f, ROWS:, :] = third_ref[...]


def prep_call(inputs, gain, w_step_t, *arrays):
    rows, width = inputs.shape[1:]
    heads = w_step_t.shape[0]
    part = arrays[0].shape[0]
    widths = [sum(a.shape[1] for a in group) for group in (arrays[:4], arrays[4:7], arrays[7:])]
    hbm = pl.BlockSpec(memory_space=pltpu.HBM)
    return pl.pallas_call(
        prep_kernel,
        in_specs=[hbm] * 12,
        out_shape=(
            jax.ShapeDtypeStruct((4, ROWS + part, width // 4), BF16),
            jax.ShapeDtypeStruct((heads, rows), F32),
            jax.ShapeDtypeStruct((part, widths[0]), BF16),
            jax.ShapeDtypeStruct((part, widths[1]), BF16),
        ),
        scratch_shapes=[
            pltpu.VMEM((rows, width), BF16),
            pltpu.VMEM((1, width), F32),
            pltpu.VMEM((heads, width), BF16),
            pltpu.VMEM((part, widths[2]), BF16),
            pltpu.SemaphoreType.DMA((3,)),
            pltpu.SemaphoreType.DMA((9,)),
        ],
        name="prep",
    )(inputs, gain.reshape(1, -1), w_step_t, *arrays)


def halo_kernel(xs_in, halo_ref, gain_ref, xs_out, rim_ref, sem):
    wide = normalised(halo_ref[...], gain_ref[...]).astype(F32)
    for f in range(4):
        for g in range(4):
            rim_ref[f, :, g * 128 : (g + 1) * 128] = shuffled(wide, f, g)
    copy = pltpu.make_async_copy(rim_ref, xs_out.at[:, pl.ds(0, HALO)], sem)
    copy.start()
    copy.wait()


def halo_call(xs, halo, gain):
    anywhere = pl.BlockSpec(memory_space=pl.ANY)
    whole = pl.BlockSpec(memory_space=pltpu.VMEM)
    return pl.pallas_call(
        halo_kernel,
        in_specs=[anywhere, whole, whole],
        out_specs=anywhere,
        out_shape=jax.ShapeDtypeStruct(xs.shape, BF16),
        input_output_aliases={0: 0},
        scratch_shapes=[pltpu.VMEM((4, HALO, xs.shape[2]), BF16), pltpu.SemaphoreType.DMA],
        name="halo",
    )(xs, halo, gain.reshape(1, -1))


def project_kernel(x_ref, w_ref, out_ref):
    for f in range(4):
        out_ref[f] = jnp.dot(
            x_ref[f, 0:ROWS, :], w_ref[...], preferred_element_type=F32
        ).astype(BF16)


def project_call(x, w):
    return pl.pallas_call(
        project_kernel,
        out_shape=jax.ShapeDtypeStruct((4, ROWS, w.shape[1]), BF16),
        compiler_params=vmem(),
        name="project",
    )(x, w)


def added(ref, at, width):
    total = ref[0, :, at : at + width].astype(F32)
    for j in range(1, 4):
        total = total + ref[j, :, at : at + width].astype(F32)
    return total.astype(BF16)


def convolved(wide_ref, taps):
    summed = None
    for i in range(CONV):
        at = HALO - CONV + 1 + i
        part = taps[i : i + 1] * wide_ref[at : at + BLOCK, :]
        summed = part if summed is None else summed + part
    return silu(summed).astype(BF16)


def local_kernel(
    ids, rate, act_ref, step_ref, off_ref, ci_ref, cb_ref, buf_ref,
    send_ref, xin_ref, bkey_ref, rows_ref, cols_ref, wide_ref, sems,
):
    tensor = ids[1]
    moved = pull(
        [
            (buf_ref.at[f, pl.ds(ROWS, 32)], send_ref.at[pl.ds(KEPT + 32 * f, 32)])
            for f in range(4)
        ],
        sems,
    )
    send_ref[0:BLOCK, :] = added(act_ref, 0, 512)[HALO:]
    wide_ref[...] = added(act_ref, 512, 384).astype(F32)
    conv = convolved(wide_ref, jnp.concatenate([ci_ref[...], cb_ref[...]], axis=1))
    xin, bkey = conv[:, 0:256], conv[:, 256:384]
    xin_ref[...] = xin
    bkey_ref[...] = bkey
    row = iota((BLOCK, BLOCK), 0)
    col = iota((BLOCK, BLOCK), 1)
    step = jnp.concatenate([step_ref[pl.ds(4 * tensor + h, 1), :] for h in range(4)], axis=0)
    rates = jnp.concatenate(
        [jnp.full((1, BLOCK), rate[4 * tensor + h], F32) for h in range(4)], axis=0
    )
    decay = off_ref[...] - rates * step
    decay8 = jnp.concatenate([decay, jnp.zeros((4, BLOCK), F32)], axis=0)
    upper = (row <= col).astype(F32)
    cum = jnp.dot(decay8, upper, precision=HIGH, preferred_element_type=F32)
    last = jnp.sum(decay, axis=1, keepdims=True)
    to_end = jnp.exp(last - cum[0:4]) * step
    eye = (row == col).astype(F32)
    cols = lax.dot_general(
        eye, jnp.concatenate([cum[0:4], to_end], axis=0), NT, precision=HIGH,
        preferred_element_type=F32,
    )
    rows_ref[...] = jnp.concatenate([cum[0:4], step], axis=0)
    cols_ref[...] = cols
    wide_key = bkey.astype(F32)
    for h in range(4):
        wk = (wide_key * cols[:, 4 + h : 5 + h]).astype(BF16)
        state = lax.dot_general(
            xin[:, h * 64 : (h + 1) * 64], wk, TN, preferred_element_type=F32
        )
        log = jnp.broadcast_to(last[h : h + 1], (8, BLOCK))
        high = log.astype(BF16).astype(F32)
        logs = jnp.concatenate([high, log - high], axis=0).astype(BF16)
        send_ref[BLOCK : BLOCK + 64, h * 128 : (h + 1) * 128] = state.astype(BF16)
        send_ref[BLOCK + 64 : KEPT, h * 128 : (h + 1) * 128] = logs
    for copy in moved:
        copy.wait()


def local_call(ids, rate, act, step, offset, conv_weight, buf):
    full = lambda *shape: pl.BlockSpec(shape, lambda i, ids, rate: (0,) * len(shape))
    return pl.pallas_call(
        local_kernel,
        grid_spec=pltpu.PrefetchScalarGridSpec(
            num_scalar_prefetch=2,
            grid=(1,),
            in_specs=[
                full(*act.shape),
                full(*step.shape),
                full(*offset.shape),
                pl.BlockSpec((CONV, 256), lambda i, ids, rate: (0, ids[1])),
                pl.BlockSpec((CONV, 128), lambda i, ids, rate: (0, 16 + ids[1])),
                pl.BlockSpec(memory_space=pl.ANY),
            ],
            out_specs=[
                full(SENT, 512), full(BLOCK, 256), full(BLOCK, 128), full(8, BLOCK),
                full(BLOCK, 8),
            ],
            scratch_shapes=[pltpu.VMEM((ROWS, 384), F32), pltpu.SemaphoreType.DMA((4,))],
        ),
        out_shape=(
            jax.ShapeDtypeStruct((SENT, 512), BF16),
            jax.ShapeDtypeStruct((BLOCK, 256), BF16),
            jax.ShapeDtypeStruct((BLOCK, 128), BF16),
            jax.ShapeDtypeStruct((8, BLOCK), F32),
            jax.ShapeDtypeStruct((BLOCK, 8), F32),
        ),
        compiler_params=vmem(),
        name="ssd_local",
    )(ids, rate, act, step, offset, conv_weight, conv_weight, buf)


def inner_kernel(
    ids, act_ref, cc_ref, xin_ref, bkey_ref, rows_ref, cols_ref,
    yin_ref, gate_ref, cq_ref, q_ref, wide_ref,
):
    gate_ref[...] = silu(added(act_ref, 0, 256)[HALO:].astype(F32))
    q_ref[...] = added(act_ref, 384, 256)[HALO:]
    wide_ref[...] = added(act_ref, 256, 128).astype(F32)
    cquery = convolved(wide_ref, cc_ref[...])
    cq_ref[...] = cquery
    lower = iota((BLOCK, BLOCK), 0) >= iota((BLOCK, BLOCK), 1)
    inner = lax.dot_general(cquery, bkey_ref[...], NT, preferred_element_type=F32)
    for h in range(4):
        spread = cols_ref[:, h : h + 1] - rows_ref[h : h + 1, :]
        decayed = jnp.exp(jnp.where(lower, spread, 0.0))
        mix = jnp.where(lower, inner * decayed * rows_ref[4 + h : 5 + h, :], 0.0).astype(BF16)
        yin_ref[:, h * 64 : (h + 1) * 64] = jnp.dot(
            mix, xin_ref[:, h * 64 : (h + 1) * 64], preferred_element_type=F32
        )


def inner_call(ids, act, conv_weight, xin, bkey, rows, cols):
    full = lambda *shape: pl.BlockSpec(shape, lambda i, ids: (0,) * len(shape))
    return pl.pallas_call(
        inner_kernel,
        grid_spec=pltpu.PrefetchScalarGridSpec(
            num_scalar_prefetch=1,
            grid=(1,),
            in_specs=[
                full(*act.shape),
                pl.BlockSpec((CONV, 128), lambda i, ids: (0, 24 + ids[1])),
                full(BLOCK, 256), full(BLOCK, 128), full(8, BLOCK), full(BLOCK, 8),
            ],
            out_specs=[full(BLOCK, 256), full(BLOCK, 256), full(BLOCK, 128), full(BLOCK, 256)],
            scratch_shapes=[pltpu.VMEM((BLOCK + HALO, 128), F32)],
        ),
        out_shape=(
            jax.ShapeDtypeStruct((BLOCK, 256), F32),
            jax.ShapeDtypeStruct((BLOCK, 256), F32),
            jax.ShapeDtypeStruct((BLOCK, 128), BF16),
            jax.ShapeDtypeStruct((BLOCK, 256), BF16),
        ),
        compiler_params=vmem(),
        name="ssd_inner",
    )(ids, act, conv_weight, xin, bkey, rows, cols)


SUB = 256
KEYS = 512
KEPT = BLOCK + 80
SENT = KEPT + BLOCK


def attend_kernel(
    ids, bias, q_ref, yin_ref, gate_ref, cq_ref, cols_ref, gain_ref, all_hbm,
    out_ref, kv_ref, st_ref, w_ref, acc_ref, late_ref, hold_ref, sems, ksems,
):
    block, tensor = ids[0], ids[1]
    per = KEYS // BLOCK
    count = all_hbm.shape[0]
    chunks = range(count // per - 1, -1, -1)

    def move(chunk):
        picked = pl.ds(chunk * per, per)
        return pltpu.make_async_copy(
            all_hbm.at[picked, pl.ds(0, BLOCK)], kv_ref.at[picked], ksems.at[chunk]
        )

    states = pltpu.make_async_copy(all_hbm.at[:, pl.ds(BLOCK, 80)], st_ref, sems.at[0])
    states.start()
    for chunk in chunks:

        @pl.when(chunk * per <= block)
        def _(chunk=chunk):
            move(chunk).start()

    weights = pltpu.make_async_copy(all_hbm.at[:, pl.ds(KEPT, BLOCK)], w_ref, sems.at[1])
    weights.start()
    acc_ref[...] = jnp.zeros_like(acc_ref)
    late_ref[...] = jnp.zeros_like(late_ref)
    hold_ref[...] = jnp.zeros_like(hold_ref)
    states.wait()

    def advance(k, carry):
        logs = st_ref[k, 64:80, :].astype(F32)
        decay = jnp.exp(logs[0:8] + logs[8:16])
        hold_ref[...] = hold_ref[...] * jnp.concatenate([decay] * 8, axis=0) + st_ref[
            k, 0:64, :
        ].astype(F32)
        return carry

    lax.fori_loop(0, block, advance, 0)
    cquery = cq_ref[...]
    ys = []
    for h in range(4):
        enter = hold_ref[:, h * 128 : (h + 1) * 128].astype(BF16)
        moved = lax.dot_general(cquery, enter, NT, preferred_element_type=F32)
        ys.append(moved * jnp.exp(cols_ref[:, h : h + 1]))
    gated = (yin_ref[...] + jnp.concatenate(ys, axis=1)) * gate_ref[...]
    scale = lax.rsqrt(jnp.mean(gated * gated, axis=-1, keepdims=True) + EPS)
    mixed = (gated * scale * gain_ref[...]).astype(BF16)
    after = (iota((SUB, SUB), 0) > iota((SUB, SUB), 1)).astype(BF16)
    ones = jnp.ones((SUB, 128), BF16)
    for chunk in chunks:

        @pl.when(chunk * per <= block)
        def _(chunk=chunk):
            move(chunk).wait()
            for h in range(2):
                late = late_ref[h]
                gained = acc_ref[h]
                query = q_ref[:, h * 128 : (h + 1) * 128]
                for sub in range(KEYS // SUB - 1, -1, -1):
                    at = chunk * KEYS + sub * SUB
                    first = at // BLOCK
                    before = at + iota((BLOCK, SUB), 1) < block * BLOCK + iota((BLOCK, SUB), 0)
                    key = kv_ref[first : first + 2, :, h * 128 : (h + 1) * 128]
                    value = kv_ref[first : first + 2, :, 256 + h * 128 : 256 + (h + 1) * 128]
                    logits = lax.dot_general(
                        query, key.reshape(SUB, 128), NT, preferred_element_type=F32
                    )
                    logits = logits * (128 ** -0.5) + bias[2 * tensor + h]
                    soft = jnp.maximum(logits, 0.0) + jnp.log(1.0 + jnp.exp(-jnp.abs(logits)))
                    passed = jnp.where(before, -soft, 0.0)
                    high = passed.astype(BF16)
                    low = (passed - high.astype(F32)).astype(BF16)
                    tail = jnp.dot(high, after, preferred_element_type=F32) + jnp.dot(
                        low, after, preferred_element_type=F32
                    )
                    whole = jnp.dot(high, ones, preferred_element_type=F32) + jnp.dot(
                        low, ones, preferred_element_type=F32
                    )
                    later = jnp.concatenate([late] * (SUB // 128), axis=1)
                    weight = jnp.where(before, jnp.exp(logits - soft + (tail + later)), 0.0)
                    gained = gained + jnp.dot(
                        weight.astype(BF16), value.reshape(SUB, 128), preferred_element_type=F32
                    )
                    late = late + whole
                late_ref[h] = late
                acc_ref[h] = gained

    both = jnp.concatenate([mixed, acc_ref[0].astype(BF16), acc_ref[1].astype(BF16)], axis=1)
    weights.wait()
    for s in range(count):
        out_ref[:, 128 * s : 128 * (s + 1)] = lax.dot_general(
            both, w_ref[s], NT, preferred_element_type=F32
        ).astype(BF16)


def attend_call(ids, bias, q, yin, gate, cq, cols, gain, gathered):
    full = lambda *shape: pl.BlockSpec(shape, lambda i, ids, bias: (0,) * len(shape))
    count = gathered.shape[0]
    return pl.pallas_call(
        attend_kernel,
        grid_spec=pltpu.PrefetchScalarGridSpec(
            num_scalar_prefetch=2,
            grid=(1,),
            in_specs=[
                full(BLOCK, 256), full(BLOCK, 256), full(BLOCK, 256), full(BLOCK, 128),
                full(BLOCK, 8), pl.BlockSpec((1, 256), lambda i, ids, bias: (0, ids[1])),
                pl.BlockSpec(memory_space=pltpu.HBM),
            ],
            out_specs=full(BLOCK, 2048),
            scratch_shapes=[
                pltpu.VMEM((count, BLOCK, 512), BF16),
                pltpu.VMEM((count, 80, 512), BF16),
                pltpu.VMEM((count, BLOCK, 512), BF16),
                pltpu.VMEM((2, BLOCK, 128), F32),
                pltpu.VMEM((2, BLOCK, 128), F32),
                pltpu.VMEM((64, 512), F32),
                pltpu.SemaphoreType.DMA((2,)),
                pltpu.SemaphoreType.DMA((count * BLOCK // KEYS,)),
            ],
        ),
        out_shape=jax.ShapeDtypeStruct((BLOCK, 2048), BF16),
        compiler_params=vmem(),
        name="attend",
    )(ids, bias, q, yin, gate, cq, cols, gain.reshape(1, -1), gathered)


def body(
    inputs, norm_gain, w_gate, w_input, w_bkey, w_cquery, w_step, conv_weight, decay_rate,
    decay_offset, ssd_gain, w_query, w_key, w_value, stick_bias, out_mixer, out_attend,
):
    length = lax.axis_size("sp")
    ids = jnp.stack([lax.axis_index("sp"), lax.axis_index("tp")]).astype(jnp.int32)
    halo = lax.ppermute(
        inputs[0, BLOCK - HALO :], "sp", [(i, i + 1) for i in range(length - 1)]
    )
    split, step, first, second = prep_call(
        inputs, norm_gain, w_step.T, w_key, w_value, w_input, w_bkey, w_gate, w_cquery, w_query,
        out_mixer.T, out_attend.T,
    )
    split = halo_call(split, halo, norm_gain)
    tokens = lax.all_to_all(split, "fs", 0, 0, tiled=True)

    def projected(weights):
        whole = lax.all_gather(weights, "sp", axis=0, tiled=True)
        return lax.all_to_all(project_call(tokens, whole), "fs", 0, 0, tiled=True)

    send, xin, bkey, srows, scols = local_call(
        ids, decay_rate, projected(first), step, decay_offset[0].T, conv_weight, tokens
    )
    gathered = lax.all_gather(send, "sp", axis=0)
    yin, gate, cq, q = inner_call(ids, projected(second), conv_weight, xin, bkey, srows, scols)
    partial = attend_call(ids, stick_bias, q, yin, gate, cq, scols, ssd_gain, gathered)
    parts = lax.all_to_all(partial.reshape(8, 16, 2048), "tp", 0, 0, tiled=True)
    return jnp.sum(parts.astype(F32), axis=0).astype(BF16)[None]


def solution(mesh):
    shard = P(("sp", "fs"), "tp")
    return jax.shard_map(
        body,
        mesh=mesh,
        in_specs=(
            P("fs", "sp", None), P(), shard, shard, shard, shard, P(), P(), P(),
            P("fs", "sp", "tp"), P(), shard, shard, shard, P(),
            P("tp", ("sp", "fs")), P("tp", ("sp", "fs")),
        ),
        out_specs=P("fs", ("sp", "tp"), None),
        check_vma=False,
    )
```

time: 209 us -> 187 us (0.89)
  waiting for transfers between devices: 25.5 us -> 55.4 us
  blocking collectives: 113 us -> 87.8 us
  starting transfers between devices: 33.3 us -> 12.9 us
  matrix products: 3.28 us -> 0 us
  local copies, waits for them, and re-layouts: 4.37 us -> 1.53 us
    all_gather x1, waiting for transfers between devices: 0.01 us -> 45.8 us  [body(): gathered = lax.all_gather(send, 'sp', axis=0)]
    all_gather x2, blocking collectives: 86.6 us -> 57.7 us  [projected(): whole = lax.all_gather(weights, 'sp', axis=0, tiled=True)]
    ppermute x3 -> x0, waiting for transfers between devices: 14.5 us -> none  [rotated(): lax.ppermute(shard, axis, [(i, (i + by) % length) for i in range(length)])]
    all_to_all x4 -> x2, starting transfers between devices: 19.4 us -> 8.6 us  [the longest x1 4.4 us: projected(): return lax.all_to_all(project_call(tokens, whole), 'fs', 0, 0, tiled=True)]
    all_to_all x0 -> x1, blocking collectives: none -> 10.5 us  [projected(): return lax.all_to_all(project_call(tokens, whole), 'fs', 0, 0, tiled=True)]
    ppermute x3 -> x0, starting transfers between devices: 9.51 us -> none  [rotated(): lax.ppermute(shard, axis, [(i, (i + by) % length) for i in range(length)])]
    all_to_all x1, blocking collectives: 26.1 us -> 19.6 us  [body(): parts = lax.all_to_all(partial.reshape(8, 16, 2048), 'tp', 0, 0, tiled=True)]
    dot_general x2 -> x0, matrix products: 3.28 us -> none  [projected(): act = jnp.dot(tokens, whole, preferred_element_type=F32).astype(BF16)]
  transfers between devices with their start and end apart: 9 -> 4, of which waited for: 5 -> 2; matrix products, arithmetic and copies ran while one was open for 1% -> 0% of each run, Pallas kernels for 3% -> 2%
where the time goes in v3:
time: 187 us
  blocking collectives  87.8 us (47%)
  waiting for transfers between devices  55.4 us (30%)
  Pallas kernels  14.8 us (8%)
  between operations  13.5 us (7%)
  starting transfers between devices  12.9 us (7%)
    all_gather x2, blocking collectives, projected(): whole = lax.all_gather(weights, 'sp', axis=0, tiled=True)  57.7 us
    all_gather x1, waiting for transfers between devices, body(): gathered = lax.all_gather(send, 'sp', axis=0)  45.8 us
    all_to_all x1, blocking collectives, body(): parts = lax.all_to_all(partial.reshape(8, 16, 2048), 'tp', 0, 0, tiled=True)  19.6 us
    all_to_all x1, blocking collectives, projected(): return lax.all_to_all(project_call(tokens, whole), 'fs', 0, 0, tiled=True)  10.5 us
    all_to_all x1, waiting for transfers between devices, projected(): return lax.all_to_all(project_call(tokens, whole), 'fs', 0, 0, tiled=True)  9.58 us
    all_to_all x1, starting transfers between devices, projected(): return lax.all_to_all(project_call(tokens, whole), 'fs', 0, 0, tiled=True)  4.4 us
    ppermute x1, starting transfers between devices, body(): lax.ppermute(inputs[0, BLOCK - HALO:], 'sp', [(i, i + 1) for i in range(l...  4.35 us
    pallas_call x1, Pallas kernels, attend_call(): pl.pallas_call(attend_kernel, grid_spec=pltpu.PrefetchScalarGridSpec(num_...  4.28 us
  transfers between devices with their start and end apart: 4, of which 2 were waited for; matrix products, arithmetic and copies ran while one was open for 0% of the time, Pallas kernels for 2%

profile of v3, /device:TPU:1, one launch (start us, length us, event | category | flops | bytes accessed | tf_op | source)
XLA Modules:
  0.0 186.7 jit_solution(17283552451983965869)
XLA Ops:
  6.5 0.9 slice_bitcast_fusion
  7.4 4.4 %collective-permute-start = (bf16[16,2048]{1,0:T(8,128)(2,1)S(1)}, bf16[16,2048]{1,0:T(8,128)(2,1)S(1)}, u32[]{:S(2)}, u32[]{:S(2)}) collective-permute-start(bf16[16,2048]{1,0:T(8,128)(2,1)S(1)} %slice_bitcast_fusion), channel_id=1, source_target_pairs={{0,32},{32,64},{64,96},{96,128},{128,160},{160,192},{192,224},{224... | collective-permute-start | bytes 196616 | tf_op jit(solution)/shard_map/ppermute | solution.py:446
  11.8 2.9 %prep.1 = (bf16[4,176,512]{2,1,0:T(8,128)(2,1)}, f32[32,128]{1,0:T(8,128)}, bf16[32,896]{1,0:T(8,128)(2,1)}, bf16[32,640]{1,0:T(8,128)(2,1)}) custom-call(bf16[1,128,2048]{2,1,0:T(8,128)(2,1)} %refs_0_.1, f32[1,2048]{1,0:T(1,128)} %bitcast.20, bf16[32,2048]{1,0:T(8,128)(2,1)} %bitcast.19, bf16[32,256]{1,0:T(8,128)(2,1)} %refs_3_.1, bf16[32,256]{1,0:T(8,128)(2,1)} %refs_4_.1, ...), custom_call_target="tpu_custom_call" | custom-call | tf_op jit(solution)/shard_map/prep/pallas_call | solution.py:99
  14.7 0.0 copy-start.1
  14.7 0.0 copy-start.7
  14.7 0.0 collective-permute-done.halo_ref
  14.7 0.0 copy-start.6
  14.8 0.6 copy-done.6
  15.4 1.7 halo.1
  17.1 4.2 %all-to-all-start = ((bf16[4,176,512]{2,1,0:T(8,128)(2,1)}), bf16[4,176,512]{2,1,0:T(8,128)(2,1)S(1)}, u32[]{:S(2)}, u32[]{:S(2)}) async-start(bf16[4,176,512]{2,1,0:T(8,128)(2,1)} %halo.1), calls=%async_computation | async-start | bytes 1441792 | tf_op jit(solution)/shard_map/all_to_all | solution.py:454
  21.3 33.6 %all_gather.13.w_ref = bf16[512,896]{1,0:T(8,128)(2,1)S(1)} all-gather(bf16[32,896]{1,0:T(8,128)(2,1)} %get-tuple-element.20), channel_id=1, replica_groups=mesh['sp'=16,'fs'=4,'tp'=8] {'sp'}, dimensions={0}, use_global_device_ids=true | all-gather | bytes 974848 | tf_op jit(solution)/shard_map/all_gather | solution.py:457
  54.9 0.0 all-to-all-done.x_ref.buf_ref
  54.9 1.8 project.3
  56.7 4.4 %all-to-all-start.2 = ((bf16[4,144,896]{2,1,0:T(8,128)(2,1)}), bf16[4,144,896]{2,1,0:T(8,128)(2,1)S(1)}, u32[]{:S(2)}, u32[]{:S(2)}) async-start(bf16[4,144,896]{2,1,0:T(8,128)(2,1)} %project.3), calls=%async_computation.2 | async-start | bytes 2064384 | tf_op jit(solution)/shard_map/all_to_all | solution.py:458
  61.1 0.0 all-gather.3.cloned.1.call-start
  61.2 0.1 pad_add_fusion.ids
  61.2 9.6 %all-to-all-done.2.act_ref = bf16[4,144,896]{2,1,0:T(8,128)(2,1)S(1)} async-done(((bf16[4,144,896]{2,1,0:T(8,128)(2,1)}), bf16[4,144,896]{2,1,0:T(8,128)(2,1)S(1)}, u32[]{:S(2)}, u32[]{:S(2)}) %all-to-all-start.2) | async-done | bytes 1032224 | tf_op jit(solution)/shard_map/all_to_all | solution.py:458
  70.8 0.0 copy-done
  70.8 0.0 copy-done.3
  70.8 0.0 copy-done.4
  70.8 0.0 copy-done.1
  70.8 2.4 %ssd_local.1 = (bf16[336,512]{1,0:T(8,128)(2,1)}, bf16[128,256]{1,0:T(8,128)(2,1)S(1)}, bf16[128,128]{1,0:T(8,128)(2,1)S(1)}, f32[8,128]{1,0:T(8,128)S(1)}, f32[128,8]{1,0:T(8,128)S(1)}) custom-call(s32[2]{0:T(128)S(1)} %pad_add_fusion.ids, f32[32]{0:T(128)S(1)} %copy-done.4, bf16[4,144,896]{2,1,0:T(8,128)(2,1)S(1)} %all-to-all-done.2.act_ref, ...), custom_call_target="tpu_custom_call" | custom-call | tf_op jit(solution)/shard_map/ssd_local/pallas_call | solution.py:230
  73.2 0.0 all-gather.3.cloned.1.call-update
  73.3 24.0 %all_gather.12.w_ref = bf16[512,640]{1,0:T(8,128)(2,1)S(1)} all-gather(bf16[32,640]{1,0:T(8,128)(2,1)S(1)} %copy-done.7), channel_id=1, replica_groups=mesh['sp'=16,'fs'=4,'tp'=8] {'sp'}, dimensions={0}, use_global_device_ids=true | all-gather | bytes 696320 | tf_op jit(solution)/shard_map/all_gather | solution.py:457
  97.3 0.6 project.2
  97.9 10.5 %all_to_all.20.act_ref = bf16[4,144,640]{2,1,0:T(8,128)(2,1)S(1)} all-to-all(bf16[4,144,640]{2,1,0:T(8,128)(2,1)S(1)} %project.2), channel_id=1, replica_groups=mesh['sp'=16,'fs'=4,'tp'=8] {'fs'}, dimensions={0} | all-to-all | bytes 1474560 | tf_op jit(solution)/shard_map/all_to_all | solution.py:458
  108.4 1.1 ssd_inner.1
  109.5 45.8 %all-gather.3.cloned.1.call-done = bf16[5376,512]{1,0:T(8,128)(2,1)} async-done(((bf16[336,512]{1,0:T(8,128)(2,1)}), bf16[5376,512]{1,0:T(8,128)(2,1)}) %all-gather.3.cloned.1.call-update) | async-done | bytes 5505040 | tf_op jit(solution)/shard_map/all_gather | solution.py:463
  155.3 0.0 copy-done.5
  155.3 4.3 %attend.1 = bf16[128,2048]{1,0:T(8,128)(2,1)S(1)} custom-call(s32[2]{0:T(128)S(1)} %pad_add_fusion.ids, f32[16]{0:T(128)S(1)} %copy-done.5, bf16[128,256]{1,0:T(8,128)(2,1)S(1)} %get-tuple-element.26.q_ref, f32[128,256]{1,0:T(8,128)S(1)} %get-tuple-element.27.yin_ref, f32[128,256]{1,0:T(8,128)S(1)} %get-tuple-element.28.gate_ref, ...), custom_call_target="tpu_custom_call" | custom-call | tf_op jit(solution)/shard_map/attend/pallas_call | solution.py:412
  159.6 19.6 %all_to_all.21 = bf16[8,16,2048]{2,1,0:T(8,128)(2,1)S(1)} all-to-all(bf16[8,16,2048]{2,1,0:T(8,128)(2,1)S(1)} %bitcast.15), channel_id=1, replica_groups=mesh['sp'=16,'fs'=4,'tp'=8] {'tp'}, dimensions={0} | all-to-all | bytes 1048576 | tf_op jit(solution)/shard_map/all_to_all | solution.py:466
  179.2 0.7 reduce_sum.12
  (7 shorter events, 0.0 us)
Async XLA Ops:
  6.5 64.3 %copy-start = (f32[4,4096]{1,0:T(4,128)S(1)}, f32[4,4096]{1,0:T(4,128)}, u32[]{:S(2)}) copy-start(f32[4,4096]{1,0:T(4,128)} %cc_ref.1) | copy-start | bytes 196612
  6.5 64.3 %copy-start.3 = (f32[1,128,4]{1,2,0:T(4,128)S(1)}, f32[1,128,4]{1,2,0:T(4,128)}, u32[]{:S(2)}) copy-start(f32[1,128,4]{1,2,0:T(4,128)} %param.26) | copy-start | bytes 6148
  6.5 64.3 %copy-start.4 = (f32[32]{0:T(128)S(1)}, f32[32]{0:T(128)}, u32[]{:S(2)}) copy-start(f32[32]{0:T(128)} %rate.1) | copy-start | bytes 388
  7.4 7.3 %collective-permute-start = (bf16[16,2048]{1,0:T(8,128)(2,1)S(1)}, bf16[16,2048]{1,0:T(8,128)(2,1)S(1)}, u32[]{:S(2)}, u32[]{:S(2)}) collective-permute-start(bf16[16,2048]{1,0:T(8,128)(2,1)S(1)} %slice_bitcast_fusion), channel_id=1, source_target_pairs={{0,32},{32,64},{64,96},{96,128},{128,160},{160,192},{192,224},{224... | collective-permute-start | bytes 196616 | tf_op jit(solution)/shard_map/ppermute | solution.py:446
  14.7 56.1 %copy-start.1 = (f32[32,128]{1,0:T(8,128)S(1)}, f32[32,128]{1,0:T(8,128)}, u32[]{:S(2)}) copy-start(f32[32,128]{1,0:T(8,128)} %get-tuple-element.21.step_ref) | copy-start | bytes 49156
  14.7 58.5 %copy-start.7 = (bf16[32,640]{1,0:T(8,128)(2,1)S(1)}, bf16[32,640]{1,0:T(8,128)(2,1)}, u32[]{:S(2)}) copy-start(bf16[32,640]{1,0:T(8,128)(2,1)} %get-tuple-element.19) | copy-start | bytes 122884
  14.7 0.6 copy-start.6
  17.1 37.8 %all-to-all-start = ((bf16[4,176,512]{2,1,0:T(8,128)(2,1)}), bf16[4,176,512]{2,1,0:T(8,128)(2,1)S(1)}, u32[]{:S(2)}, u32[]{:S(2)}) async-start(bf16[4,176,512]{2,1,0:T(8,128)(2,1)} %halo.1), calls=%async_computation | async-start | bytes 1441792 | tf_op jit(solution)/shard_map/all_to_all | solution.py:454
  54.9 100.4 %copy-start.2 = (f32[2048]{0:T(1024)S(1)}, f32[2048]{0:T(1024)}, u32[]{:S(2)}) copy-start(f32[2048]{0:T(1024)} %param.27) | copy-start | bytes 24580
  54.9 100.4 %copy-start.5 = (f32[16]{0:T(128)S(1)}, f32[16]{0:T(128)}, u32[]{:S(2)}) copy-start(f32[16]{0:T(128)} %bias.1) | copy-start | bytes 196
  56.7 14.1 %all-to-all-start.2 = ((bf16[4,144,896]{2,1,0:T(8,128)(2,1)}), bf16[4,144,896]{2,1,0:T(8,128)(2,1)S(1)}, u32[]{:S(2)}, u32[]{:S(2)}) async-start(bf16[4,144,896]{2,1,0:T(8,128)(2,1)} %project.3), calls=%async_computation.2 | async-start | bytes 2064384 | tf_op jit(solution)/shard_map/all_to_all | solution.py:458
  61.1 94.1 %all-gather.3.cloned.1.call-start = ((), (), s32[]{:S(2)}) async-start(), calls=%async_computation.4 | async-start | bytes 5849088 | tf_op jit(solution)/shard_map/all_gather | solution.py:463
Sparse Core Ops, SparseCore 0:
  73.4 81.8 all-gather.2

commit v4 on v3

--- a/solution.py
+++ b/solution.py
@@ -69,7 +69,7 @@
     outs = (first_ref, second_ref, third_ref)
     at, which = 0, 0
     for n, src in enumerate(sources):
-        if n in (4, 7):
+        if n in (4, 8):
             at, which = 0, which + 1
         pairs.append((src, outs[which].at[:, pl.ds(at, src.shape[1])]))
         at += src.shape[1]
@@ -87,20 +87,21 @@
     for copy in later:
         copy.wait()
     for f in range(4):
-        xs_ref[f, ROWS:, :] = third_ref[...]
+        xs_ref[f, ROWS:, 0:256] = third_ref[0:16, :]
+        xs_ref[f, ROWS:, 256:512] = third_ref[16:32, :]
 
 
 def prep_call(inputs, gain, w_step_t, *arrays):
     rows, width = inputs.shape[1:]
     heads = w_step_t.shape[0]
     part = arrays[0].shape[0]
-    widths = [sum(a.shape[1] for a in group) for group in (arrays[:4], arrays[4:7], arrays[7:])]
+    widths = [sum(a.shape[1] for a in group) for group in (arrays[:4], arrays[4:8], arrays[8:])]
     hbm = pl.BlockSpec(memory_space=pltpu.HBM)
     return pl.pallas_call(
         prep_kernel,
         in_specs=[hbm] * 12,
         out_shape=(
-            jax.ShapeDtypeStruct((4, ROWS + part, width // 4), BF16),
+            jax.ShapeDtypeStruct((4, ROWS + HALO, width // 4), BF16),
             jax.ShapeDtypeStruct((heads, rows), F32),
             jax.ShapeDtypeStruct((part, widths[0]), BF16),
             jax.ShapeDtypeStruct((part, widths[1]), BF16),
@@ -141,17 +142,23 @@
     )(xs, halo, gain.reshape(1, -1))
 
 
-def project_kernel(x_ref, w_ref, out_ref):
+def project_kernel(x_ref, w_ref, out_ref, *kept):
+    width = out_ref.shape[2]
     for f in range(4):
         out_ref[f] = jnp.dot(
-            x_ref[f, 0:ROWS, :], w_ref[...], preferred_element_type=F32
+            x_ref[f, 0:ROWS, :], w_ref[:, 0:width], preferred_element_type=F32
         ).astype(BF16)
-
-
-def project_call(x, w):
+    for ref in kept:
+        ref[...] = w_ref[:, width:]
+
+
+def project_call(x, w, width):
+    outs = [jax.ShapeDtypeStruct((4, ROWS, width), BF16)]
+    if w.shape[1] > width:
+        outs.append(jax.ShapeDtypeStruct((w.shape[0], w.shape[1] - width), BF16))
     return pl.pallas_call(
         project_kernel,
-        out_shape=jax.ShapeDtypeStruct((4, ROWS, w.shape[1]), BF16),
+        out_shape=outs,
         compiler_params=vmem(),
         name="project",
     )(x, w)
@@ -180,7 +187,7 @@
     tensor = ids[1]
     moved = pull(
         [
-            (buf_ref.at[f, pl.ds(ROWS, 32)], send_ref.at[pl.ds(KEPT + 32 * f, 32)])
+            (buf_ref.at[f, pl.ds(ROWS, HALO)], send_ref.at[pl.ds(KEPT + HALO * f, HALO)])
             for f in range(4)
         ],
         sems,
@@ -307,17 +314,19 @@
 SUB = 256
 KEYS = 512
 KEPT = BLOCK + 80
-SENT = KEPT + BLOCK
+SENT = KEPT + 64
+LOG2E = 1.4426950408889634
 
 
 def attend_kernel(
-    ids, bias, q_ref, yin_ref, gate_ref, cq_ref, cols_ref, gain_ref, all_hbm,
-    out_ref, kv_ref, st_ref, w_ref, acc_ref, late_ref, hold_ref, sems, ksems,
+    ids, bias, q_ref, yin_ref, gate_ref, cq_ref, cols_ref, gain_ref, all_hbm, a0, a1, a2, a3,
+    out_ref, kv_ref, st_ref, wm_ref, wa_ref, acc_ref, late_ref, hold_ref, sems, ksems,
 ):
-    block, tensor = ids[0], ids[1]
+    block, tensor, mine = ids[0], ids[1], ids[2]
     per = KEYS // BLOCK
     count = all_hbm.shape[0]
     chunks = range(count // per - 1, -1, -1)
+    last = block // per
 
     def move(chunk):
         picked = pl.ds(chunk * per, per)
@@ -329,12 +338,17 @@
     states.start()
     for chunk in chunks:
 
-        @pl.when(chunk * per <= block)
+        @pl.when(chunk <= last)
         def _(chunk=chunk):
             move(chunk).start()
 
-    weights = pltpu.make_async_copy(all_hbm.at[:, pl.ds(KEPT, BLOCK)], w_ref, sems.at[1])
-    weights.start()
+    weights = [pltpu.make_async_copy(all_hbm.at[:, pl.ds(KEPT, 64)], wm_ref, sems.at[1])]
+    weights += [
+        pltpu.make_async_copy(w, wa_ref.at[(mine + 4 - r) % 4], sems.at[2 + r])
+        for r, w in enumerate((a0, a1, a2, a3))
+    ]
+    for copy in weights:
+        copy.start()
     acc_ref[...] = jnp.zeros_like(acc_ref)
     late_ref[...] = jnp.zeros_like(late_ref)
     hold_ref[...] = jnp.zeros_like(hold_ref)
@@ -358,57 +372,75 @@
     gated = (yin_ref[...] + jnp.concatenate(ys, axis=1)) * gate_ref[...]
     scale = lax.rsqrt(jnp.mean(gated * gated, axis=-1, keepdims=True) + EPS)
     mixed = (gated * scale * gain_ref[...]).astype(BF16)
-    after = (iota((SUB, SUB), 0) > iota((SUB, SUB), 1)).astype(BF16)
-    ones = jnp.ones((SUB, 128), BF16)
+    onward = (iota((2 * SUB, SUB), 0) % SUB > iota((2 * SUB, SUB), 1)).astype(BF16)
+
+    def piece(chunk, masked):
+        move(chunk).wait()
+        for h in range(2):
+            late = late_ref[h]
+            gained = acc_ref[h]
+            query = q_ref[:, h * 128 : (h + 1) * 128]
+            offset = bias[2 * tensor + h] * LOG2E
+            for sub in range(KEYS // SUB - 1, -1, -1):
+                at = chunk * KEYS + sub * SUB
+                first = at // BLOCK
+                key = kv_ref[first : first + 2, :, h * 128 : (h + 1) * 128]
+                value = kv_ref[first : first + 2, :, 256 + h * 128 : 256 + (h + 1) * 128]
+                logits = lax.dot_general(
+                    query, key.reshape(SUB, 128), NT, preferred_element_type=F32
+                )
+                logits = logits * (128 ** -0.5 * LOG2E) + offset
+                soft = jnp.maximum(logits, 0.0) + LOG2E * jnp.log(
+                    1.0 + jnp.exp2(-jnp.abs(logits))
+                )
+                taken = logits - soft
+                if masked:
+                    before = at + iota((BLOCK, SUB), 1) < block * BLOCK + iota((BLOCK, SUB), 0)
+                    soft = jnp.where(before, soft, 0.0)
+                high = soft.astype(BF16)
+                low = (soft - high.astype(F32)).astype(BF16)
+                tail = jnp.dot(
+                    jnp.concatenate([high, low], axis=1), onward, preferred_element_type=F32
+                )
+                later = jnp.concatenate([late] * (SUB // 128), axis=1)
+                weight = jnp.exp2(taken - (tail + later))
+                if masked:
+                    weight = jnp.where(before, weight, 0.0)
+                gained = gained + jnp.dot(
+                    weight.astype(BF16), value.reshape(SUB, 128), preferred_element_type=F32
+                )
+                late = late + jnp.broadcast_to(tail[:, 0:1] + soft[:, 0:1], (BLOCK, 128))
+            late_ref[h] = late
+            acc_ref[h] = gained
+
     for chunk in chunks:
-
-        @pl.when(chunk * per <= block)
-        def _(chunk=chunk):
-            move(chunk).wait()
-            for h in range(2):
-                late = late_ref[h]
-                gained = acc_ref[h]
-                query = q_ref[:, h * 128 : (h + 1) * 128]
-                for sub in range(KEYS // SUB - 1, -1, -1):
-                    at = chunk * KEYS + sub * SUB
-                    first = at // BLOCK
-                    before = at + iota((BLOCK, SUB), 1) < block * BLOCK + iota((BLOCK, SUB), 0)
-                    key = kv_ref[first : first + 2, :, h * 128 : (h + 1) * 128]
-                    value = kv_ref[first : first + 2, :, 256 + h * 128 : 256 + (h + 1) * 128]
-                    logits = lax.dot_general(
-                        query, key.reshape(SUB, 128), NT, preferred_element_type=F32
-                    )
-                    logits = logits * (128 ** -0.5) + bias[2 * tensor + h]
-                    soft = jnp.maximum(logits, 0.0) + jnp.log(1.0 + jnp.exp(-jnp.abs(logits)))
-                    passed = jnp.where(before, -soft, 0.0)
-                    high = passed.astype(BF16)
-                    low = (passed - high.astype(F32)).astype(BF16)
-                    tail = jnp.dot(high, after, preferred_element_type=F32) + jnp.dot(
-                        low, after, preferred_element_type=F32
-                    )
-                    whole = jnp.dot(high, ones, preferred_element_type=F32) + jnp.dot(
-                        low, ones, preferred_element_type=F32
-                    )
-                    later = jnp.concatenate([late] * (SUB // 128), axis=1)
-                    weight = jnp.where(before, jnp.exp(logits - soft + (tail + later)), 0.0)
-                    gained = gained + jnp.dot(
-                        weight.astype(BF16), value.reshape(SUB, 128), preferred_element_type=F32
-                    )
-                    late = late + whole
-                late_ref[h] = late
-                acc_ref[h] = gained
-
-    both = jnp.concatenate([mixed, acc_ref[0].astype(BF16), acc_ref[1].astype(BF16)], axis=1)
-    weights.wait()
+        pl.when(chunk == last)(lambda chunk=chunk: piece(chunk, True))
+        pl.when(chunk < last)(lambda chunk=chunk: piece(chunk, False))
+
+    attended = jnp.concatenate([acc_ref[0].astype(BF16), acc_ref[1].astype(BF16)], axis=1)
+    for copy in weights:
+        copy.wait()
     for s in range(count):
-        out_ref[:, 128 * s : 128 * (s + 1)] = lax.dot_general(
-            both, w_ref[s], NT, preferred_element_type=F32
+        halves = []
+        for f in range(4):
+            for half in range(2):
+                halves.append(
+                    wm_ref[s, 16 * f : 16 * (f + 1), 256 * half : 256 * (half + 1)]
+                )
+        rows_m = jnp.concatenate(halves, axis=0)
+        rows_a = jnp.concatenate(
+            [wa_ref[f, 32 * s : 32 * (s + 1), :] for f in range(4)], axis=0
+        )
+        out_ref[:, 128 * s : 128 * (s + 1)] = (
+            lax.dot_general(mixed, rows_m, NT, preferred_element_type=F32)
+            + lax.dot_general(attended, rows_a, NT, preferred_element_type=F32)
         ).astype(BF16)
 
 
-def attend_call(ids, bias, q, yin, gate, cq, cols, gain, gathered):
+def attend_call(ids, bias, q, yin, gate, cq, cols, gain, gathered, rows):
     full = lambda *shape: pl.BlockSpec(shape, lambda i, ids, bias: (0,) * len(shape))
     count = gathered.shape[0]
+    hbm = pl.BlockSpec(memory_space=pl.ANY)
     return pl.pallas_call(
         attend_kernel,
         grid_spec=pltpu.PrefetchScalarGridSpec(
@@ -417,24 +449,30 @@
             in_specs=[
                 full(BLOCK, 256), full(BLOCK, 256), full(BLOCK, 256), full(BLOCK, 128),
                 full(BLOCK, 8), pl.BlockSpec((1, 256), lambda i, ids, bias: (0, ids[1])),
-                pl.BlockSpec(memory_space=pltpu.HBM),
+                pl.BlockSpec(memory_space=pltpu.HBM), hbm, hbm, hbm, hbm,
             ],
             out_specs=full(BLOCK, 2048),
             scratch_shapes=[
                 pltpu.VMEM((count, BLOCK, 512), BF16),
                 pltpu.VMEM((count, 80, 512), BF16),
-                pltpu.VMEM((count, BLOCK, 512), BF16),
+                pltpu.VMEM((count, 64, 512), BF16),
+                pltpu.VMEM((4, 512, 256), BF16),
                 pltpu.VMEM((2, BLOCK, 128), F32),
                 pltpu.VMEM((2, BLOCK, 128), F32),
                 pltpu.VMEM((64, 512), F32),
-                pltpu.SemaphoreType.DMA((2,)),
+                pltpu.SemaphoreType.DMA((6,)),
                 pltpu.SemaphoreType.DMA((count * BLOCK // KEYS,)),
             ],
         ),
         out_shape=jax.ShapeDtypeStruct((BLOCK, 2048), BF16),
         compiler_params=vmem(),
         name="attend",
-    )(ids, bias, q, yin, gate, cq, cols, gain.reshape(1, -1), gathered)
+    )(ids, bias, q, yin, gate, cq, cols, gain.reshape(1, -1), gathered, *rows)
+
+
+def rotated(shard, axis, by):
+    length = lax.axis_size(axis)
+    return lax.ppermute(shard, axis, [(i, (i + by) % length) for i in range(length)])
 
 
 def body(
@@ -442,27 +480,31 @@
     decay_offset, ssd_gain, w_query, w_key, w_value, stick_bias, out_mixer, out_attend,
 ):
     length = lax.axis_size("sp")
-    ids = jnp.stack([lax.axis_index("sp"), lax.axis_index("tp")]).astype(jnp.int32)
+    ids = jnp.stack([lax.axis_index(name) for name in ("sp", "tp", "fs")]).astype(jnp.int32)
     halo = lax.ppermute(
         inputs[0, BLOCK - HALO :], "sp", [(i, i + 1) for i in range(length - 1)]
     )
     split, step, first, second = prep_call(
         inputs, norm_gain, w_step.T, w_key, w_value, w_input, w_bkey, w_gate, w_cquery, w_query,
-        out_mixer.T, out_attend.T,
+        out_attend.T, out_mixer.T,
     )
     split = halo_call(split, halo, norm_gain)
     tokens = lax.all_to_all(split, "fs", 0, 0, tiled=True)
 
-    def projected(weights):
+    def projected(weights, width):
         whole = lax.all_gather(weights, "sp", axis=0, tiled=True)
-        return lax.all_to_all(project_call(tokens, whole), "fs", 0, 0, tiled=True)
-
+        act, *kept = project_call(tokens, whole, width)
+        return lax.all_to_all(act, "fs", 0, 0, tiled=True), *kept
+
+    (act,) = projected(first, 896)
     send, xin, bkey, srows, scols = local_call(
-        ids, decay_rate, projected(first), step, decay_offset[0].T, conv_weight, tokens
+        ids, decay_rate, act, step, decay_offset[0].T, conv_weight, tokens
     )
     gathered = lax.all_gather(send, "sp", axis=0)
-    yin, gate, cq, q = inner_call(ids, projected(second), conv_weight, xin, bkey, srows, scols)
-    partial = attend_call(ids, stick_bias, q, yin, gate, cq, scols, ssd_gain, gathered)
+    act, kept = projected(second, 640)
+    rows = [kept] + [rotated(kept, "fs", by) for by in (1, 2, 3)]
+    yin, gate, cq, q = inner_call(ids, act, conv_weight, xin, bkey, srows, scols)
+    partial = attend_call(ids, stick_bias, q, yin, gate, cq, scols, ssd_gain, gathered, rows)
     parts = lax.all_to_all(partial.reshape(8, 16, 2048), "tp", 0, 0, tiled=True)
     return jnp.sum(parts.astype(F32), axis=0).astype(BF16)[None]
 

time: 187 us -> 184 us (0.984)
  starting transfers between devices: 12.9 us -> 25.7 us
  waiting for transfers between devices: 55.4 us -> 43.7 us
  blocking collectives: 87.8 us -> 82.6 us
    all_gather x1, waiting for transfers between devices: 45.8 us -> 28.4 us  [body(): gathered = lax.all_gather(send, 'sp', axis=0)]
    all_to_all x1 -> x0, blocking collectives: 10.5 us -> none  [projected(): return lax.all_to_all(project_call(tokens, whole), 'fs', 0, 0, tiled=True)]
    ppermute x0 -> x3, starting transfers between devices: none -> 9.51 us  [rotated(): lax.ppermute(shard, axis, [(i, (i + by) % length) for i in range(length)])]
    ppermute x0 -> x3, waiting for transfers between devices: none -> 5.72 us  [rotated(): lax.ppermute(shard, axis, [(i, (i + by) % length) for i in range(length)])]
    all_gather x2, blocking collectives: 57.7 us -> 60.8 us  [projected(): whole = lax.all_gather(weights, 'sp', axis=0, tiled=True)]
    all_to_all x1 -> x2, starting transfers between devices: 4.4 us -> 7.48 us  [projected(): return (lax.all_to_all(act, 'fs', 0, 0, tiled=True), *kept)]
    all_to_all x1, blocking collectives: 19.6 us -> 21.7 us  [body(): parts = lax.all_to_all(partial.reshape(8, 16, 2048), 'tp', 0, 0, tiled=True)]
    all_to_all x1 -> x2, waiting for transfers between devices: 9.58 us -> 9.58 us  [projected(): return (lax.all_to_all(act, 'fs', 0, 0, tiled=True), *kept)]
  transfers between devices with their start and end apart: 4 -> 8, of which waited for: 2 -> 4; matrix products, arithmetic and copies ran while one was open for 0% -> 0% of each run, Pallas kernels for 2% -> 3%
where the time goes in v4:
time: 184 us
  blocking collectives  82.6 us (45%)
  waiting for transfers between devices  43.7 us (24%)
  starting transfers between devices  25.7 us (14%)
  Pallas kernels  16 us (9%)
  between operations  13.6 us (7%)
    all_gather x2, blocking collectives, projected(): whole = lax.all_gather(weights, 'sp', axis=0, tiled=True)  60.8 us
    all_gather x1, waiting for transfers between devices, body(): gathered = lax.all_gather(send, 'sp', axis=0)  28.4 us
    all_to_all x1, blocking collectives, body(): parts = lax.all_to_all(partial.reshape(8, 16, 2048), 'tp', 0, 0, tiled=True)  21.7 us
    all_to_all x2, waiting for transfers between devices, projected(): return (lax.all_to_all(act, 'fs', 0, 0, tiled=True), *kept)  9.58 us
    ppermute x3, starting transfers between devices, rotated(): lax.ppermute(shard, axis, [(i, (i + by) % length) for i in range(length)])  9.51 us
    all_to_all x2, starting transfers between devices, projected(): return (lax.all_to_all(act, 'fs', 0, 0, tiled=True), *kept)  7.48 us
    ppermute x3, waiting for transfers between devices, rotated(): lax.ppermute(shard, axis, [(i, (i + by) % length) for i in range(length)])  5.72 us
    pallas_call x1, Pallas kernels, attend_call(): pl.pallas_call(attend_kernel, grid_spec=pltpu.PrefetchScalarGridSpec(num_...  4.61 us
  transfers between devices with their start and end apart: 8, of which 4 were waited for; matrix products, arithmetic and copies ran while one was open for 0% of the time, Pallas kernels for 3%

profile of v4, /device:TPU:1, one launch (start us, length us, event | category | flops | bytes accessed | tf_op | source)
XLA Modules:
  0.0 183.8 jit_solution(10265157495887831002)
XLA Ops:
  6.5 0.8 slice_bitcast_fusion
  7.4 4.4 %collective-permute-start = (bf16[16,2048]{1,0:T(8,128)(2,1)S(1)}, bf16[16,2048]{1,0:T(8,128)(2,1)S(1)}, u32[]{:S(2)}, u32[]{:S(2)}) collective-permute-start(bf16[16,2048]{1,0:T(8,128)(2,1)S(1)} %slice_bitcast_fusion), channel_id=1, source_target_pairs={{0,32},{32,64},{64,96},{96,128},{128,160},{160,192},{192,224},{224... | collective-permute-start | bytes 196616 | tf_op jit(solution)/shard_map/ppermute | solution.py:484
  11.7 0.0 copy-start
  11.7 0.0 copy-start.3
  11.8 0.0 copy-start.4
  11.8 2.9 %prep.1 = (bf16[4,160,512]{2,1,0:T(8,128)(2,1)}, f32[32,128]{1,0:T(8,128)}, bf16[32,896]{1,0:T(8,128)(2,1)}, bf16[32,896]{1,0:T(8,128)(2,1)}) custom-call(bf16[1,128,2048]{2,1,0:T(8,128)(2,1)} %refs_0_.1, f32[1,2048]{1,0:T(1,128)} %bitcast.21, bf16[32,2048]{1,0:T(8,128)(2,1)} %bitcast.20, bf16[32,256]{1,0:T(8,128)(2,1)} %refs_3_.1, bf16[32,256]{1,0:T(8,128)(2,1)} %refs_4_.1, ...), custom_call_target="tpu_custom_call" | custom-call | tf_op jit(solution)/shard_map/prep/pallas_call | solution.py:100
  14.7 0.0 collective-permute-done.halo_ref
  14.7 0.0 copy-start.6
  14.8 0.6 copy-done.6
  15.4 1.7 halo.1
  17.1 4.3 %all-to-all-start = ((bf16[4,160,512]{2,1,0:T(8,128)(2,1)}), bf16[4,160,512]{2,1,0:T(8,128)(2,1)S(1)}, u32[]{:S(2)}, u32[]{:S(2)}) async-start(bf16[4,160,512]{2,1,0:T(8,128)(2,1)} %halo.1), calls=%async_computation | async-start | bytes 1310720 | tf_op jit(solution)/shard_map/all_to_all | solution.py:492
  21.4 33.8 %all_gather.13.w_ref = bf16[512,896]{1,0:T(8,128)(2,1)S(1)} all-gather(bf16[32,896]{1,0:T(8,128)(2,1)} %get-tuple-element.23), channel_id=1, replica_groups=mesh['sp'=16,'fs'=4,'tp'=8] {'sp'}, dimensions={0}, use_global_device_ids=true | all-gather | bytes 974848 | tf_op jit(solution)/shard_map/all_gather | solution.py:495
  55.2 0.0 all-to-all-done.x_ref.buf_ref
  55.2 1.8 project.3
  57.0 4.0 %all-to-all-start.2 = ((bf16[4,144,896]{2,1,0:T(8,128)(2,1)}), bf16[4,144,896]{2,1,0:T(8,128)(2,1)S(1)}, u32[]{:S(2)}, u32[]{:S(2)}) async-start(bf16[4,144,896]{2,1,0:T(8,128)(2,1)} %project.3), calls=%async_computation.2 | async-start | bytes 2064384 | tf_op jit(solution)/shard_map/all_to_all | solution.py:497
  61.0 0.1 pad_add_fusion.ids
  61.0 9.6 %all-to-all-done.2.act_ref = bf16[4,144,896]{2,1,0:T(8,128)(2,1)S(1)} async-done(((bf16[4,144,896]{2,1,0:T(8,128)(2,1)}), bf16[4,144,896]{2,1,0:T(8,128)(2,1)S(1)}, u32[]{:S(2)}, u32[]{:S(2)}) %all-to-all-start.2) | async-done | bytes 1032224 | tf_op jit(solution)/shard_map/all_to_all | solution.py:497
  70.6 2.3 %ssd_local.1 = (bf16[272,512]{1,0:T(8,128)(2,1)}, bf16[128,256]{1,0:T(8,128)(2,1)S(1)}, bf16[128,128]{1,0:T(8,128)(2,1)S(1)}, f32[8,128]{1,0:T(8,128)S(1)}, f32[128,8]{1,0:T(8,128)S(1)}) custom-call(s32[3]{0:T(128)S(1)} %pad_add_fusion.ids, f32[32]{0:T(128)S(1)} %copy-done.4, bf16[4,144,896]{2,1,0:T(8,128)(2,1)S(1)} %all-to-all-done.2.act_ref, ...), custom_call_target="tpu_custom_call" | custom-call | tf_op jit(solution)/shard_map/ssd_local/pallas_call | solution.py:237
  72.9 0.0 all-gather.3.cloned.1.call-update
  73.0 27.1 %all_gather.12.w_ref = bf16[512,896]{1,0:T(8,128)(2,1)S(1)} all-gather(bf16[32,896]{1,0:T(8,128)(2,1)S(1)} %copy-done.7), channel_id=1, replica_groups=mesh['sp'=16,'fs'=4,'tp'=8] {'sp'}, dimensions={0}, use_global_device_ids=true | all-gather | bytes 974848 | tf_op jit(solution)/shard_map/all_gather | solution.py:495
  100.1 1.5 project.2
  101.6 3.5 %all-to-all-start.1 = ((bf16[4,144,640]{2,1,0:T(8,128)(2,1)}), bf16[4,144,640]{2,1,0:T(8,128)(2,1)S(1)}, u32[]{:S(2)}, u32[]{:S(2)}) async-start(bf16[4,144,640]{2,1,0:T(8,128)(2,1)} %get-tuple-element.22), calls=%async_computation.1 | async-start | bytes 1474560 | tf_op jit(solution)/shard_map/all_to_all | solution.py:497
  105.1 4.5 %collective-permute-start.3 = (bf16[512,256]{1,0:T(8,128)(2,1)S(1)}, bf16[512,256]{1,0:T(8,128)(2,1)S(1)}, u32[]{:S(2)}, u32[]{:S(2)}) collective-permute-start(bf16[512,256]{1,0:T(8,128)(2,1)S(1)} %get-tuple-element.34.a0), channel_id=1, source_target_pairs={{0,24},{8,0},{16,8},{24,16},{1,25},{9,1},{17,9},{25,17},{2,26},{10... | collective-permute-start | bytes 786440 | tf_op jit(solution)/shard_map/ppermute | solution.py:475
  109.6 2.5 %collective-permute-start.2 = (bf16[512,256]{1,0:T(8,128)(2,1)S(1)}, bf16[512,256]{1,0:T(8,128)(2,1)S(1)}, u32[]{:S(2)}, u32[]{:S(2)}) collective-permute-start(bf16[512,256]{1,0:T(8,128)(2,1)S(1)} %get-tuple-element.34.a0), channel_id=1, source_target_pairs={{0,16},{8,24},{16,0},{24,8},{1,17},{9,25},{17,1},{25,9},{2,18},{10... | collective-permute-start | bytes 786440 | tf_op jit(solution)/shard_map/ppermute | solution.py:475
  112.1 2.5 %collective-permute-start.1 = (bf16[512,256]{1,0:T(8,128)(2,1)S(1)}, bf16[512,256]{1,0:T(8,128)(2,1)S(1)}, u32[]{:S(2)}, u32[]{:S(2)}) collective-permute-start(bf16[512,256]{1,0:T(8,128)(2,1)S(1)} %get-tuple-element.34.a0), channel_id=1, source_target_pairs={{0,8},{8,16},{16,24},{24,0},{1,9},{9,17},{17,25},{25,1},{2,10},{10... | collective-permute-start | bytes 786440 | tf_op jit(solution)/shard_map/ppermute | solution.py:475
  114.6 1.1 ssd_inner.1
  115.8 2.6 %collective-permute-done.2.a2 = bf16[512,256]{1,0:T(8,128)(2,1)S(1)} collective-permute-done((bf16[512,256]{1,0:T(8,128)(2,1)S(1)}, bf16[512,256]{1,0:T(8,128)(2,1)S(1)}, u32[]{:S(2)}, u32[]{:S(2)}) %collective-permute-start.2) | collective-permute-done | bytes 262176 | tf_op jit(solution)/shard_map/ppermute | solution.py:475
  118.3 3.1 %collective-permute-done.1.a1 = bf16[512,256]{1,0:T(8,128)(2,1)S(1)} collective-permute-done((bf16[512,256]{1,0:T(8,128)(2,1)S(1)}, bf16[512,256]{1,0:T(8,128)(2,1)S(1)}, u32[]{:S(2)}, u32[]{:S(2)}) %collective-permute-start.1) | collective-permute-done | bytes 262176 | tf_op jit(solution)/shard_map/ppermute | solution.py:475
  121.5 28.4 %all-gather.3.cloned.1.call-done = bf16[4352,512]{1,0:T(8,128)(2,1)} async-done(((bf16[272,512]{1,0:T(8,128)(2,1)}), bf16[4352,512]{1,0:T(8,128)(2,1)}) %all-gather.3.cloned.1.call-update) | async-done | bytes 4456464 | tf_op jit(solution)/shard_map/all_gather | solution.py:503
  149.9 4.6 %attend.1 = bf16[128,2048]{1,0:T(8,128)(2,1)S(1)} custom-call(s32[3]{0:T(128)S(1)} %pad_add_fusion.ids, f32[16]{0:T(128)S(1)} %copy-done.5, bf16[128,256]{1,0:T(8,128)(2,1)S(1)} %get-tuple-element.29.q_ref, f32[128,256]{1,0:T(8,128)S(1)} %get-tuple-element.30.yin_ref, f32[128,256]{1,0:T(8,128)S(1)} %get-tuple-element.31.gate_ref, ...), custom_call_target="tpu_custom_call" | custom-call | tf_op jit(solution)/shard_map/attend/pallas_call | solution.py:444
  154.5 21.7 %all_to_all.20 = bf16[8,16,2048]{2,1,0:T(8,128)(2,1)S(1)} all-to-all(bf16[8,16,2048]{2,1,0:T(8,128)(2,1)S(1)} %bitcast.16), channel_id=1, replica_groups=mesh['sp'=16,'fs'=4,'tp'=8] {'tp'}, dimensions={0} | all-to-all | bytes 1048576 | tf_op jit(solution)/shard_map/all_to_all | solution.py:508
  176.2 0.7 reduce_sum.12
  (14 shorter events, 0.0 us)
Async XLA Ops:
  7.4 7.4 %collective-permute-start = (bf16[16,2048]{1,0:T(8,128)(2,1)S(1)}, bf16[16,2048]{1,0:T(8,128)(2,1)S(1)}, u32[]{:S(2)}, u32[]{:S(2)}) collective-permute-start(bf16[16,2048]{1,0:T(8,128)(2,1)S(1)} %slice_bitcast_fusion), channel_id=1, source_target_pairs={{0,32},{32,64},{64,96},{96,128},{128,160},{160,192},{192,224},{224... | collective-permute-start | bytes 196616 | tf_op jit(solution)/shard_map/ppermute | solution.py:484
  11.7 58.9 %copy-start = (f32[4,4096]{1,0:T(4,128)S(1)}, f32[4,4096]{1,0:T(4,128)}, u32[]{:S(2)}) copy-start(f32[4,4096]{1,0:T(4,128)} %cc_ref.1) | copy-start | bytes 196612
  11.7 58.9 %copy-start.3 = (f32[1,128,4]{1,2,0:T(4,128)S(1)}, f32[1,128,4]{1,2,0:T(4,128)}, u32[]{:S(2)}) copy-start(f32[1,128,4]{1,2,0:T(4,128)} %param.26) | copy-start | bytes 6148
  11.8 58.9 %copy-start.4 = (f32[32]{0:T(128)S(1)}, f32[32]{0:T(128)}, u32[]{:S(2)}) copy-start(f32[32]{0:T(128)} %rate.1) | copy-start | bytes 388
  14.7 55.9 %copy-start.1 = (f32[32,128]{1,0:T(8,128)S(1)}, f32[32,128]{1,0:T(8,128)}, u32[]{:S(2)}) copy-start(f32[32,128]{1,0:T(8,128)} %get-tuple-element.24.step_ref) | copy-start | bytes 49156
  14.7 0.6 copy-start.6
  17.1 55.9 %copy-start.7 = (bf16[32,896]{1,0:T(8,128)(2,1)S(1)}, bf16[32,896]{1,0:T(8,128)(2,1)}, u32[]{:S(2)}) copy-start(bf16[32,896]{1,0:T(8,128)(2,1)} %get-tuple-element.21) | copy-start | bytes 172036
  17.1 38.1 %all-to-all-start = ((bf16[4,160,512]{2,1,0:T(8,128)(2,1)}), bf16[4,160,512]{2,1,0:T(8,128)(2,1)S(1)}, u32[]{:S(2)}, u32[]{:S(2)}) async-start(bf16[4,160,512]{2,1,0:T(8,128)(2,1)} %halo.1), calls=%async_computation | async-start | bytes 1310720 | tf_op jit(solution)/shard_map/all_to_all | solution.py:492
  57.0 92.9 %copy-start.2 = (f32[2048]{0:T(1024)S(1)}, f32[2048]{0:T(1024)}, u32[]{:S(2)}) copy-start(f32[2048]{0:T(1024)} %param.27) | copy-start | bytes 24580
  57.0 92.9 %copy-start.5 = (f32[16]{0:T(128)S(1)}, f32[16]{0:T(128)}, u32[]{:S(2)}) copy-start(f32[16]{0:T(128)} %bias.1) | copy-start | bytes 196
  57.0 13.6 %all-to-all-start.2 = ((bf16[4,144,896]{2,1,0:T(8,128)(2,1)}), bf16[4,144,896]{2,1,0:T(8,128)(2,1)S(1)}, u32[]{:S(2)}, u32[]{:S(2)}) async-start(bf16[4,144,896]{2,1,0:T(8,128)(2,1)} %project.3), calls=%async_computation.2 | async-start | bytes 2064384 | tf_op jit(solution)/shard_map/all_to_all | solution.py:497
  61.0 88.9 %all-gather.3.cloned.1.call-start = ((), (), s32[]{:S(2)}) async-start(), calls=%async_computation.4 | async-start | bytes 4734976 | tf_op jit(solution)/shard_map/all_gather | solution.py:503
  101.6 13.0 %all-to-all-start.1 = ((bf16[4,144,640]{2,1,0:T(8,128)(2,1)}), bf16[4,144,640]{2,1,0:T(8,128)(2,1)S(1)}, u32[]{:S(2)}, u32[]{:S(2)}) async-start(bf16[4,144,640]{2,1,0:T(8,128)(2,1)} %get-tuple-element.22), calls=%async_computation.1 | async-start | bytes 1474560 | tf_op jit(solution)/shard_map/all_to_all | solution.py:497
  105.1 10.6 %collective-permute-start.3 = (bf16[512,256]{1,0:T(8,128)(2,1)S(1)}, bf16[512,256]{1,0:T(8,128)(2,1)S(1)}, u32[]{:S(2)}, u32[]{:S(2)}) collective-permute-start(bf16[512,256]{1,0:T(8,128)(2,1)S(1)} %get-tuple-element.34.a0), channel_id=1, source_target_pairs={{0,24},{8,0},{16,8},{24,16},{1,25},{9,1},{17,9},{25,17},{2,26},{10... | collective-permute-start | bytes 786440 | tf_op jit(solution)/shard_map/ppermute | solution.py:475
  109.6 8.7 %collective-permute-start.2 = (bf16[512,256]{1,0:T(8,128)(2,1)S(1)}, bf16[512,256]{1,0:T(8,128)(2,1)S(1)}, u32[]{:S(2)}, u32[]{:S(2)}) collective-permute-start(bf16[512,256]{1,0:T(8,128)(2,1)S(1)} %get-tuple-element.34.a0), channel_id=1, source_target_pairs={{0,16},{8,24},{16,0},{24,8},{1,17},{9,25},{17,1},{25,9},{2,18},{10... | collective-permute-start | bytes 786440 | tf_op jit(solution)/shard_map/ppermute | solution.py:475
  112.1 9.3 %collective-permute-start.1 = (bf16[512,256]{1,0:T(8,128)(2,1)S(1)}, bf16[512,256]{1,0:T(8,128)(2,1)S(1)}, u32[]{:S(2)}, u32[]{:S(2)}) collective-permute-start(bf16[512,256]{1,0:T(8,128)(2,1)S(1)} %get-tuple-element.34.a0), channel_id=1, source_target_pairs={{0,8},{8,16},{16,24},{24,0},{1,9},{9,17},{17,25},{25,1},{2,10},{10... | collective-permute-start | bytes 786440 | tf_op jit(solution)/shard_map/ppermute | solution.py:475
Sparse Core Ops, SparseCore 0:
  73.1 76.7 all-gather.2

commit v5 on v4

--- a/solution.py
+++ b/solution.py
@@ -83,12 +83,12 @@
     wide = normed.astype(F32)
     for f in range(4):
         for g in range(4):
-            xs_ref[f, HALO:ROWS, g * 128 : (g + 1) * 128] = shuffled(wide, f, g)
+            xs_ref[f, 0:BLOCK, g * 128 : (g + 1) * 128] = shuffled(wide, f, g)
     for copy in later:
         copy.wait()
     for f in range(4):
-        xs_ref[f, ROWS:, 0:256] = third_ref[0:16, :]
-        xs_ref[f, ROWS:, 256:512] = third_ref[16:32, :]
+        xs_ref[f, BLOCK:, 0:256] = third_ref[0:16, :]
+        xs_ref[f, BLOCK:, 256:512] = third_ref[16:32, :]
 
 
 def prep_call(inputs, gain, w_step_t, *arrays):
@@ -101,7 +101,7 @@
         prep_kernel,
         in_specs=[hbm] * 12,
         out_shape=(
-            jax.ShapeDtypeStruct((4, ROWS + HALO, width // 4), BF16),
+            jax.ShapeDtypeStruct((4, rows + HALO, width // 4), BF16),
             jax.ShapeDtypeStruct((heads, rows), F32),
             jax.ShapeDtypeStruct((part, widths[0]), BF16),
             jax.ShapeDtypeStruct((part, widths[1]), BF16),
@@ -118,50 +118,38 @@
     )(inputs, gain.reshape(1, -1), w_step_t, *arrays)
 
 
-def halo_kernel(xs_in, halo_ref, gain_ref, xs_out, rim_ref, sem):
-    wide = normalised(halo_ref[...], gain_ref[...]).astype(F32)
+def project_kernel(x_ref, rim_ref, w_ref, out_hbm, *rest):
+    kept, (out_ref, sems) = rest[:-2], rest[-2:]
+    width = out_hbm.shape[2]
+    weights = w_ref[:, 0:width]
+    copies = []
     for f in range(4):
-        for g in range(4):
-            rim_ref[f, :, g * 128 : (g + 1) * 128] = shuffled(wide, f, g)
-    copy = pltpu.make_async_copy(rim_ref, xs_out.at[:, pl.ds(0, HALO)], sem)
-    copy.start()
-    copy.wait()
-
-
-def halo_call(xs, halo, gain):
-    anywhere = pl.BlockSpec(memory_space=pl.ANY)
-    whole = pl.BlockSpec(memory_space=pltpu.VMEM)
-    return pl.pallas_call(
-        halo_kernel,
-        in_specs=[anywhere, whole, whole],
-        out_specs=anywhere,
-        out_shape=jax.ShapeDtypeStruct(xs.shape, BF16),
-        input_output_aliases={0: 0},
-        scratch_shapes=[pltpu.VMEM((4, HALO, xs.shape[2]), BF16), pltpu.SemaphoreType.DMA],
-        name="halo",
-    )(xs, halo, gain.reshape(1, -1))
-
-
-def project_kernel(x_ref, w_ref, out_ref, *kept):
-    width = out_ref.shape[2]
-    for f in range(4):
-        out_ref[f] = jnp.dot(
-            x_ref[f, 0:ROWS, :], w_ref[:, 0:width], preferred_element_type=F32
-        ).astype(BF16)
+        rows = jnp.concatenate([rim_ref[f], x_ref[f, 0:BLOCK, :]], axis=0)
+        out_ref[f] = jnp.dot(rows, weights, preferred_element_type=F32).astype(BF16)
+        copies.append(pltpu.make_async_copy(out_ref.at[f], out_hbm.at[f], sems.at[f]))
+        copies[-1].start()
     for ref in kept:
         ref[...] = w_ref[:, width:]
-
-
-def project_call(x, w, width):
+    for copy in copies:
+        copy.wait()
+
+
+def project_call(x, rim, w, width):
+    whole = pl.BlockSpec(memory_space=pltpu.VMEM)
     outs = [jax.ShapeDtypeStruct((4, ROWS, width), BF16)]
+    specs = [pl.BlockSpec(memory_space=pltpu.HBM)]
     if w.shape[1] > width:
         outs.append(jax.ShapeDtypeStruct((w.shape[0], w.shape[1] - width), BF16))
+        specs.append(whole)
     return pl.pallas_call(
         project_kernel,
+        in_specs=[whole] * 3,
+        out_specs=specs,
         out_shape=outs,
+        scratch_shapes=[pltpu.VMEM((4, ROWS, width), BF16), pltpu.SemaphoreType.DMA((4,))],
         compiler_params=vmem(),
         name="project",
-    )(x, w)
+    )(x, rim, w)
 
 
 def added(ref, at, width):
@@ -187,7 +175,7 @@
     tensor = ids[1]
     moved = pull(
         [
-            (buf_ref.at[f, pl.ds(ROWS, HALO)], send_ref.at[pl.ds(KEPT + HALO * f, HALO)])
+            (buf_ref.at[f, pl.ds(BLOCK, HALO)], send_ref.at[pl.ds(KEPT + HALO * f, HALO)])
             for f in range(4)
         ],
         sems,
@@ -335,47 +323,22 @@
         )
 
     states = pltpu.make_async_copy(all_hbm.at[:, pl.ds(BLOCK, 80)], st_ref, sems.at[0])
-    states.start()
-    for chunk in chunks:
-
-        @pl.when(chunk <= last)
-        def _(chunk=chunk):
-            move(chunk).start()
-
     weights = [pltpu.make_async_copy(all_hbm.at[:, pl.ds(KEPT, 64)], wm_ref, sems.at[1])]
     weights += [
         pltpu.make_async_copy(w, wa_ref.at[(mine + 4 - r) % 4], sems.at[2 + r])
         for r, w in enumerate((a0, a1, a2, a3))
     ]
-    for copy in weights:
-        copy.start()
+    for chunk in chunks:
+        pl.when((chunk <= last) & (chunk >= last - 1))(lambda chunk=chunk: move(chunk).start())
     acc_ref[...] = jnp.zeros_like(acc_ref)
     late_ref[...] = jnp.zeros_like(late_ref)
     hold_ref[...] = jnp.zeros_like(hold_ref)
-    states.wait()
-
-    def advance(k, carry):
-        logs = st_ref[k, 64:80, :].astype(F32)
-        decay = jnp.exp(logs[0:8] + logs[8:16])
-        hold_ref[...] = hold_ref[...] * jnp.concatenate([decay] * 8, axis=0) + st_ref[
-            k, 0:64, :
-        ].astype(F32)
-        return carry
-
-    lax.fori_loop(0, block, advance, 0)
-    cquery = cq_ref[...]
-    ys = []
-    for h in range(4):
-        enter = hold_ref[:, h * 128 : (h + 1) * 128].astype(BF16)
-        moved = lax.dot_general(cquery, enter, NT, preferred_element_type=F32)
-        ys.append(moved * jnp.exp(cols_ref[:, h : h + 1]))
-    gated = (yin_ref[...] + jnp.concatenate(ys, axis=1)) * gate_ref[...]
-    scale = lax.rsqrt(jnp.mean(gated * gated, axis=-1, keepdims=True) + EPS)
-    mixed = (gated * scale * gain_ref[...]).astype(BF16)
     onward = (iota((2 * SUB, SUB), 0) % SUB > iota((2 * SUB, SUB), 1)).astype(BF16)
 
     def piece(chunk, masked):
         move(chunk).wait()
+        if chunk > 1:
+            move(chunk - 2).start()
         for h in range(2):
             late = late_ref[h]
             gained = acc_ref[h]
@@ -414,9 +377,33 @@
             acc_ref[h] = gained
 
     for chunk in chunks:
+        if chunk == 1:
+            states.start()
+            for copy in weights:
+                copy.start()
         pl.when(chunk == last)(lambda chunk=chunk: piece(chunk, True))
         pl.when(chunk < last)(lambda chunk=chunk: piece(chunk, False))
 
+    states.wait()
+
+    def advance(k, carry):
+        logs = st_ref[k, 64:80, :].astype(F32)
+        decay = jnp.exp(logs[0:8] + logs[8:16])
+        hold_ref[...] = hold_ref[...] * jnp.concatenate([decay] * 8, axis=0) + st_ref[
+            k, 0:64, :
+        ].astype(F32)
+        return carry
+
+    lax.fori_loop(0, block, advance, 0)
+    cquery = cq_ref[...]
+    ys = []
+    for h in range(4):
+        enter = hold_ref[:, h * 128 : (h + 1) * 128].astype(BF16)
+        moved = lax.dot_general(cquery, enter, NT, preferred_element_type=F32)
+        ys.append(moved * jnp.exp(cols_ref[:, h : h + 1]))
+    gated = (yin_ref[...] + jnp.concatenate(ys, axis=1)) * gate_ref[...]
+    scale = lax.rsqrt(jnp.mean(gated * gated, axis=-1, keepdims=True) + EPS)
+    mixed = (gated * scale * gain_ref[...]).astype(BF16)
     attended = jnp.concatenate([acc_ref[0].astype(BF16), acc_ref[1].astype(BF16)], axis=1)
     for copy in weights:
         copy.wait()
@@ -481,27 +468,27 @@
 ):
     length = lax.axis_size("sp")
     ids = jnp.stack([lax.axis_index(name) for name in ("sp", "tp", "fs")]).astype(jnp.int32)
-    halo = lax.ppermute(
-        inputs[0, BLOCK - HALO :], "sp", [(i, i + 1) for i in range(length - 1)]
-    )
     split, step, first, second = prep_call(
         inputs, norm_gain, w_step.T, w_key, w_value, w_input, w_bkey, w_gate, w_cquery, w_query,
         out_attend.T, out_mixer.T,
     )
-    split = halo_call(split, halo, norm_gain)
     tokens = lax.all_to_all(split, "fs", 0, 0, tiled=True)
-
-    def projected(weights, width):
-        whole = lax.all_gather(weights, "sp", axis=0, tiled=True)
-        act, *kept = project_call(tokens, whole, width)
+    early = lax.all_gather(first, "sp", axis=0, tiled=True)
+    tokens, early = lax.optimization_barrier((tokens, early))
+    rim = lax.ppermute(
+        tokens[:, BLOCK - HALO : BLOCK], "sp", [(i, i + 1) for i in range(length - 1)]
+    )
+
+    def projected(whole, width):
+        act, *kept = project_call(tokens, rim, whole, width)
         return lax.all_to_all(act, "fs", 0, 0, tiled=True), *kept
 
-    (act,) = projected(first, 896)
+    (act,) = projected(early, 896)
     send, xin, bkey, srows, scols = local_call(
         ids, decay_rate, act, step, decay_offset[0].T, conv_weight, tokens
     )
     gathered = lax.all_gather(send, "sp", axis=0)
-    act, kept = projected(second, 640)
+    act, kept = projected(lax.all_gather(second, "sp", axis=0, tiled=True), 640)
     rows = [kept] + [rotated(kept, "fs", by) for by in (1, 2, 3)]
     yin, gate, cq, q = inner_call(ids, act, conv_weight, xin, bkey, srows, scols)
     partial = attend_call(ids, stick_bias, q, yin, gate, cq, scols, ssd_gain, gathered, rows)

time: 184 us -> 183 us (level)
  waiting for transfers between devices: 43.7 us -> 46.7 us
  Pallas kernels: 16 us -> 13.5 us
    all_gather x1, waiting for transfers between devices: 28.4 us -> 32.5 us  [body(): gathered = lax.all_gather(send, 'sp', axis=0)]
    ppermute x1, starting transfers between devices: 4.35 us -> 1.7 us  [body(): lax.ppermute(tokens[:, BLOCK - HALO:BLOCK], 'sp', [(i, i + 1) for i in ra...]
    ppermute x3, waiting for transfers between devices: 5.72 us -> 3.3 us  [rotated(): lax.ppermute(shard, axis, [(i, (i + by) % length) for i in range(length)])]
    pallas_call x3 -> x2, Pallas kernels: 5.02 us -> 2.88 us  [project_call(): pl.pallas_call(project_kernel, in_specs=[whole] * 3, out_specs=specs, out...]
  transfers between devices with their start and end apart: 8 -> 8, of which waited for: 4 -> 5; matrix products, arithmetic and copies ran while one was open for 0% -> 0% of each run, Pallas kernels for 3% -> 1%
where the time goes in v5:
time: 183 us
  blocking collectives  82.6 us (45%)
  waiting for transfers between devices  46.7 us (26%)
  starting transfers between devices  25.6 us (14%)
  between operations  13.6 us (7%)
  Pallas kernels  13.5 us (7%)
    all_gather x1, blocking collectives, body(): early = lax.all_gather(first, 'sp', axis=0, tiled=True)  34.2 us
    all_gather x1, waiting for transfers between devices, body(): gathered = lax.all_gather(send, 'sp', axis=0)  32.5 us
    all_gather x1, blocking collectives, body(): act, kept = projected(lax.all_gather(second, 'sp', axis=0, tiled=True), 640)  27.7 us
    all_to_all x1, blocking collectives, body(): parts = lax.all_to_all(partial.reshape(8, 16, 2048), 'tp', 0, 0, tiled=True)  20.6 us
    ppermute x3, starting transfers between devices, rotated(): lax.ppermute(shard, axis, [(i, (i + by) % length) for i in range(length)])  10.7 us
    all_to_all x2, waiting for transfers between devices, projected(): return (lax.all_to_all(act, 'fs', 0, 0, tiled=True), *kept)  9.58 us
    all_to_all x2, starting transfers between devices, projected(): return (lax.all_to_all(act, 'fs', 0, 0, tiled=True), *kept)  8.03 us
    all_to_all x1, starting transfers between devices, body(): tokens = lax.all_to_all(split, 'fs', 0, 0, tiled=True)  5.14 us
  transfers between devices with their start and end apart: 8, of which 5 were waited for; matrix products, arithmetic and copies ran while one was open for 0% of the time, Pallas kernels for 1%

profile of v5, /device:TPU:1, one launch (start us, length us, event | category | flops | bytes accessed | tf_op | source)
XLA Modules:
  0.0 182.7 jit_solution(7085314830483610119)
XLA Ops:
  6.5 2.9 %prep.1 = (bf16[4,144,512]{2,1,0:T(8,128)(2,1)}, f32[32,128]{1,0:T(8,128)}, bf16[32,896]{1,0:T(8,128)(2,1)}, bf16[32,896]{1,0:T(8,128)(2,1)}) custom-call(bf16[1,128,2048]{2,1,0:T(8,128)(2,1)} %refs_0_.1, f32[1,2048]{1,0:T(1,128)} %bitcast.21, bf16[32,2048]{1,0:T(8,128)(2,1)} %bitcast.18, bf16[32,256]{1,0:T(8,128)(2,1)} %refs_3_.1, bf16[32,256]{1,0:T(8,128)(2,1)} %refs_4_.1, ...), custom_call_target="tpu_custom_call" | custom-call | tf_op jit(solution)/shard_map/prep/pallas_call | solution.py:100
  9.4 0.0 copy-start.1
  9.4 0.0 copy-start.6
  9.5 5.1 %all-to-all-start = ((bf16[4,144,512]{2,1,0:T(8,128)(2,1)}), bf16[4,144,512]{2,1,0:T(8,128)(2,1)S(1)}, u32[]{:S(2)}, u32[]{:S(2)}) async-start(bf16[4,144,512]{2,1,0:T(8,128)(2,1)} %get-tuple-element.22), calls=%async_computation | async-start | bytes 1179648 | tf_op jit(solution)/shard_map/all_to_all | solution.py:475
  14.6 34.2 %all_gather.12.w_ref = bf16[512,896]{1,0:T(8,128)(2,1)S(1)} all-gather(bf16[32,896]{1,0:T(8,128)(2,1)} %get-tuple-element.23), channel_id=1, replica_groups=mesh['sp'=16,'fs'=4,'tp'=8] {'sp'}, dimensions={0}, use_global_device_ids=true | all-gather | bytes 974848 | tf_op jit(solution)/shard_map/all_gather | solution.py:476
  48.8 0.0 all-to-all-done.x_ref.buf_ref
  48.8 1.7 collective-permute-start
  50.6 1.3 collective-permute-done.rim_ref
  51.9 1.5 project.3
  53.4 0.0 copy-start.2
  53.4 0.0 copy-start.5
  53.4 4.5 %all-to-all-start.2 = ((bf16[4,144,896]{2,1,0:T(8,128)(2,1)}), bf16[4,144,896]{2,1,0:T(8,128)(2,1)S(1)}, u32[]{:S(2)}, u32[]{:S(2)}) async-start(bf16[4,144,896]{2,1,0:T(8,128)(2,1)} %project.3), calls=%async_computation.2 | async-start | bytes 2064384 | tf_op jit(solution)/shard_map/all_to_all | solution.py:484
  58.0 0.1 pad_add_fusion.ids
  58.0 9.6 %all-to-all-done.2.act_ref = bf16[4,144,896]{2,1,0:T(8,128)(2,1)S(1)} async-done(((bf16[4,144,896]{2,1,0:T(8,128)(2,1)}), bf16[4,144,896]{2,1,0:T(8,128)(2,1)S(1)}, u32[]{:S(2)}, u32[]{:S(2)}) %all-to-all-start.2) | async-done | bytes 1032224 | tf_op jit(solution)/shard_map/all_to_all | solution.py:484
  67.6 0.0 copy-done
  67.6 2.3 %ssd_local.1 = (bf16[272,512]{1,0:T(8,128)(2,1)}, bf16[128,256]{1,0:T(8,128)(2,1)S(1)}, bf16[128,128]{1,0:T(8,128)(2,1)S(1)}, f32[8,128]{1,0:T(8,128)S(1)}, f32[128,8]{1,0:T(8,128)S(1)}) custom-call(s32[3]{0:T(128)S(1)} %pad_add_fusion.ids, f32[32]{0:T(128)S(1)} %copy-done.4, bf16[4,144,896]{2,1,0:T(8,128)(2,1)S(1)} %all-to-all-done.2.act_ref, ...), custom_call_target="tpu_custom_call" | custom-call | tf_op jit(solution)/shard_map/ssd_local/pallas_call | solution.py:225
  69.9 0.0 all-gather.3.cloned.1.call-update
  70.0 27.7 %all_gather.13.w_ref = bf16[512,896]{1,0:T(8,128)(2,1)S(1)} all-gather(bf16[32,896]{1,0:T(8,128)(2,1)S(1)} %copy-done.6), channel_id=1, replica_groups=mesh['sp'=16,'fs'=4,'tp'=8] {'sp'}, dimensions={0}, use_global_device_ids=true | all-gather | bytes 974848 | tf_op jit(solution)/shard_map/all_gather | solution.py:491
  97.7 1.4 project.2
  99.1 3.5 %all-to-all-start.1 = ((bf16[4,144,640]{2,1,0:T(8,128)(2,1)}), bf16[4,144,640]{2,1,0:T(8,128)(2,1)S(1)}, u32[]{:S(2)}, u32[]{:S(2)}) async-start(bf16[4,144,640]{2,1,0:T(8,128)(2,1)} %get-tuple-element.26), calls=%async_computation.1 | async-start | bytes 1474560 | tf_op jit(solution)/shard_map/all_to_all | solution.py:484
  102.6 3.3 %collective-permute-start.1 = (bf16[512,256]{1,0:T(8,128)(2,1)S(1)}, bf16[512,256]{1,0:T(8,128)(2,1)S(1)}, u32[]{:S(2)}, u32[]{:S(2)}) collective-permute-start(bf16[512,256]{1,0:T(8,128)(2,1)S(1)} %get-tuple-element.38.a0), channel_id=1, source_target_pairs={{0,8},{8,16},{16,24},{24,0},{1,9},{9,17},{17,25},{25,1},{2,10},{10... | collective-permute-start | bytes 786440 | tf_op jit(solution)/shard_map/ppermute | solution.py:462
  105.9 4.3 %collective-permute-start.2 = (bf16[512,256]{1,0:T(8,128)(2,1)S(1)}, bf16[512,256]{1,0:T(8,128)(2,1)S(1)}, u32[]{:S(2)}, u32[]{:S(2)}) collective-permute-start(bf16[512,256]{1,0:T(8,128)(2,1)S(1)} %get-tuple-element.38.a0), channel_id=1, source_target_pairs={{0,16},{8,24},{16,0},{24,8},{1,17},{9,25},{17,1},{25,9},{2,18},{10... | collective-permute-start | bytes 786440 | tf_op jit(solution)/shard_map/ppermute | solution.py:462
  110.2 3.1 %collective-permute-start.3 = (bf16[512,256]{1,0:T(8,128)(2,1)S(1)}, bf16[512,256]{1,0:T(8,128)(2,1)S(1)}, u32[]{:S(2)}, u32[]{:S(2)}) collective-permute-start(bf16[512,256]{1,0:T(8,128)(2,1)S(1)} %get-tuple-element.38.a0), channel_id=1, source_target_pairs={{0,24},{8,0},{16,8},{24,16},{1,25},{9,1},{17,9},{25,17},{2,26},{10... | collective-permute-start | bytes 786440 | tf_op jit(solution)/shard_map/ppermute | solution.py:462
  113.3 0.0 all-to-all-done.1.act_ref
  113.3 1.1 ssd_inner.1
  114.5 0.0 collective-permute-done.1.a1
  114.5 1.9 %collective-permute-done.2.a2 = bf16[512,256]{1,0:T(8,128)(2,1)S(1)} collective-permute-done((bf16[512,256]{1,0:T(8,128)(2,1)S(1)}, bf16[512,256]{1,0:T(8,128)(2,1)S(1)}, u32[]{:S(2)}, u32[]{:S(2)}) %collective-permute-start.2) | collective-permute-done | bytes 262176 | tf_op jit(solution)/shard_map/ppermute | solution.py:462
  116.4 1.4 collective-permute-done.3.a3
  117.8 32.5 %all-gather.3.cloned.1.call-done = bf16[4352,512]{1,0:T(8,128)(2,1)} async-done(((bf16[272,512]{1,0:T(8,128)(2,1)}), bf16[4352,512]{1,0:T(8,128)(2,1)}) %all-gather.3.cloned.1.call-update) | async-done | bytes 4456464 | tf_op jit(solution)/shard_map/all_gather | solution.py:490
  150.2 4.3 %attend.1 = bf16[128,2048]{1,0:T(8,128)(2,1)S(1)} custom-call(s32[3]{0:T(128)S(1)} %pad_add_fusion.ids, f32[16]{0:T(128)S(1)} %copy-done.5, bf16[128,256]{1,0:T(8,128)(2,1)S(1)} %get-tuple-element.33.q_ref, f32[128,256]{1,0:T(8,128)S(1)} %get-tuple-element.34.yin_ref, f32[128,256]{1,0:T(8,128)S(1)} %get-tuple-element.35.gate_ref, ...), custom_call_target="tpu_custom_call" | custom-call | tf_op jit(solution)/shard_map/attend/pallas_call | solution.py:431
  154.6 20.6 %all_to_all.20 = bf16[8,16,2048]{2,1,0:T(8,128)(2,1)S(1)} all-to-all(bf16[8,16,2048]{2,1,0:T(8,128)(2,1)S(1)} %bitcast.14), channel_id=1, replica_groups=mesh['sp'=16,'fs'=4,'tp'=8] {'tp'}, dimensions={0} | all-to-all | bytes 1048576 | tf_op jit(solution)/shard_map/all_to_all | solution.py:495
  175.2 0.7 reduce_sum.12
  (11 shorter events, 0.0 us)
Async XLA Ops:
  6.5 61.1 %copy-start.3 = (f32[1,128,4]{1,2,0:T(4,128)S(1)}, f32[1,128,4]{1,2,0:T(4,128)}, u32[]{:S(2)}) copy-start(f32[1,128,4]{1,2,0:T(4,128)} %param.26) | copy-start | bytes 6148
  6.5 61.1 %copy-start = (f32[4,4096]{1,0:T(4,128)S(1)}, f32[4,4096]{1,0:T(4,128)}, u32[]{:S(2)}) copy-start(f32[4,4096]{1,0:T(4,128)} %cc_ref.1) | copy-start | bytes 196612
  6.5 61.1 %copy-start.4 = (f32[32]{0:T(128)S(1)}, f32[32]{0:T(128)}, u32[]{:S(2)}) copy-start(f32[32]{0:T(128)} %rate.1) | copy-start | bytes 388
  9.4 58.2 %copy-start.1 = (f32[32,128]{1,0:T(8,128)S(1)}, f32[32,128]{1,0:T(8,128)}, u32[]{:S(2)}) copy-start(f32[32,128]{1,0:T(8,128)} %get-tuple-element.28.step_ref) | copy-start | bytes 49156
  9.4 60.5 %copy-start.6 = (bf16[32,896]{1,0:T(8,128)(2,1)S(1)}, bf16[32,896]{1,0:T(8,128)(2,1)}, u32[]{:S(2)}) copy-start(bf16[32,896]{1,0:T(8,128)(2,1)} %get-tuple-element.25) | copy-start | bytes 172036
  9.5 39.4 %all-to-all-start = ((bf16[4,144,512]{2,1,0:T(8,128)(2,1)}), bf16[4,144,512]{2,1,0:T(8,128)(2,1)S(1)}, u32[]{:S(2)}, u32[]{:S(2)}) async-start(bf16[4,144,512]{2,1,0:T(8,128)(2,1)} %get-tuple-element.22), calls=%async_computation | async-start | bytes 1179648 | tf_op jit(solution)/shard_map/all_to_all | solution.py:475
  48.8 3.0 %collective-permute-start = (bf16[4,16,512]{2,1,0:T(8,128)(2,1)S(1)}, bf16[4,16,512]{2,1,0:T(8,128)(2,1)S(1)}, u32[]{:S(2)}, u32[]{:S(2)}) collective-permute-start(bf16[4,16,512]{2,1,0:T(8,128)(2,1)S(1)} %slice.3), channel_id=1, source_target_pairs={{0,32},{32,64},{64,96},{96,128},{128,160},{160,192},{192,224},{224... | collective-permute-start | bytes 196616 | tf_op jit(solution)/shard_map/ppermute | solution.py:478
  53.4 96.8 %copy-start.2 = (f32[2048]{0:T(1024)S(1)}, f32[2048]{0:T(1024)}, u32[]{:S(2)}) copy-start(f32[2048]{0:T(1024)} %param.27) | copy-start | bytes 24580
  53.4 96.8 %copy-start.5 = (f32[16]{0:T(128)S(1)}, f32[16]{0:T(128)}, u32[]{:S(2)}) copy-start(f32[16]{0:T(128)} %bias.1) | copy-start | bytes 196
  53.4 14.2 %all-to-all-start.2 = ((bf16[4,144,896]{2,1,0:T(8,128)(2,1)}), bf16[4,144,896]{2,1,0:T(8,128)(2,1)S(1)}, u32[]{:S(2)}, u32[]{:S(2)}) async-start(bf16[4,144,896]{2,1,0:T(8,128)(2,1)} %project.3), calls=%async_computation.2 | async-start | bytes 2064384 | tf_op jit(solution)/shard_map/all_to_all | solution.py:484
  58.0 92.3 %all-gather.3.cloned.1.call-start = ((), (), s32[]{:S(2)}) async-start(), calls=%async_computation.4 | async-start | bytes 4734976 | tf_op jit(solution)/shard_map/all_gather | solution.py:490
  99.1 14.3 %all-to-all-start.1 = ((bf16[4,144,640]{2,1,0:T(8,128)(2,1)}), bf16[4,144,640]{2,1,0:T(8,128)(2,1)S(1)}, u32[]{:S(2)}, u32[]{:S(2)}) async-start(bf16[4,144,640]{2,1,0:T(8,128)(2,1)} %get-tuple-element.26), calls=%async_computation.1 | async-start | bytes 1474560 | tf_op jit(solution)/shard_map/all_to_all | solution.py:484
  102.6 11.9 %collective-permute-start.1 = (bf16[512,256]{1,0:T(8,128)(2,1)S(1)}, bf16[512,256]{1,0:T(8,128)(2,1)S(1)}, u32[]{:S(2)}, u32[]{:S(2)}) collective-permute-start(bf16[512,256]{1,0:T(8,128)(2,1)S(1)} %get-tuple-element.38.a0), channel_id=1, source_target_pairs={{0,8},{8,16},{16,24},{24,0},{1,9},{9,17},{17,25},{25,1},{2,10},{10... | collective-permute-start | bytes 786440 | tf_op jit(solution)/shard_map/ppermute | solution.py:462
  105.9 10.4 %collective-permute-start.2 = (bf16[512,256]{1,0:T(8,128)(2,1)S(1)}, bf16[512,256]{1,0:T(8,128)(2,1)S(1)}, u32[]{:S(2)}, u32[]{:S(2)}) collective-permute-start(bf16[512,256]{1,0:T(8,128)(2,1)S(1)} %get-tuple-element.38.a0), channel_id=1, source_target_pairs={{0,16},{8,24},{16,0},{24,8},{1,17},{9,25},{17,1},{25,9},{2,18},{10... | collective-permute-start | bytes 786440 | tf_op jit(solution)/shard_map/ppermute | solution.py:462
  110.2 7.5 %collective-permute-start.3 = (bf16[512,256]{1,0:T(8,128)(2,1)S(1)}, bf16[512,256]{1,0:T(8,128)(2,1)S(1)}, u32[]{:S(2)}, u32[]{:S(2)}) collective-permute-start(bf16[512,256]{1,0:T(8,128)(2,1)S(1)} %get-tuple-element.38.a0), channel_id=1, source_target_pairs={{0,24},{8,0},{16,8},{24,16},{1,25},{9,1},{17,9},{25,17},{2,26},{10... | collective-permute-start | bytes 786440 | tf_op jit(solution)/shard_map/ppermute | solution.py:462
Sparse Core Ops, SparseCore 0:
  70.1 80.0 all-gather.2

commit v6 on v5

--- a/solution.py
+++ b/solution.py
@@ -45,10 +45,7 @@
     out = None
     for k in range(4):
         at = (4 * g + k) * 128
-        piece = normed[:, at : at + 128]
-        shift = ((k - f) * 32) % 128
-        if shift:
-            piece = pltpu.roll(piece, shift, 1)
+        piece = pltpu.roll(normed[:, at : at + 128], (k + 4 - f) * 32 % 128, 1)
         out = piece if out is None else jnp.where(lane == k, piece, out)
     return out.astype(BF16)
 
@@ -63,7 +60,7 @@
     x_hbm, gain_hbm, ws_hbm = refs[:3]
     sources = refs[3:12]
     xs_ref, step_ref, first_ref, second_ref = refs[12:16]
-    x_ref, gain_ref, ws_ref, third_ref, sems, wsems = refs[16:]
+    x_ref, gain_ref, ws_ref, third_ref, wide_ref, sems, wsems = refs[16:]
     early = pull(((x_hbm.at[0], x_ref), (gain_hbm, gain_ref), (ws_hbm, ws_ref)), sems)
     pairs = []
     outs = (first_ref, second_ref, third_ref)
@@ -81,9 +78,14 @@
         lax.dot_general(ws_ref[...], normed, NT, preferred_element_type=F32)
     )
     wide = normed.astype(F32)
-    for f in range(4):
+    wide_ref[...] = wide
+
+    def each(f, carry):
         for g in range(4):
-            xs_ref[f, 0:BLOCK, g * 128 : (g + 1) * 128] = shuffled(wide, f, g)
+            xs_ref[f, 0:BLOCK, g * 128 : (g + 1) * 128] = shuffled(wide_ref, f, g)
+        return carry
+
+    lax.fori_loop(0, 4, each, 0)
     for copy in later:
         copy.wait()
     for f in range(4):
@@ -111,6 +113,7 @@
             pltpu.VMEM((1, width), F32),
             pltpu.VMEM((heads, width), BF16),
             pltpu.VMEM((part, widths[2]), BF16),
+            pltpu.VMEM((rows, width), F32),
             pltpu.SemaphoreType.DMA((3,)),
             pltpu.SemaphoreType.DMA((9,)),
         ],
@@ -122,16 +125,21 @@
     kept, (out_ref, sems) = rest[:-2], rest[-2:]
     width = out_hbm.shape[2]
     weights = w_ref[:, 0:width]
-    copies = []
-    for f in range(4):
+
+    def copy(f):
+        return pltpu.make_async_copy(out_ref.at[f], out_hbm.at[f], sems.at[f])
+
+    def each(f, carry):
         rows = jnp.concatenate([rim_ref[f], x_ref[f, 0:BLOCK, :]], axis=0)
         out_ref[f] = jnp.dot(rows, weights, preferred_element_type=F32).astype(BF16)
-        copies.append(pltpu.make_async_copy(out_ref.at[f], out_hbm.at[f], sems.at[f]))
-        copies[-1].start()
+        copy(f).start()
+        return carry
+
+    lax.fori_loop(0, 4, each, 0)
     for ref in kept:
         ref[...] = w_ref[:, width:]
-    for copy in copies:
-        copy.wait()
+    for f in range(4):
+        copy(f).wait()
 
 
 def project_call(x, rim, w, width):
@@ -335,10 +343,17 @@
     hold_ref[...] = jnp.zeros_like(hold_ref)
     onward = (iota((2 * SUB, SUB), 0) % SUB > iota((2 * SUB, SUB), 1)).astype(BF16)
 
-    def piece(chunk, masked):
+    def piece(turn, carry):
+        chunk = last - turn
         move(chunk).wait()
-        if chunk > 1:
-            move(chunk - 2).start()
+        pl.when(chunk > 1)(lambda: move(chunk - 2).start())
+
+        @pl.when(turn == jnp.minimum(last, 1))
+        def _():
+            states.start()
+            for copy in weights:
+                copy.start()
+
         for h in range(2):
             late = late_ref[h]
             gained = acc_ref[h]
@@ -346,9 +361,9 @@
             offset = bias[2 * tensor + h] * LOG2E
             for sub in range(KEYS // SUB - 1, -1, -1):
                 at = chunk * KEYS + sub * SUB
-                first = at // BLOCK
-                key = kv_ref[first : first + 2, :, h * 128 : (h + 1) * 128]
-                value = kv_ref[first : first + 2, :, 256 + h * 128 : 256 + (h + 1) * 128]
+                picked = pl.ds(chunk * per + sub * (SUB // BLOCK), SUB // BLOCK)
+                key = kv_ref[picked, :, h * 128 : (h + 1) * 128]
+                value = kv_ref[picked, :, 256 + h * 128 : 256 + (h + 1) * 128]
                 logits = lax.dot_general(
                     query, key.reshape(SUB, 128), NT, preferred_element_type=F32
                 )
@@ -357,33 +372,24 @@
                     1.0 + jnp.exp2(-jnp.abs(logits))
                 )
                 taken = logits - soft
-                if masked:
-                    before = at + iota((BLOCK, SUB), 1) < block * BLOCK + iota((BLOCK, SUB), 0)
-                    soft = jnp.where(before, soft, 0.0)
+                before = at + iota((BLOCK, SUB), 1) < block * BLOCK + iota((BLOCK, SUB), 0)
+                soft = jnp.where(before, soft, 0.0)
                 high = soft.astype(BF16)
                 low = (soft - high.astype(F32)).astype(BF16)
                 tail = jnp.dot(
                     jnp.concatenate([high, low], axis=1), onward, preferred_element_type=F32
                 )
                 later = jnp.concatenate([late] * (SUB // 128), axis=1)
-                weight = jnp.exp2(taken - (tail + later))
-                if masked:
-                    weight = jnp.where(before, weight, 0.0)
+                weight = jnp.where(before, jnp.exp2(taken - (tail + later)), 0.0)
                 gained = gained + jnp.dot(
                     weight.astype(BF16), value.reshape(SUB, 128), preferred_element_type=F32
                 )
                 late = late + jnp.broadcast_to(tail[:, 0:1] + soft[:, 0:1], (BLOCK, 128))
             late_ref[h] = late
             acc_ref[h] = gained
-
-    for chunk in chunks:
-        if chunk == 1:
-            states.start()
-            for copy in weights:
-                copy.start()
-        pl.when(chunk == last)(lambda chunk=chunk: piece(chunk, True))
-        pl.when(chunk < last)(lambda chunk=chunk: piece(chunk, False))
-
+        return carry
+
+    lax.fori_loop(0, last + 1, piece, 0)
     states.wait()
 
     def advance(k, carry):

time: 183 us -> 185 us (1.011)
  Pallas kernels: 13.5 us -> 15.4 us
  transfers between devices with their start and end apart: 8 -> 8, of which waited for: 5 -> 5; matrix products, arithmetic and copies ran while one was open for 0% -> 0% of each run, Pallas kernels for 1% -> 2%
where the time goes in v6:
time: 185 us; the launch traced here: 184 us
  blocking collectives  83.5 us (45%)
  waiting for transfers between devices  45.2 us (24%)
  starting transfers between devices  25.6 us (14%)
  Pallas kernels  15.4 us (8%)
  between operations  13.6 us (7%)
    all_gather x1, blocking collectives, body(): early = lax.all_gather(first, 'sp', axis=0, tiled=True)  34.2 us
    all_gather x1, waiting for transfers between devices, body(): gathered = lax.all_gather(send, 'sp', axis=0)  31 us
    all_gather x1, blocking collectives, body(): act, kept = projected(lax.all_gather(second, 'sp', axis=0, tiled=True), 640)  27.8 us
    all_to_all x1, blocking collectives, body(): parts = lax.all_to_all(partial.reshape(8, 16, 2048), 'tp', 0, 0, tiled=True)  21.6 us
    ppermute x3, starting transfers between devices, rotated(): lax.ppermute(shard, axis, [(i, (i + by) % length) for i in range(length)])  10.7 us
    all_to_all x2, waiting for transfers between devices, projected(): return (lax.all_to_all(act, 'fs', 0, 0, tiled=True), *kept)  9.58 us
    all_to_all x2, starting transfers between devices, projected(): return (lax.all_to_all(act, 'fs', 0, 0, tiled=True), *kept)  8.03 us
    all_to_all x1, starting transfers between devices, body(): tokens = lax.all_to_all(split, 'fs', 0, 0, tiled=True)  5.14 us
  transfers between devices with their start and end apart: 8, of which 5 were waited for; matrix products, arithmetic and copies ran while one was open for 0% of the time, Pallas kernels for 2%

profile of v6, /device:TPU:1, one launch (start us, length us, event | category | flops | bytes accessed | tf_op | source)
XLA Modules:
  0.0 184.1 jit_solution(3326483179014195710)
XLA Ops:
  6.5 3.5 %prep.1 = (bf16[4,144,512]{2,1,0:T(8,128)(2,1)}, f32[32,128]{1,0:T(8,128)}, bf16[32,896]{1,0:T(8,128)(2,1)}, bf16[32,896]{1,0:T(8,128)(2,1)}) custom-call(bf16[1,128,2048]{2,1,0:T(8,128)(2,1)} %refs_0_.1, f32[1,2048]{1,0:T(1,128)} %bitcast.21, bf16[32,2048]{1,0:T(8,128)(2,1)} %bitcast.18, bf16[32,256]{1,0:T(8,128)(2,1)} %refs_3_.1, bf16[32,256]{1,0:T(8,128)(2,1)} %refs_4_.1, ...), custom_call_target="tpu_custom_call" | custom-call | tf_op jit(solution)/shard_map/prep/pallas_call | solution.py:102
  10.0 0.0 copy-start.1
  10.1 5.1 %all-to-all-start = ((bf16[4,144,512]{2,1,0:T(8,128)(2,1)}), bf16[4,144,512]{2,1,0:T(8,128)(2,1)S(1)}, u32[]{:S(2)}, u32[]{:S(2)}) async-start(bf16[4,144,512]{2,1,0:T(8,128)(2,1)} %get-tuple-element.22), calls=%async_computation | async-start | bytes 1179648 | tf_op jit(solution)/shard_map/all_to_all | solution.py:481
  15.2 34.2 %all_gather.12.w_ref = bf16[512,896]{1,0:T(8,128)(2,1)S(1)} all-gather(bf16[32,896]{1,0:T(8,128)(2,1)} %get-tuple-element.23), channel_id=1, replica_groups=mesh['sp'=16,'fs'=4,'tp'=8] {'sp'}, dimensions={0}, use_global_device_ids=true | all-gather | bytes 974848 | tf_op jit(solution)/shard_map/all_gather | solution.py:482
  49.4 0.0 all-to-all-done.x_ref.buf_ref
  49.5 1.7 collective-permute-start
  51.2 1.3 collective-permute-done.rim_ref
  52.5 2.2 %project.3 = bf16[4,144,896]{2,1,0:T(8,128)(2,1)} custom-call(bf16[4,144,512]{2,1,0:T(8,128)(2,1)S(1)} %all-to-all-done.x_ref.buf_ref, bf16[4,16,512]{2,1,0:T(8,128)(2,1)S(1)} %collective-permute-done.rim_ref, bf16[512,896]{1,0:T(8,128)(2,1)S(1)} %all_gather.12.w_ref), custom_call_target="tpu_custom_call" | custom-call | tf_op jit(solution)/shard_map/project/pallas_call | solution.py:152
  54.6 0.0 copy-start.2
  54.7 0.0 copy-start.5
  54.7 4.5 %all-to-all-start.2 = ((bf16[4,144,896]{2,1,0:T(8,128)(2,1)}), bf16[4,144,896]{2,1,0:T(8,128)(2,1)S(1)}, u32[]{:S(2)}, u32[]{:S(2)}) async-start(bf16[4,144,896]{2,1,0:T(8,128)(2,1)} %project.3), calls=%async_computation.2 | async-start | bytes 2064384 | tf_op jit(solution)/shard_map/all_to_all | solution.py:490
  59.2 0.0 all-gather.3.cloned.1.call-start
  59.2 0.1 pad_add_fusion.ids
  59.3 9.6 %all-to-all-done.2.act_ref = bf16[4,144,896]{2,1,0:T(8,128)(2,1)S(1)} async-done(((bf16[4,144,896]{2,1,0:T(8,128)(2,1)}), bf16[4,144,896]{2,1,0:T(8,128)(2,1)S(1)}, u32[]{:S(2)}, u32[]{:S(2)}) %all-to-all-start.2) | async-done | bytes 1032224 | tf_op jit(solution)/shard_map/all_to_all | solution.py:490
  68.9 2.3 %ssd_local.1 = (bf16[272,512]{1,0:T(8,128)(2,1)}, bf16[128,256]{1,0:T(8,128)(2,1)S(1)}, bf16[128,128]{1,0:T(8,128)(2,1)S(1)}, f32[8,128]{1,0:T(8,128)S(1)}, f32[128,8]{1,0:T(8,128)S(1)}) custom-call(s32[3]{0:T(128)S(1)} %pad_add_fusion.ids, f32[32]{0:T(128)S(1)} %copy-done.4, bf16[4,144,896]{2,1,0:T(8,128)(2,1)S(1)} %all-to-all-done.2.act_ref, ...), custom_call_target="tpu_custom_call" | custom-call | tf_op jit(solution)/shard_map/ssd_local/pallas_call | solution.py:233
  71.2 0.0 all-gather.3.cloned.1.call-update
  71.2 27.8 %all_gather.13.w_ref = bf16[512,896]{1,0:T(8,128)(2,1)S(1)} all-gather(bf16[32,896]{1,0:T(8,128)(2,1)S(1)} %copy-done.6), channel_id=1, replica_groups=mesh['sp'=16,'fs'=4,'tp'=8] {'sp'}, dimensions={0}, use_global_device_ids=true | all-gather | bytes 974848 | tf_op jit(solution)/shard_map/all_gather | solution.py:497
  99.0 1.9 %project.2 = (bf16[4,144,640]{2,1,0:T(8,128)(2,1)}, bf16[512,256]{1,0:T(8,128)(2,1)S(1)}) custom-call(bf16[4,144,512]{2,1,0:T(8,128)(2,1)S(1)} %all-to-all-done.x_ref.buf_ref, bf16[4,16,512]{2,1,0:T(8,128)(2,1)S(1)} %collective-permute-done.rim_ref, bf16[512,896]{1,0:T(8,128)(2,1)S(1)} %all_gather.13.w_ref), custom_call_target="tpu_custom_call" | custom-call | tf_op jit(solution)/shard_map/project/pallas_call | solution.py:152
  100.9 3.5 %all-to-all-start.1 = ((bf16[4,144,640]{2,1,0:T(8,128)(2,1)}), bf16[4,144,640]{2,1,0:T(8,128)(2,1)S(1)}, u32[]{:S(2)}, u32[]{:S(2)}) async-start(bf16[4,144,640]{2,1,0:T(8,128)(2,1)} %get-tuple-element.26), calls=%async_computation.1 | async-start | bytes 1474560 | tf_op jit(solution)/shard_map/all_to_all | solution.py:490
  104.4 3.3 %collective-permute-start.1 = (bf16[512,256]{1,0:T(8,128)(2,1)S(1)}, bf16[512,256]{1,0:T(8,128)(2,1)S(1)}, u32[]{:S(2)}, u32[]{:S(2)}) collective-permute-start(bf16[512,256]{1,0:T(8,128)(2,1)S(1)} %get-tuple-element.38.a0), channel_id=1, source_target_pairs={{0,8},{8,16},{16,24},{24,0},{1,9},{9,17},{17,25},{25,1},{2,10},{10... | collective-permute-start | bytes 786440 | tf_op jit(solution)/shard_map/ppermute | solution.py:468
  107.7 4.3 %collective-permute-start.2 = (bf16[512,256]{1,0:T(8,128)(2,1)S(1)}, bf16[512,256]{1,0:T(8,128)(2,1)S(1)}, u32[]{:S(2)}, u32[]{:S(2)}) collective-permute-start(bf16[512,256]{1,0:T(8,128)(2,1)S(1)} %get-tuple-element.38.a0), channel_id=1, source_target_pairs={{0,16},{8,24},{16,0},{24,8},{1,17},{9,25},{17,1},{25,9},{2,18},{10... | collective-permute-start | bytes 786440 | tf_op jit(solution)/shard_map/ppermute | solution.py:468
  112.1 3.1 %collective-permute-start.3 = (bf16[512,256]{1,0:T(8,128)(2,1)S(1)}, bf16[512,256]{1,0:T(8,128)(2,1)S(1)}, u32[]{:S(2)}, u32[]{:S(2)}) collective-permute-start(bf16[512,256]{1,0:T(8,128)(2,1)S(1)} %get-tuple-element.38.a0), channel_id=1, source_target_pairs={{0,24},{8,0},{16,8},{24,16},{1,25},{9,1},{17,9},{25,17},{2,26},{10... | collective-permute-start | bytes 786440 | tf_op jit(solution)/shard_map/ppermute | solution.py:468
  115.2 0.0 all-to-all-done.1.act_ref
  115.2 1.1 ssd_inner.1
  116.3 0.0 collective-permute-done.1.a1
  116.3 1.9 %collective-permute-done.2.a2 = bf16[512,256]{1,0:T(8,128)(2,1)S(1)} collective-permute-done((bf16[512,256]{1,0:T(8,128)(2,1)S(1)}, bf16[512,256]{1,0:T(8,128)(2,1)S(1)}, u32[]{:S(2)}, u32[]{:S(2)}) %collective-permute-start.2) | collective-permute-done | bytes 262176 | tf_op jit(solution)/shard_map/ppermute | solution.py:468
  118.2 1.4 collective-permute-done.3.a3
  119.6 31.0 %all-gather.3.cloned.1.call-done = bf16[4352,512]{1,0:T(8,128)(2,1)} async-done(((bf16[272,512]{1,0:T(8,128)(2,1)}), bf16[4352,512]{1,0:T(8,128)(2,1)}) %all-gather.3.cloned.1.call-update) | async-done | bytes 4456464 | tf_op jit(solution)/shard_map/all_gather | solution.py:496
  150.5 0.0 copy-done.2
  150.5 4.4 %attend.1 = bf16[128,2048]{1,0:T(8,128)(2,1)S(1)} custom-call(s32[3]{0:T(128)S(1)} %pad_add_fusion.ids, f32[16]{0:T(128)S(1)} %copy-done.5, bf16[128,256]{1,0:T(8,128)(2,1)S(1)} %get-tuple-element.33.q_ref, f32[128,256]{1,0:T(8,128)S(1)} %get-tuple-element.34.yin_ref, f32[128,256]{1,0:T(8,128)S(1)} %get-tuple-element.35.gate_ref, ...), custom_call_target="tpu_custom_call" | custom-call | tf_op jit(solution)/shard_map/attend/pallas_call | solution.py:437
  155.0 21.6 %all_to_all.20 = bf16[8,16,2048]{2,1,0:T(8,128)(2,1)S(1)} all-to-all(bf16[8,16,2048]{2,1,0:T(8,128)(2,1)S(1)} %bitcast.14), channel_id=1, replica_groups=mesh['sp'=16,'fs'=4,'tp'=8] {'tp'}, dimensions={0} | all-to-all | bytes 1048576 | tf_op jit(solution)/shard_map/all_to_all | solution.py:501
  176.5 0.7 reduce_sum.12
  (11 shorter events, 0.0 us)
Async XLA Ops:
  6.5 62.3 %copy-start.3 = (f32[1,128,4]{1,2,0:T(4,128)S(1)}, f32[1,128,4]{1,2,0:T(4,128)}, u32[]{:S(2)}) copy-start(f32[1,128,4]{1,2,0:T(4,128)} %param.26) | copy-start | bytes 6148
  6.5 62.3 %copy-start = (f32[4,4096]{1,0:T(4,128)S(1)}, f32[4,4096]{1,0:T(4,128)}, u32[]{:S(2)}) copy-start(f32[4,4096]{1,0:T(4,128)} %cc_ref.1) | copy-start | bytes 196612
  6.5 62.3 %copy-start.4 = (f32[32]{0:T(128)S(1)}, f32[32]{0:T(128)}, u32[]{:S(2)}) copy-start(f32[32]{0:T(128)} %rate.1) | copy-start | bytes 388
  10.0 58.8 %copy-start.1 = (f32[32,128]{1,0:T(8,128)S(1)}, f32[32,128]{1,0:T(8,128)}, u32[]{:S(2)}) copy-start(f32[32,128]{1,0:T(8,128)} %get-tuple-element.28.step_ref) | copy-start | bytes 49156
  10.1 61.2 %copy-start.6 = (bf16[32,896]{1,0:T(8,128)(2,1)S(1)}, bf16[32,896]{1,0:T(8,128)(2,1)}, u32[]{:S(2)}) copy-start(bf16[32,896]{1,0:T(8,128)(2,1)} %get-tuple-element.25) | copy-start | bytes 172036
  10.1 39.4 %all-to-all-start = ((bf16[4,144,512]{2,1,0:T(8,128)(2,1)}), bf16[4,144,512]{2,1,0:T(8,128)(2,1)S(1)}, u32[]{:S(2)}, u32[]{:S(2)}) async-start(bf16[4,144,512]{2,1,0:T(8,128)(2,1)} %get-tuple-element.22), calls=%async_computation | async-start | bytes 1179648 | tf_op jit(solution)/shard_map/all_to_all | solution.py:481
  49.5 3.0 %collective-permute-start = (bf16[4,16,512]{2,1,0:T(8,128)(2,1)S(1)}, bf16[4,16,512]{2,1,0:T(8,128)(2,1)S(1)}, u32[]{:S(2)}, u32[]{:S(2)}) collective-permute-start(bf16[4,16,512]{2,1,0:T(8,128)(2,1)S(1)} %slice.3), channel_id=1, source_target_pairs={{0,32},{32,64},{64,96},{96,128},{128,160},{160,192},{192,224},{224... | collective-permute-start | bytes 196616 | tf_op jit(solution)/shard_map/ppermute | solution.py:484
  54.6 95.9 %copy-start.2 = (f32[2048]{0:T(1024)S(1)}, f32[2048]{0:T(1024)}, u32[]{:S(2)}) copy-start(f32[2048]{0:T(1024)} %param.27) | copy-start | bytes 24580
  54.7 95.9 %copy-start.5 = (f32[16]{0:T(128)S(1)}, f32[16]{0:T(128)}, u32[]{:S(2)}) copy-start(f32[16]{0:T(128)} %bias.1) | copy-start | bytes 196
  54.7 14.2 %all-to-all-start.2 = ((bf16[4,144,896]{2,1,0:T(8,128)(2,1)}), bf16[4,144,896]{2,1,0:T(8,128)(2,1)S(1)}, u32[]{:S(2)}, u32[]{:S(2)}) async-start(bf16[4,144,896]{2,1,0:T(8,128)(2,1)} %project.3), calls=%async_computation.2 | async-start | bytes 2064384 | tf_op jit(solution)/shard_map/all_to_all | solution.py:490
  59.2 91.4 %all-gather.3.cloned.1.call-start = ((), (), s32[]{:S(2)}) async-start(), calls=%async_computation.4 | async-start | bytes 4734976 | tf_op jit(solution)/shard_map/all_gather | solution.py:496
  100.9 14.3 %all-to-all-start.1 = ((bf16[4,144,640]{2,1,0:T(8,128)(2,1)}), bf16[4,144,640]{2,1,0:T(8,128)(2,1)S(1)}, u32[]{:S(2)}, u32[]{:S(2)}) async-start(bf16[4,144,640]{2,1,0:T(8,128)(2,1)} %get-tuple-element.26), calls=%async_computation.1 | async-start | bytes 1474560 | tf_op jit(solution)/shard_map/all_to_all | solution.py:490
  104.4 11.9 %collective-permute-start.1 = (bf16[512,256]{1,0:T(8,128)(2,1)S(1)}, bf16[512,256]{1,0:T(8,128)(2,1)S(1)}, u32[]{:S(2)}, u32[]{:S(2)}) collective-permute-start(bf16[512,256]{1,0:T(8,128)(2,1)S(1)} %get-tuple-element.38.a0), channel_id=1, source_target_pairs={{0,8},{8,16},{16,24},{24,0},{1,9},{9,17},{17,25},{25,1},{2,10},{10... | collective-permute-start | bytes 786440 | tf_op jit(solution)/shard_map/ppermute | solution.py:468
  107.7 10.4 %collective-permute-start.2 = (bf16[512,256]{1,0:T(8,128)(2,1)S(1)}, bf16[512,256]{1,0:T(8,128)(2,1)S(1)}, u32[]{:S(2)}, u32[]{:S(2)}) collective-permute-start(bf16[512,256]{1,0:T(8,128)(2,1)S(1)} %get-tuple-element.38.a0), channel_id=1, source_target_pairs={{0,16},{8,24},{16,0},{24,8},{1,17},{9,25},{17,1},{25,9},{2,18},{10... | collective-permute-start | bytes 786440 | tf_op jit(solution)/shard_map/ppermute | solution.py:468
  112.1 7.5 %collective-permute-start.3 = (bf16[512,256]{1,0:T(8,128)(2,1)S(1)}, bf16[512,256]{1,0:T(8,128)(2,1)S(1)}, u32[]{:S(2)}, u32[]{:S(2)}) collective-permute-start(bf16[512,256]{1,0:T(8,128)(2,1)S(1)} %get-tuple-element.38.a0), channel_id=1, source_target_pairs={{0,24},{8,0},{16,8},{24,16},{1,25},{9,1},{17,9},{25,17},{2,26},{10... | collective-permute-start | bytes 786440 | tf_op jit(solution)/shard_map/ppermute | solution.py:468
Sparse Core Ops, SparseCore 0:
  71.3 79.1 all-gather.2

commit v7 on v3

--- a/solution.py
+++ b/solution.py
@@ -40,76 +40,76 @@
     return copies
 
 
-def shuffled(normed, f, g):
-    lane = iota((normed.shape[0], 128), 1) // 32
-    out = None
-    for k in range(4):
-        at = (4 * g + k) * 128
-        piece = normed[:, at : at + 128]
-        shift = ((k - f) * 32) % 128
-        if shift:
-            piece = pltpu.roll(piece, shift, 1)
-        out = piece if out is None else jnp.where(lane == k, piece, out)
-    return out.astype(BF16)
-
-
 def normalised(x, gain):
     wide = x.astype(F32)
     scale = lax.rsqrt(jnp.mean(wide * wide, axis=-1, keepdims=True) + EPS)
     return (wide * scale * gain).astype(BF16)
 
 
+def turned(tile, by):
+    return pltpu.roll(tile, by % 128, 1) if by % 128 else tile
+
+
 def prep_kernel(*refs):
     x_hbm, gain_hbm, ws_hbm = refs[:3]
     sources = refs[3:12]
-    xs_ref, step_ref, first_ref, second_ref = refs[12:16]
-    x_ref, gain_ref, ws_ref, third_ref, sems, wsems = refs[16:]
+    xs_ref, step_ref, cut_ref = refs[12:15]
+    x_ref, gain_ref, ws_ref, all_ref, sems, wsems = refs[15:]
     early = pull(((x_hbm.at[0], x_ref), (gain_hbm, gain_ref), (ws_hbm, ws_ref)), sems)
-    pairs = []
-    outs = (first_ref, second_ref, third_ref)
-    at, which = 0, 0
-    for n, src in enumerate(sources):
-        if n in (4, 7):
-            at, which = 0, which + 1
-        pairs.append((src, outs[which].at[:, pl.ds(at, src.shape[1])]))
+    pairs, starts, at = [], [], 0
+    for src in sources:
+        pairs.append((src, all_ref.at[:, pl.ds(at, src.shape[1])]))
+        starts.append(at)
         at += src.shape[1]
     later = pull(pairs, wsems)
     for copy in early:
         copy.wait()
     normed = normalised(x_ref[...], gain_ref[...])
+    xs_ref[HALO:, :] = normed
     step_ref[...] = softplus(
         lax.dot_general(ws_ref[...], normed, NT, preferred_element_type=F32)
     )
-    wide = normed.astype(F32)
-    for f in range(4):
-        for g in range(4):
-            xs_ref[f, HALO:ROWS, g * 128 : (g + 1) * 128] = shuffled(wide, f, g)
     for copy in later:
         copy.wait()
+    rows = all_ref.shape[0]
+    lane = iota((rows, 128), 1)
+    key, value, entry, gate, query, bkey, cquery, outs = starts[:8]
+
+    def tile(at):
+        return all_ref[:, at : at + 128].astype(F32)
+
     for f in range(4):
-        xs_ref[f, ROWS:, :] = third_ref[...]
+        side, half = 64 * (f % 2), 128 * (f // 2)
+        pair = lambda a, b: jnp.where(
+            lane < 64, turned(tile(a + half), -side), turned(tile(b + half), 64 - side)
+        ).astype(BF16)
+        cut_ref[f, :, 0:128] = pair(key, value)
+        cut_ref[f, :, 128:256] = jnp.where(
+            lane < 64, turned(tile(entry + half), -side), turned(tile(bkey), 64 - 32 * f)
+        ).astype(BF16)
+        cut_ref[f, :, 256:384] = pair(gate, query)
+        cut_ref[f, :, 384:512] = turned(tile(cquery), -32 * f).astype(BF16)
+        cut_ref[f, :, 512:] = all_ref[:, outs : outs + 512]
 
 
 def prep_call(inputs, gain, w_step_t, *arrays):
     rows, width = inputs.shape[1:]
     heads = w_step_t.shape[0]
     part = arrays[0].shape[0]
-    widths = [sum(a.shape[1] for a in group) for group in (arrays[:4], arrays[4:7], arrays[7:])]
     hbm = pl.BlockSpec(memory_space=pltpu.HBM)
     return pl.pallas_call(
         prep_kernel,
         in_specs=[hbm] * 12,
         out_shape=(
-            jax.ShapeDtypeStruct((4, ROWS + part, width // 4), BF16),
+            jax.ShapeDtypeStruct((rows + HALO, width), BF16),
             jax.ShapeDtypeStruct((heads, rows), F32),
-            jax.ShapeDtypeStruct((part, widths[0]), BF16),
-            jax.ShapeDtypeStruct((part, widths[1]), BF16),
+            jax.ShapeDtypeStruct((4, part, 1024), BF16),
         ),
         scratch_shapes=[
             pltpu.VMEM((rows, width), BF16),
             pltpu.VMEM((1, width), F32),
             pltpu.VMEM((heads, width), BF16),
-            pltpu.VMEM((part, widths[2]), BF16),
+            pltpu.VMEM((part, sum(a.shape[1] for a in arrays)), BF16),
             pltpu.SemaphoreType.DMA((3,)),
             pltpu.SemaphoreType.DMA((9,)),
         ],
@@ -118,11 +118,8 @@
 
 
 def halo_kernel(xs_in, halo_ref, gain_ref, xs_out, rim_ref, sem):
-    wide = normalised(halo_ref[...], gain_ref[...]).astype(F32)
-    for f in range(4):
-        for g in range(4):
-            rim_ref[f, :, g * 128 : (g + 1) * 128] = shuffled(wide, f, g)
-    copy = pltpu.make_async_copy(rim_ref, xs_out.at[:, pl.ds(0, HALO)], sem)
+    rim_ref[...] = normalised(halo_ref[...], gain_ref[...])
+    copy = pltpu.make_async_copy(rim_ref, xs_out.at[pl.ds(0, HALO)], sem)
     copy.start()
     copy.wait()
 
@@ -136,32 +133,53 @@
         out_specs=anywhere,
         out_shape=jax.ShapeDtypeStruct(xs.shape, BF16),
         input_output_aliases={0: 0},
-        scratch_shapes=[pltpu.VMEM((4, HALO, xs.shape[2]), BF16), pltpu.SemaphoreType.DMA],
+        scratch_shapes=[pltpu.VMEM((HALO, xs.shape[1]), BF16), pltpu.SemaphoreType.DMA],
         name="halo",
     )(xs, halo, gain.reshape(1, -1))
 
 
 def project_kernel(x_ref, w_ref, out_ref):
-    for f in range(4):
-        out_ref[f] = jnp.dot(
-            x_ref[f, 0:ROWS, :], w_ref[...], preferred_element_type=F32
-        ).astype(BF16)
+    act = jnp.dot(x_ref[0], w_ref[...], preferred_element_type=F32).astype(BF16)
+    width = act.shape[1]
+    out_ref[0, :, 0:width] = act
+    out_ref[0, :, width:] = jnp.zeros((act.shape[0], out_ref.shape[2] - width), BF16)
 
 
 def project_call(x, w):
+    count, rows, depth = x.shape
     return pl.pallas_call(
         project_kernel,
-        out_shape=jax.ShapeDtypeStruct((4, ROWS, w.shape[1]), BF16),
-        compiler_params=vmem(),
+        grid=(count,),
+        in_specs=[
+            pl.BlockSpec((1, rows, depth), lambda i: (i, 0, 0)),
+            pl.BlockSpec(w.shape, lambda i: (0, 0)),
+        ],
+        out_specs=pl.BlockSpec((1, rows, 256), lambda i: (i, 0, 0)),
+        out_shape=jax.ShapeDtypeStruct((count, rows, 256), BF16),
         name="project",
     )(x, w)
 
 
-def added(ref, at, width):
-    total = ref[0, :, at : at + width].astype(F32)
-    for j in range(1, 4):
-        total = total + ref[j, :, at : at + width].astype(F32)
-    return total.astype(BF16)
+def joined(ref, rows, swap):
+    lane = iota((rows, 128), 1) < 64
+    tiles = []
+    for j in range(2):
+        left = ref[2 * j, ref.shape[1] - rows :, 0:128].astype(F32)
+        right = ref[2 * j + 1, ref.shape[1] - rows :, 0:128].astype(F32)
+        if swap:
+            tiles.append(jnp.where(lane, turned(left, 64), right))
+        else:
+            tiles.append(jnp.where(lane, left, turned(right, 64)))
+    return tiles
+
+
+def quarters(ref, at):
+    lane = iota((ROWS, 128), 1) // 32
+    out = None
+    for f in range(4):
+        tile = turned(ref[f, :, 128:256].astype(F32), 32 * f - at)
+        out = tile if out is None else jnp.where(lane == f, tile, out)
+    return out
 
 
 def convolved(wide_ref, taps):
@@ -180,13 +198,18 @@
     tensor = ids[1]
     moved = pull(
         [
-            (buf_ref.at[f, pl.ds(ROWS, 32)], send_ref.at[pl.ds(KEPT + 32 * f, 32)])
+            (buf_ref.at[f, :, pl.ds(512, 512)], send_ref.at[pl.ds(KEPT + 32 * f, 32)])
             for f in range(4)
         ],
         sems,
     )
-    send_ref[0:BLOCK, :] = added(act_ref, 0, 512)[HALO:]
-    wide_ref[...] = added(act_ref, 512, 384).astype(F32)
+    keys = joined(act_ref, BLOCK, False) + joined(act_ref, BLOCK, True)
+    send_ref[0:BLOCK, :] = jnp.concatenate(keys, axis=1).astype(BF16)
+    entry = [act_ref[f, :, 128:256].astype(F32) for f in range(4)]
+    left = iota((ROWS, 128), 1) < 64
+    wide_ref[:, 0:128] = jnp.where(left, entry[0], turned(entry[1], 64))
+    wide_ref[:, 128:256] = jnp.where(left, entry[2], turned(entry[3], 64))
+    wide_ref[:, 256:384] = quarters(act_ref, 64)
     conv = convolved(wide_ref, jnp.concatenate([ci_ref[...], cb_ref[...]], axis=1))
     xin, bkey = conv[:, 0:256], conv[:, 256:384]
     xin_ref[...] = xin
@@ -253,7 +276,6 @@
             jax.ShapeDtypeStruct((8, BLOCK), F32),
             jax.ShapeDtypeStruct((BLOCK, 8), F32),
         ),
-        compiler_params=vmem(),
         name="ssd_local",
     )(ids, rate, act, step, offset, conv_weight, conv_weight, buf)
 
@@ -262,9 +284,9 @@
     ids, act_ref, cc_ref, xin_ref, bkey_ref, rows_ref, cols_ref,
     yin_ref, gate_ref, cq_ref, q_ref, wide_ref,
 ):
-    gate_ref[...] = silu(added(act_ref, 0, 256)[HALO:].astype(F32))
-    q_ref[...] = added(act_ref, 384, 256)[HALO:]
-    wide_ref[...] = added(act_ref, 256, 128).astype(F32)
+    gate_ref[...] = silu(jnp.concatenate(joined(act_ref, BLOCK, False), axis=1))
+    q_ref[...] = jnp.concatenate(joined(act_ref, BLOCK, True), axis=1).astype(BF16)
+    wide_ref[...] = quarters(act_ref, 0)
     cquery = convolved(wide_ref, cc_ref[...])
     cq_ref[...] = cquery
     lower = iota((BLOCK, BLOCK), 0) >= iota((BLOCK, BLOCK), 1)
@@ -304,10 +326,10 @@
     )(ids, act, conv_weight, xin, bkey, rows, cols)
 
 
-SUB = 256
 KEYS = 512
 KEPT = BLOCK + 80
 SENT = KEPT + BLOCK
+LOG2E = 1.4426950408889634
 
 
 def attend_kernel(
@@ -318,6 +340,7 @@
     per = KEYS // BLOCK
     count = all_hbm.shape[0]
     chunks = range(count // per - 1, -1, -1)
+    last = block // per
 
     def move(chunk):
         picked = pl.ds(chunk * per, per)
@@ -326,18 +349,64 @@
         )
 
     states = pltpu.make_async_copy(all_hbm.at[:, pl.ds(BLOCK, 80)], st_ref, sems.at[0])
-    states.start()
+    weights = pltpu.make_async_copy(all_hbm.at[:, pl.ds(KEPT, BLOCK)], w_ref, sems.at[1])
     for chunk in chunks:
-
-        @pl.when(chunk * per <= block)
-        def _(chunk=chunk):
-            move(chunk).start()
-
-    weights = pltpu.make_async_copy(all_hbm.at[:, pl.ds(KEPT, BLOCK)], w_ref, sems.at[1])
-    weights.start()
+        pl.when((chunk <= last) & (chunk >= last - 1))(lambda chunk=chunk: move(chunk).start())
     acc_ref[...] = jnp.zeros_like(acc_ref)
     late_ref[...] = jnp.zeros_like(late_ref)
     hold_ref[...] = jnp.zeros_like(hold_ref)
+    row = iota((256, 256), 0) % 128
+    col = iota((256, 256), 1)
+    onward = ((row > col) | (col >= 128)).astype(BF16)
+
+    def piece(turn, carry):
+        chunk = last - turn
+        move(chunk).wait()
+        pl.when(chunk > 1)(lambda: move(chunk - 2).start())
+
+        @pl.when(turn == jnp.minimum(last, 1))
+        def _():
+            states.start()
+            weights.start()
+
+        picked = pl.ds(chunk * per, per)
+        before = [
+            chunk * KEYS + sub * BLOCK + iota((BLOCK, BLOCK), 1)
+            < block * BLOCK + iota((BLOCK, BLOCK), 0)
+            for sub in range(per)
+        ]
+        taken, parts = {}, []
+        for h in range(2):
+            query = q_ref[:, h * 128 : (h + 1) * 128]
+            key = kv_ref[picked, :, h * 128 : (h + 1) * 128].reshape(KEYS, 128)
+            logits = lax.dot_general(query, key, NT, preferred_element_type=F32)
+            logits = logits * (128 ** -0.5 * LOG2E) + bias[2 * tensor + h] * LOG2E
+            soft = jnp.maximum(logits, 0.0) + LOG2E * jnp.log(1.0 + jnp.exp2(-jnp.abs(logits)))
+            for sub in range(per):
+                at = slice(sub * BLOCK, (sub + 1) * BLOCK)
+                taken[h, sub] = logits[:, at] - soft[:, at]
+                kept = jnp.where(before[sub], soft[:, at], 0.0)
+                high = kept.astype(BF16)
+                low = (kept - high.astype(F32)).astype(BF16)
+                parts.append(jnp.concatenate([high, low], axis=1))
+        sums = jnp.dot(jnp.concatenate(parts, axis=0), onward, preferred_element_type=F32)
+        for h in range(2):
+            late = late_ref[h]
+            weights_h = [None] * per
+            for sub in range(per - 1, -1, -1):
+                at = (h * per + sub) * BLOCK
+                mine_sums = sums[at : at + BLOCK]
+                weight = jnp.exp2(taken[h, sub] - (mine_sums[:, 0:128] + late))
+                weights_h[sub] = jnp.where(before[sub], weight, 0.0).astype(BF16)
+                late = late + mine_sums[:, 128:256]
+            value = kv_ref[picked, :, 256 + h * 128 : 256 + (h + 1) * 128].reshape(KEYS, 128)
+            acc_ref[h] += jnp.dot(
+                jnp.concatenate(weights_h, axis=1), value, preferred_element_type=F32
+            )
+            late_ref[h] = late
+        return carry
+
+    lax.fori_loop(0, last + 1, piece, 0)
     states.wait()
 
     def advance(k, carry):
@@ -358,46 +427,6 @@
     gated = (yin_ref[...] + jnp.concatenate(ys, axis=1)) * gate_ref[...]
     scale = lax.rsqrt(jnp.mean(gated * gated, axis=-1, keepdims=True) + EPS)
     mixed = (gated * scale * gain_ref[...]).astype(BF16)
-    after = (iota((SUB, SUB), 0) > iota((SUB, SUB), 1)).astype(BF16)
-    ones = jnp.ones((SUB, 128), BF16)
-    for chunk in chunks:
-
-        @pl.when(chunk * per <= block)
-        def _(chunk=chunk):
-            move(chunk).wait()
-            for h in range(2):
-                late = late_ref[h]
-                gained = acc_ref[h]
-                query = q_ref[:, h * 128 : (h + 1) * 128]
-                for sub in range(KEYS // SUB - 1, -1, -1):
-                    at = chunk * KEYS + sub * SUB
-                    first = at // BLOCK
-                    before = at + iota((BLOCK, SUB), 1) < block * BLOCK + iota((BLOCK, SUB), 0)
-                    key = kv_ref[first : first + 2, :, h * 128 : (h + 1) * 128]
-                    value = kv_ref[first : first + 2, :, 256 + h * 128 : 256 + (h + 1) * 128]
-                    logits = lax.dot_general(
-                        query, key.reshape(SUB, 128), NT, preferred_element_type=F32
-                    )
-                    logits = logits * (128 ** -0.5) + bias[2 * tensor + h]
-                    soft = jnp.maximum(logits, 0.0) + jnp.log(1.0 + jnp.exp(-jnp.abs(logits)))
-                    passed = jnp.where(before, -soft, 0.0)
-                    high = passed.astype(BF16)
-                    low = (passed - high.astype(F32)).astype(BF16)
-                    tail = jnp.dot(high, after, preferred_element_type=F32) + jnp.dot(
-                        low, after, preferred_element_type=F32
-                    )
-                    whole = jnp.dot(high, ones, preferred_element_type=F32) + jnp.dot(
-                        low, ones, preferred_element_type=F32
-                    )
-                    later = jnp.concatenate([late] * (SUB // 128), axis=1)
-                    weight = jnp.where(before, jnp.exp(logits - soft + (tail + later)), 0.0)
-                    gained = gained + jnp.dot(
-                        weight.astype(BF16), value.reshape(SUB, 128), preferred_element_type=F32
-                    )
-                    late = late + whole
-                late_ref[h] = late
-                acc_ref[h] = gained
-
     both = jnp.concatenate([mixed, acc_ref[0].astype(BF16), acc_ref[1].astype(BF16)], axis=1)
     weights.wait()
     for s in range(count):
@@ -442,26 +471,29 @@
     decay_offset, ssd_gain, w_query, w_key, w_value, stick_bias, out_mixer, out_attend,
 ):
     length = lax.axis_size("sp")
-    ids = jnp.stack([lax.axis_index("sp"), lax.axis_index("tp")]).astype(jnp.int32)
+    ids = jnp.stack([lax.axis_index(name) for name in ("sp", "tp")]).astype(jnp.int32)
     halo = lax.ppermute(
         inputs[0, BLOCK - HALO :], "sp", [(i, i + 1) for i in range(length - 1)]
     )
-    split, step, first, second = prep_call(
-        inputs, norm_gain, w_step.T, w_key, w_value, w_input, w_bkey, w_gate, w_cquery, w_query,
+    normed, step, cut = prep_call(
+        inputs, norm_gain, w_step.T, w_key, w_value, w_input, w_gate, w_query, w_bkey, w_cquery,
         out_mixer.T, out_attend.T,
     )
-    split = halo_call(split, halo, norm_gain)
-    tokens = lax.all_to_all(split, "fs", 0, 0, tiled=True)
-
-    def projected(weights):
-        whole = lax.all_gather(weights, "sp", axis=0, tiled=True)
-        return lax.all_to_all(project_call(tokens, whole), "fs", 0, 0, tiled=True)
+    cut = lax.all_to_all(cut, "fs", 0, 0, tiled=True)
+    tokens = lax.all_gather(halo_call(normed, halo, norm_gain), "fs", axis=0)
+
+    def projected(at, width):
+        part = cut[:, :, at : at + width].reshape(-1, width)
+        act = project_call(tokens, lax.all_gather(part, "sp", axis=0, tiled=True))
+        return lax.all_to_all(act, "fs", 0, 0, tiled=True)
 
     send, xin, bkey, srows, scols = local_call(
-        ids, decay_rate, projected(first), step, decay_offset[0].T, conv_weight, tokens
+        ids, decay_rate, projected(0, 224), step, decay_offset[0].T, conv_weight, cut
     )
     gathered = lax.all_gather(send, "sp", axis=0)
-    yin, gate, cq, q = inner_call(ids, projected(second), conv_weight, xin, bkey, srows, scols)
+    yin, gate, cq, q = inner_call(
+        ids, projected(256, 160), conv_weight, xin, bkey, srows, scols
+    )
     partial = attend_call(ids, stick_bias, q, yin, gate, cq, scols, ssd_gain, gathered)
     parts = lax.all_to_all(partial.reshape(8, 16, 2048), "tp", 0, 0, tiled=True)
     return jnp.sum(parts.astype(F32), axis=0).astype(BF16)[None]

time: 187 us -> 198 us (1.059)
  blocking collectives: 87.8 us -> 111 us
  waiting for transfers between devices: 55.4 us -> 38.6 us
  Pallas kernels: 14.8 us -> 21.9 us
  starting transfers between devices: 12.9 us -> 7.84 us
    all_gather x2, blocking collectives: 57.7 us -> 73.4 us  [projected(): act = project_call(tokens, lax.all_gather(part, 'sp', axis=0, tiled=True))]
    all_gather x1, waiting for transfers between devices: 45.8 us -> 33.5 us  [body(): gathered = lax.all_gather(send, 'sp', axis=0)]
    all_to_all x1 -> x2, blocking collectives: 10.5 us -> 18.9 us  [the longest x1 9.73 us: body(): cut = lax.all_to_all(cut, 'fs', 0, 0, tiled=True)]
    pallas_call x2, Pallas kernels: 2.44 us -> 8.91 us  [project_call(): pl.pallas_call(project_kernel, grid=(count,), in_specs=[pl.BlockSpec((1,...]
    all_to_all x2 -> x1, starting transfers between devices: 8.6 us -> 3.45 us  [projected(): return lax.all_to_all(act, 'fs', 0, 0, tiled=True)]
    all_to_all x2 -> x1, waiting for transfers between devices: 9.58 us -> 5.02 us  [projected(): return lax.all_to_all(act, 'fs', 0, 0, tiled=True)]
  transfers between devices with their start and end apart: 4 -> 4, of which waited for: 2 -> 2; matrix products, arithmetic and copies ran while one was open for 0% -> 1% of each run, Pallas kernels for 2% -> 4%
where the time goes in v7:
time: 198 us; the launch traced here: 197 us
  blocking collectives  111 us (56%)
  waiting for transfers between devices  38.6 us (19%)
  Pallas kernels  21.9 us (11%)
  between operations  13.6 us (7%)
  starting transfers between devices  7.84 us (4%)
  local copies, waits for them, and re-layouts  3.13 us (2%)
    all_gather x2, blocking collectives, projected(): act = project_call(tokens, lax.all_gather(part, 'sp', axis=0, tiled=True))  73.4 us
    all_gather x1, waiting for transfers between devices, body(): gathered = lax.all_gather(send, 'sp', axis=0)  33.5 us
    all_to_all x1, blocking collectives, body(): parts = lax.all_to_all(partial.reshape(8, 16, 2048), 'tp', 0, 0, tiled=True)  18.6 us
    all_to_all x1, blocking collectives, body(): cut = lax.all_to_all(cut, 'fs', 0, 0, tiled=True)  9.73 us
    all_to_all x1, blocking collectives, projected(): return lax.all_to_all(act, 'fs', 0, 0, tiled=True)  9.18 us
    pallas_call x2, Pallas kernels, project_call(): pl.pallas_call(project_kernel, grid=(count,), in_specs=[pl.BlockSpec((1,...  8.91 us
    all_to_all x1, waiting for transfers between devices, projected(): return lax.all_to_all(act, 'fs', 0, 0, tiled=True)  5.02 us
    pallas_call x1, Pallas kernels, attend_call(): pl.pallas_call(attend_kernel, grid_spec=pltpu.PrefetchScalarGridSpec(num_...  4.45 us
  transfers between devices with their start and end apart: 4, of which 2 were waited for; matrix products, arithmetic and copies ran while one was open for 1% of the time, Pallas kernels for 4%

profile of v7, /device:TPU:1, one launch (start us, length us, event | category | flops | bytes accessed | tf_op | source)
XLA Modules:
  0.0 197.3 jit_solution(18362911965238742369)
XLA Ops:
  6.5 0.8 slice_bitcast_fusion
  7.4 4.4 %collective-permute-start = (bf16[16,2048]{1,0:T(8,128)(2,1)S(1)}, bf16[16,2048]{1,0:T(8,128)(2,1)S(1)}, u32[]{:S(2)}, u32[]{:S(2)}) collective-permute-start(bf16[16,2048]{1,0:T(8,128)(2,1)S(1)} %slice_bitcast_fusion), channel_id=1, source_target_pairs={{0,32},{32,64},{64,96},{96,128},{128,160},{160,192},{192,224},{224... | collective-permute-start | bytes 196616 | tf_op jit(solution)/shard_map/ppermute | solution.py:475
  11.7 2.7 %prep.1 = (bf16[144,2048]{1,0:T(8,128)(2,1)}, f32[32,128]{1,0:T(8,128)}, bf16[4,32,1024]{2,1,0:T(8,128)(2,1)}) custom-call(bf16[1,128,2048]{2,1,0:T(8,128)(2,1)} %refs_0_.1, f32[1,2048]{1,0:T(1,128)} %bitcast.26, bf16[32,2048]{1,0:T(8,128)(2,1)} %bitcast.25, bf16[32,256]{1,0:T(8,128)(2,1)} %refs_3_.1, bf16[32,256]{1,0:T(8,128)(2,1)} %refs_4_.1, ...), custom_call_target="tpu_custom_call" | custom-call | tf_op jit(solution)/shard_map/prep/pallas_call | solution.py:100
  14.4 0.0 collective-permute-done.halo_ref
  14.4 0.0 copy-start.10
  14.5 0.6 copy-done.10
  15.1 1.6 halo.1
  16.7 0.0 all-gather.5.cloned.1.call-update
  16.7 9.7 %all_to_all.20.buf_ref = bf16[4,32,1024]{2,1,0:T(8,128)(2,1)S(1)} all-to-all(bf16[4,32,1024]{2,1,0:T(8,128)(2,1)} %get-tuple-element.18), channel_id=1, replica_groups=mesh['sp'=16,'fs'=4,'tp'=8] {'fs'}, dimensions={0} | all-to-all | bytes 524288 | tf_op jit(solution)/shard_map/all_to_all | solution.py:482
  26.4 37.0 %all_gather.21.w_ref = bf16[2048,224]{1,0:T(8,128)(2,1)} all-gather(bf16[128,224]{1,0:T(8,128)(2,1)S(1)} %bitcast.24), channel_id=1, replica_groups=mesh['sp'=16,'fs'=4,'tp'=8] {'sp'}, dimensions={0}, use_global_device_ids=true | all-gather | bytes 974848 | tf_op jit(solution)/shard_map/all_gather | solution.py:487
  63.5 4.5 %project.3 = bf16[4,144,256]{2,1,0:T(8,128)(2,1)} custom-call(bf16[4,144,2048]{2,1,0:T(8,128)(2,1)} %bitcast.20, bf16[2048,224]{1,0:T(8,128)(2,1)} %all_gather.21.w_ref), custom_call_target="tpu_custom_call" | custom-call | tf_op jit(solution)/shard_map/project/pallas_call | solution.py:150
  68.0 3.5 %all-to-all-start.2 = ((bf16[4,144,256]{2,1,0:T(8,128)(2,1)}), bf16[4,144,256]{2,1,0:T(8,128)(2,1)S(1)}, u32[]{:S(2)}, u32[]{:S(2)}) async-start(bf16[4,144,256]{2,1,0:T(8,128)(2,1)} %project.3), calls=%async_computation.2 | async-start | bytes 589824 | tf_op jit(solution)/shard_map/all_to_all | solution.py:488
  71.4 0.0 all-gather.7.cloned.1.call-start
  71.5 0.6 pad_add_fusion.ids
  72.1 5.0 %all-to-all-done.2.act_ref = bf16[4,144,256]{2,1,0:T(8,128)(2,1)S(1)} async-done(((bf16[4,144,256]{2,1,0:T(8,128)(2,1)}), bf16[4,144,256]{2,1,0:T(8,128)(2,1)S(1)}, u32[]{:S(2)}, u32[]{:S(2)}) %all-to-all-start.2) | async-done | bytes 294944 | tf_op jit(solution)/shard_map/all_to_all | solution.py:488
  77.1 0.0 copy-done.8
  77.1 0.8 copy-done.9
  77.8 3.3 %ssd_local.1 = (bf16[336,512]{1,0:T(8,128)(2,1)}, bf16[128,256]{1,0:T(8,128)(2,1)}, bf16[128,128]{1,0:T(8,128)(2,1)}, f32[8,128]{1,0:T(8,128)}, f32[128,8]{1,0:T(8,128)}) custom-call(s32[2]{0:T(128)} %pad_add_fusion.ids, f32[32]{0:T(128)} %rate.1, bf16[4,144,256]{2,1,0:T(8,128)(2,1)} %copy-done.9, f32[32,128]{1,0:T(8,128)} %get-tuple-element.19.step_ref, ...), custom_call_target="tpu_custom_call" | custom-call | tf_op jit(solution)/shard_map/ssd_local/pallas_call | solution.py:253
  81.1 0.0 copy-start.2
  81.2 0.0 copy-start.3
  81.2 0.0 copy-start.6
  81.2 0.0 all-gather.7.cloned.1.call-update
  81.2 0.9 slice.12
  82.1 36.4 %all_gather.20.w_ref = bf16[2048,160]{1,0:T(8,128)(2,1)} all-gather(bf16[128,160]{1,0:T(8,128)(2,1)S(1)} %bitcast.23), channel_id=1, replica_groups=mesh['sp'=16,'fs'=4,'tp'=8] {'sp'}, dimensions={0}, use_global_device_ids=true | all-gather | bytes 696320 | tf_op jit(solution)/shard_map/all_gather | solution.py:487
  118.4 4.4 %project.2 = bf16[4,144,256]{2,1,0:T(8,128)(2,1)} custom-call(bf16[4,144,2048]{2,1,0:T(8,128)(2,1)} %bitcast.21, bf16[2048,160]{1,0:T(8,128)(2,1)} %all_gather.20.w_ref), custom_call_target="tpu_custom_call" | custom-call | tf_op jit(solution)/shard_map/project/pallas_call | solution.py:150
  122.9 9.2 %all_to_all.21.act_ref = bf16[4,144,256]{2,1,0:T(8,128)(2,1)S(1)} all-to-all(bf16[4,144,256]{2,1,0:T(8,128)(2,1)} %project.2), channel_id=1, replica_groups=mesh['sp'=16,'fs'=4,'tp'=8] {'fs'}, dimensions={0} | all-to-all | bytes 589824 | tf_op jit(solution)/shard_map/all_to_all | solution.py:488
  132.1 0.0 copy-done
  132.1 1.0 ssd_inner.1
  133.1 33.5 %all-gather.7.cloned.1.call-done = bf16[5376,512]{1,0:T(8,128)(2,1)} async-done(((bf16[336,512]{1,0:T(8,128)(2,1)}), bf16[5376,512]{1,0:T(8,128)(2,1)}) %all-gather.7.cloned.1.call-update) | async-done | bytes 5505040 | tf_op jit(solution)/shard_map/all_gather | solution.py:493
  166.7 4.4 %attend.1 = bf16[128,2048]{1,0:T(8,128)(2,1)S(1)} custom-call(s32[2]{0:T(128)S(1)} %copy-done.5, f32[16]{0:T(128)S(1)} %copy-done.7, bf16[128,256]{1,0:T(8,128)(2,1)S(1)} %get-tuple-element.24.q_ref, f32[128,256]{1,0:T(8,128)S(1)} %get-tuple-element.25.yin_ref, f32[128,256]{1,0:T(8,128)S(1)} %get-tuple-element.26.gate_ref, ...), custom_call_target="tpu_custom_call" | custom-call | tf_op jit(solution)/shard_map/attend/pallas_call | solution.py:441
  171.1 18.6 %all_to_all.22 = bf16[8,16,2048]{2,1,0:T(8,128)(2,1)S(1)} all-to-all(bf16[8,16,2048]{2,1,0:T(8,128)(2,1)S(1)} %bitcast.18), channel_id=1, replica_groups=mesh['sp'=16,'fs'=4,'tp'=8] {'tp'}, dimensions={0} | all-to-all | bytes 1048576 | tf_op jit(solution)/shard_map/all_to_all | solution.py:498
  189.7 0.7 reduce_sum.12
  (17 shorter events, 0.0 us)
Async XLA Ops:
  6.5 56.9 %all-gather.5.cloned.1.call-start = ((), (), s32[]{:S(2)}) async-start(), calls=%async_computation.4 | async-start | bytes 2949120 | tf_op jit(solution)/shard_map/all_gather | solution.py:483
  7.4 7.0 %collective-permute-start = (bf16[16,2048]{1,0:T(8,128)(2,1)S(1)}, bf16[16,2048]{1,0:T(8,128)(2,1)S(1)}, u32[]{:S(2)}, u32[]{:S(2)}) collective-permute-start(bf16[16,2048]{1,0:T(8,128)(2,1)S(1)} %slice_bitcast_fusion), channel_id=1, source_target_pairs={{0,32},{32,64},{64,96},{96,128},{128,160},{160,192},{192,224},{224... | collective-permute-start | bytes 196616 | tf_op jit(solution)/shard_map/ppermute | solution.py:475
  14.4 0.6 copy-start.10
  26.4 50.7 %copy-start.8 = (bf16[4,32,1024]{2,1,0:T(8,128)(2,1)}, bf16[4,32,1024]{2,1,0:T(8,128)(2,1)S(1)}, u32[]{:S(2)}) copy-start(bf16[4,32,1024]{2,1,0:T(8,128)(2,1)S(1)} %all_to_all.20.buf_ref) | copy-start | bytes 786436
  63.5 68.6 %copy-start = (f32[4,4096]{1,0:T(4,128)S(1)}, f32[4,4096]{1,0:T(4,128)}, u32[]{:S(2)}) copy-start(f32[4,4096]{1,0:T(4,128)} %cc_ref.1) | copy-start | bytes 196612
  63.5 103.2 %copy-start.4 = (f32[2048]{0:T(1024)S(1)}, f32[2048]{0:T(1024)}, u32[]{:S(2)}) copy-start(f32[2048]{0:T(1024)} %param.27) | copy-start | bytes 24580
  63.5 103.2 %copy-start.7 = (f32[16]{0:T(128)S(1)}, f32[16]{0:T(128)}, u32[]{:S(2)}) copy-start(f32[16]{0:T(128)} %bias.1) | copy-start | bytes 196
  68.0 9.1 %all-to-all-start.2 = ((bf16[4,144,256]{2,1,0:T(8,128)(2,1)}), bf16[4,144,256]{2,1,0:T(8,128)(2,1)S(1)}, u32[]{:S(2)}, u32[]{:S(2)}) async-start(bf16[4,144,256]{2,1,0:T(8,128)(2,1)} %project.3), calls=%async_computation.2 | async-start | bytes 589824 | tf_op jit(solution)/shard_map/all_to_all | solution.py:488
  71.4 95.3 %all-gather.7.cloned.1.call-start = ((), (), s32[]{:S(2)}) async-start(), calls=%async_computation.5 | async-start | bytes 5849088 | tf_op jit(solution)/shard_map/all_gather | solution.py:493
  72.1 60.0 %copy-start.5 = (s32[2]{0:T(128)S(1)}, s32[2]{0:T(128)}, u32[]{:S(2)}) copy-start(s32[2]{0:T(128)} %pad_add_fusion.ids) | copy-start | bytes 28
  77.1 0.8 copy-start.9
  81.1 50.9 %copy-start.1 = (f32[128,8]{1,0:T(8,128)S(1)}, f32[128,8]{1,0:T(8,128)}, u32[]{:S(2)}) copy-start(f32[128,8]{1,0:T(8,128)} %get-tuple-element.23.cols_ref) | copy-start | bytes 12292
  81.1 50.9 %copy-start.2 = (bf16[128,256]{1,0:T(8,128)(2,1)S(1)}, bf16[128,256]{1,0:T(8,128)(2,1)}, u32[]{:S(2)}) copy-start(bf16[128,256]{1,0:T(8,128)(2,1)} %get-tuple-element.20.xin_ref) | copy-start | bytes 196612
  81.2 50.9 %copy-start.3 = (bf16[128,128]{1,0:T(8,128)(2,1)S(1)}, bf16[128,128]{1,0:T(8,128)(2,1)}, u32[]{:S(2)}) copy-start(bf16[128,128]{1,0:T(8,128)(2,1)} %get-tuple-element.21.bkey_ref) | copy-start | bytes 98308
  81.2 50.9 %copy-start.6 = (f32[8,128]{1,0:T(8,128)S(1)}, f32[8,128]{1,0:T(8,128)}, u32[]{:S(2)}) copy-start(f32[8,128]{1,0:T(8,128)} %get-tuple-element.22.rows_ref) | copy-start | bytes 12292
Sparse Core Ops, SparseCore 0:
  16.8 46.0 all-gather.4
  81.3 85.3 all-gather.6

commit v8 on v5

--- a/solution.py
+++ b/solution.py
@@ -62,8 +62,8 @@
 def prep_kernel(*refs):
     x_hbm, gain_hbm, ws_hbm = refs[:3]
     sources = refs[3:12]
-    xs_ref, step_ref, first_ref, second_ref = refs[12:16]
-    x_ref, gain_ref, ws_ref, third_ref, sems, wsems = refs[16:]
+    xs_hbm, step_ref, first_ref, second_ref = refs[12:16]
+    x_ref, gain_ref, ws_ref, third_ref, xs_ref, sems, wsems, xsems = refs[16:]
     early = pull(((x_hbm.at[0], x_ref), (gain_hbm, gain_ref), (ws_hbm, ws_ref)), sems)
     pairs = []
     outs = (first_ref, second_ref, third_ref)
@@ -81,14 +81,18 @@
         lax.dot_general(ws_ref[...], normed, NT, preferred_element_type=F32)
     )
     wide = normed.astype(F32)
+    for copy in later:
+        copy.wait()
+    writes = []
     for f in range(4):
         for g in range(4):
             xs_ref[f, 0:BLOCK, g * 128 : (g + 1) * 128] = shuffled(wide, f, g)
-    for copy in later:
-        copy.wait()
-    for f in range(4):
         xs_ref[f, BLOCK:, 0:256] = third_ref[0:16, :]
         xs_ref[f, BLOCK:, 256:512] = third_ref[16:32, :]
+        writes.append(pltpu.make_async_copy(xs_ref.at[f], xs_hbm.at[f], xsems.at[f]))
+        writes[-1].start()
+    for copy in writes:
+        copy.wait()
 
 
 def prep_call(inputs, gain, w_step_t, *arrays):
@@ -100,6 +104,7 @@
     return pl.pallas_call(
         prep_kernel,
         in_specs=[hbm] * 12,
+        out_specs=[hbm] + [pl.BlockSpec(memory_space=pltpu.VMEM)] * 3,
         out_shape=(
             jax.ShapeDtypeStruct((4, rows + HALO, width // 4), BF16),
             jax.ShapeDtypeStruct((heads, rows), F32),
@@ -111,8 +116,10 @@
             pltpu.VMEM((1, width), F32),
             pltpu.VMEM((heads, width), BF16),
             pltpu.VMEM((part, widths[2]), BF16),
+            pltpu.VMEM((4, rows + HALO, width // 4), BF16),
             pltpu.SemaphoreType.DMA((3,)),
             pltpu.SemaphoreType.DMA((9,)),
+            pltpu.SemaphoreType.DMA((4,)),
         ],
         name="prep",
     )(inputs, gain.reshape(1, -1), w_step_t, *arrays)
@@ -170,17 +177,23 @@
 
 def local_kernel(
     ids, rate, act_ref, step_ref, off_ref, ci_ref, cb_ref, buf_ref,
-    send_ref, xin_ref, bkey_ref, rows_ref, cols_ref, wide_ref, sems,
+    send_hbm, xin_ref, bkey_ref, rows_ref, cols_ref, wide_ref, send_ref, sems,
 ):
     tensor = ids[1]
     moved = pull(
         [
-            (buf_ref.at[f, pl.ds(BLOCK, HALO)], send_ref.at[pl.ds(KEPT + HALO * f, HALO)])
+            (buf_ref.at[f, pl.ds(BLOCK, HALO)], send_hbm.at[pl.ds(KEPT + HALO * f, HALO)])
             for f in range(4)
         ],
         sems,
     )
     send_ref[0:BLOCK, :] = added(act_ref, 0, 512)[HALO:]
+    moved.append(
+        pltpu.make_async_copy(
+            send_ref.at[pl.ds(0, BLOCK)], send_hbm.at[pl.ds(0, BLOCK)], sems.at[4]
+        )
+    )
+    moved[-1].start()
     wide_ref[...] = added(act_ref, 512, 384).astype(F32)
     conv = convolved(wide_ref, jnp.concatenate([ci_ref[...], cb_ref[...]], axis=1))
     xin, bkey = conv[:, 0:256], conv[:, 256:384]
@@ -216,6 +229,9 @@
         logs = jnp.concatenate([high, log - high], axis=0).astype(BF16)
         send_ref[BLOCK : BLOCK + 64, h * 128 : (h + 1) * 128] = state.astype(BF16)
         send_ref[BLOCK + 64 : KEPT, h * 128 : (h + 1) * 128] = logs
+    kept = pl.ds(BLOCK, KEPT - BLOCK)
+    moved.append(pltpu.make_async_copy(send_ref.at[kept], send_hbm.at[kept], sems.at[5]))
+    moved[-1].start()
     for copy in moved:
         copy.wait()
 
@@ -236,10 +252,15 @@
                 pl.BlockSpec(memory_space=pl.ANY),
             ],
             out_specs=[
-                full(SENT, 512), full(BLOCK, 256), full(BLOCK, 128), full(8, BLOCK),
+                pl.BlockSpec(memory_space=pltpu.HBM), full(BLOCK, 256), full(BLOCK, 128),
+                full(8, BLOCK),
                 full(BLOCK, 8),
             ],
-            scratch_shapes=[pltpu.VMEM((ROWS, 384), F32), pltpu.SemaphoreType.DMA((4,))],
+            scratch_shapes=[
+                pltpu.VMEM((ROWS, 384), F32),
+                pltpu.VMEM((KEPT, 512), BF16),
+                pltpu.SemaphoreType.DMA((6,)),
+            ],
         ),
         out_shape=(
             jax.ShapeDtypeStruct((SENT, 512), BF16),
@@ -299,7 +320,6 @@
     )(ids, act, conv_weight, xin, bkey, rows, cols)
 
 
-SUB = 256
 KEYS = 512
 KEPT = BLOCK + 80
 SENT = KEPT + 64
@@ -308,7 +328,7 @@
 
 def attend_kernel(
     ids, bias, q_ref, yin_ref, gate_ref, cq_ref, cols_ref, gain_ref, all_hbm, a0, a1, a2, a3,
-    out_ref, kv_ref, st_ref, wm_ref, wa_ref, acc_ref, late_ref, hold_ref, sems, ksems,
+    out_ref, kv_ref, st_ref, wm_ref, wa_ref, acc_ref, late_ref, hold_ref, sems, ksems, gsems,
 ):
     block, tensor, mine = ids[0], ids[1], ids[2]
     per = KEYS // BLOCK
@@ -322,69 +342,26 @@
             all_hbm.at[picked, pl.ds(0, BLOCK)], kv_ref.at[picked], ksems.at[chunk]
         )
 
-    states = pltpu.make_async_copy(all_hbm.at[:, pl.ds(BLOCK, 80)], st_ref, sems.at[0])
-    weights = [pltpu.make_async_copy(all_hbm.at[:, pl.ds(KEPT, 64)], wm_ref, sems.at[1])]
+    def states(group):
+        picked = pl.ds(group * per, per)
+        return pltpu.make_async_copy(
+            all_hbm.at[picked, pl.ds(BLOCK, 80)], st_ref.at[picked], gsems.at[group]
+        )
+
+    weights = [pltpu.make_async_copy(all_hbm.at[:, pl.ds(KEPT, 64)], wm_ref, sems.at[0])]
     weights += [
-        pltpu.make_async_copy(w, wa_ref.at[(mine + 4 - r) % 4], sems.at[2 + r])
+        pltpu.make_async_copy(w, wa_ref.at[(mine + 4 - r) % 4], sems.at[1 + r])
         for r, w in enumerate((a0, a1, a2, a3))
     ]
+    for group in range(count // per):
+        pl.when(group * per < block)(lambda group=group: states(group).start())
     for chunk in chunks:
         pl.when((chunk <= last) & (chunk >= last - 1))(lambda chunk=chunk: move(chunk).start())
     acc_ref[...] = jnp.zeros_like(acc_ref)
     late_ref[...] = jnp.zeros_like(late_ref)
     hold_ref[...] = jnp.zeros_like(hold_ref)
-    onward = (iota((2 * SUB, SUB), 0) % SUB > iota((2 * SUB, SUB), 1)).astype(BF16)
-
-    def piece(chunk, masked):
-        move(chunk).wait()
-        if chunk > 1:
-            move(chunk - 2).start()
-        for h in range(2):
-            late = late_ref[h]
-            gained = acc_ref[h]
-            query = q_ref[:, h * 128 : (h + 1) * 128]
-            offset = bias[2 * tensor + h] * LOG2E
-            for sub in range(KEYS // SUB - 1, -1, -1):
-                at = chunk * KEYS + sub * SUB
-                first = at // BLOCK
-                key = kv_ref[first : first + 2, :, h * 128 : (h + 1) * 128]
-                value = kv_ref[first : first + 2, :, 256 + h * 128 : 256 + (h + 1) * 128]
-                logits = lax.dot_general(
-                    query, key.reshape(SUB, 128), NT, preferred_element_type=F32
-                )
-                logits = logits * (128 ** -0.5 * LOG2E) + offset
-                soft = jnp.maximum(logits, 0.0) + LOG2E * jnp.log(
-                    1.0 + jnp.exp2(-jnp.abs(logits))
-                )
-                taken = logits - soft
-                if masked:
-                    before = at + iota((BLOCK, SUB), 1) < block * BLOCK + iota((BLOCK, SUB), 0)
-                    soft = jnp.where(before, soft, 0.0)
-                high = soft.astype(BF16)
-                low = (soft - high.astype(F32)).astype(BF16)
-                tail = jnp.dot(
-                    jnp.concatenate([high, low], axis=1), onward, preferred_element_type=F32
-                )
-                later = jnp.concatenate([late] * (SUB // 128), axis=1)
-                weight = jnp.exp2(taken - (tail + later))
-                if masked:
-                    weight = jnp.where(before, weight, 0.0)
-                gained = gained + jnp.dot(
-                    weight.astype(BF16), value.reshape(SUB, 128), preferred_element_type=F32
-                )
-                late = late + jnp.broadcast_to(tail[:, 0:1] + soft[:, 0:1], (BLOCK, 128))
-            late_ref[h] = late
-            acc_ref[h] = gained
-
-    for chunk in chunks:
-        if chunk == 1:
-            states.start()
-            for copy in weights:
-                copy.start()
-        pl.when(chunk == last)(lambda chunk=chunk: piece(chunk, True))
-        pl.when(chunk < last)(lambda chunk=chunk: piece(chunk, False))
-
-    states.wait()
+    for group in range(count // per):
+        pl.when(group * per < block)(lambda group=group: states(group).wait())
 
     def advance(k, carry):
         logs = st_ref[k, 64:80, :].astype(F32)
@@ -404,6 +381,58 @@
     gated = (yin_ref[...] + jnp.concatenate(ys, axis=1)) * gate_ref[...]
     scale = lax.rsqrt(jnp.mean(gated * gated, axis=-1, keepdims=True) + EPS)
     mixed = (gated * scale * gain_ref[...]).astype(BF16)
+    row = iota((256, 256), 0) % 128
+    col = iota((256, 256), 1)
+    onward = ((row > col) | (col >= 128)).astype(BF16)
+
+    def piece(turn, carry):
+        chunk = last - turn
+        move(chunk).wait()
+        pl.when(chunk > 1)(lambda: move(chunk - 2).start())
+
+        @pl.when(turn == jnp.minimum(last, 1))
+        def _():
+            for copy in weights:
+                copy.start()
+
+        picked = pl.ds(chunk * per, per)
+        before = [
+            chunk * KEYS + sub * BLOCK + iota((BLOCK, BLOCK), 1)
+            < block * BLOCK + iota((BLOCK, BLOCK), 0)
+            for sub in range(per)
+        ]
+        taken, parts = {}, []
+        for h in range(2):
+            query = q_ref[:, h * 128 : (h + 1) * 128]
+            key = kv_ref[picked, :, h * 128 : (h + 1) * 128].reshape(KEYS, 128)
+            logits = lax.dot_general(query, key, NT, preferred_element_type=F32)
+            logits = logits * (128 ** -0.5 * LOG2E) + bias[2 * tensor + h] * LOG2E
+            soft = jnp.maximum(logits, 0.0) + LOG2E * jnp.log(1.0 + jnp.exp2(-jnp.abs(logits)))
+            for sub in range(per):
+                at = slice(sub * BLOCK, (sub + 1) * BLOCK)
+                taken[h, sub] = logits[:, at] - soft[:, at]
+                kept = jnp.where(before[sub], soft[:, at], 0.0)
+                high = kept.astype(BF16)
+                low = (kept - high.astype(F32)).astype(BF16)
+                parts.append(jnp.concatenate([high, low], axis=1))
+        sums = jnp.dot(jnp.concatenate(parts, axis=0), onward, preferred_element_type=F32)
+        for h in range(2):
+            late = late_ref[h]
+            weights_h = [None] * per
+            for sub in range(per - 1, -1, -1):
+                at = (h * per + sub) * BLOCK
+                mine_sums = sums[at : at + BLOCK]
+                weight = jnp.exp2(taken[h, sub] - (mine_sums[:, 0:128] + late))
+                weights_h[sub] = jnp.where(before[sub], weight, 0.0).astype(BF16)
+                late = late + mine_sums[:, 128:256]
+            value = kv_ref[picked, :, 256 + h * 128 : 256 + (h + 1) * 128].reshape(KEYS, 128)
+            acc_ref[h] += jnp.dot(
+                jnp.concatenate(weights_h, axis=1), value, preferred_element_type=F32
+            )
+            late_ref[h] = late
+        return carry
+
+    lax.fori_loop(0, last + 1, piece, 0)
     attended = jnp.concatenate([acc_ref[0].astype(BF16), acc_ref[1].astype(BF16)], axis=1)
     for copy in weights:
         copy.wait()
@@ -427,7 +456,7 @@
 def attend_call(ids, bias, q, yin, gate, cq, cols, gain, gathered, rows):
     full = lambda *shape: pl.BlockSpec(shape, lambda i, ids, bias: (0,) * len(shape))
     count = gathered.shape[0]
-    hbm = pl.BlockSpec(memory_space=pl.ANY)
+    near = pl.BlockSpec(memory_space=pltpu.VMEM)
     return pl.pallas_call(
         attend_kernel,
         grid_spec=pltpu.PrefetchScalarGridSpec(
@@ -436,7 +465,7 @@
             in_specs=[
                 full(BLOCK, 256), full(BLOCK, 256), full(BLOCK, 256), full(BLOCK, 128),
                 full(BLOCK, 8), pl.BlockSpec((1, 256), lambda i, ids, bias: (0, ids[1])),
-                pl.BlockSpec(memory_space=pltpu.HBM), hbm, hbm, hbm, hbm,
+                pl.BlockSpec(memory_space=pltpu.HBM), near, near, near, near,
             ],
             out_specs=full(BLOCK, 2048),
             scratch_shapes=[
@@ -447,7 +476,8 @@
                 pltpu.VMEM((2, BLOCK, 128), F32),
                 pltpu.VMEM((2, BLOCK, 128), F32),
                 pltpu.VMEM((64, 512), F32),
-                pltpu.SemaphoreType.DMA((6,)),
+                pltpu.SemaphoreType.DMA((5,)),
+                pltpu.SemaphoreType.DMA((count * BLOCK // KEYS,)),
                 pltpu.SemaphoreType.DMA((count * BLOCK // KEYS,)),
             ],
         ),

time: 183 us -> 184 us (level)
  no operation moved by 1% of the time
where the time goes in v8:
time: 184 us; the launch traced here: 183 us
  blocking collectives  83.8 us (46%)
  waiting for transfers between devices  46 us (25%)
  starting transfers between devices  25.6 us (14%)
  between operations  13.6 us (7%)
  Pallas kernels  13.3 us (7%)
    all_gather x1, blocking collectives, body(): early = lax.all_gather(first, 'sp', axis=0, tiled=True)  34.2 us
    all_gather x1, waiting for transfers between devices, body(): gathered = lax.all_gather(send, 'sp', axis=0)  31.8 us
    all_gather x1, blocking collectives, body(): act, kept = projected(lax.all_gather(second, 'sp', axis=0, tiled=True), 640)  27.8 us
    all_to_all x1, blocking collectives, body(): parts = lax.all_to_all(partial.reshape(8, 16, 2048), 'tp', 0, 0, tiled=True)  21.8 us
    ppermute x3, starting transfers between devices, rotated(): lax.ppermute(shard, axis, [(i, (i + by) % length) for i in range(length)])  10.7 us
    all_to_all x2, waiting for transfers between devices, projected(): return (lax.all_to_all(act, 'fs', 0, 0, tiled=True), *kept)  9.58 us
    all_to_all x2, starting transfers between devices, projected(): return (lax.all_to_all(act, 'fs', 0, 0, tiled=True), *kept)  8.03 us
    all_to_all x1, starting transfers between devices, body(): tokens = lax.all_to_all(split, 'fs', 0, 0, tiled=True)  5.14 us
  transfers between devices with their start and end apart: 8, of which 5 were waited for; matrix products, arithmetic and copies ran while one was open for 0% of the time, Pallas kernels for 1%

profile of v8, /device:TPU:1, one launch (start us, length us, event | category | flops | bytes accessed | tf_op | source)
XLA Modules:
  0.0 183.1 jit_solution(6812667343052372142)
XLA Ops:
  6.5 3.6 %prep.1 = (bf16[4,144,512]{2,1,0:T(8,128)(2,1)}, f32[32,128]{1,0:T(8,128)}, bf16[32,896]{1,0:T(8,128)(2,1)}, bf16[32,896]{1,0:T(8,128)(2,1)}) custom-call(bf16[1,128,2048]{2,1,0:T(8,128)(2,1)} %refs_0_.1, f32[1,2048]{1,0:T(1,128)} %bitcast.21, bf16[32,2048]{1,0:T(8,128)(2,1)} %bitcast.18, bf16[32,256]{1,0:T(8,128)(2,1)} %refs_3_.1, bf16[32,256]{1,0:T(8,128)(2,1)} %refs_4_.1, ...), custom_call_target="tpu_custom_call" | custom-call | tf_op jit(solution)/shard_map/prep/pallas_call | solution.py:104
  10.2 0.0 copy-start.1
  10.2 0.0 copy-start.6
  10.2 5.1 %all-to-all-start = ((bf16[4,144,512]{2,1,0:T(8,128)(2,1)}), bf16[4,144,512]{2,1,0:T(8,128)(2,1)S(1)}, u32[]{:S(2)}, u32[]{:S(2)}) async-start(bf16[4,144,512]{2,1,0:T(8,128)(2,1)} %get-tuple-element.22), calls=%async_computation | async-start | bytes 1179648 | tf_op jit(solution)/shard_map/all_to_all | solution.py:505
  15.3 34.2 %all_gather.12.w_ref = bf16[512,896]{1,0:T(8,128)(2,1)S(1)} all-gather(bf16[32,896]{1,0:T(8,128)(2,1)} %get-tuple-element.23), channel_id=1, replica_groups=mesh['sp'=16,'fs'=4,'tp'=8] {'sp'}, dimensions={0}, use_global_device_ids=true | all-gather | bytes 974848 | tf_op jit(solution)/shard_map/all_gather | solution.py:506
  49.5 0.0 all-to-all-done.x_ref.buf_ref
  49.6 1.7 collective-permute-start
  51.3 1.3 collective-permute-done.rim_ref
  52.6 1.5 project.3
  54.1 0.0 copy-start.2
  54.1 0.0 copy-start.5
  54.1 4.5 %all-to-all-start.2 = ((bf16[4,144,896]{2,1,0:T(8,128)(2,1)}), bf16[4,144,896]{2,1,0:T(8,128)(2,1)S(1)}, u32[]{:S(2)}, u32[]{:S(2)}) async-start(bf16[4,144,896]{2,1,0:T(8,128)(2,1)} %project.3), calls=%async_computation.2 | async-start | bytes 2064384 | tf_op jit(solution)/shard_map/all_to_all | solution.py:514
  58.7 0.1 pad_add_fusion.ids
  58.8 9.6 %all-to-all-done.2.act_ref = bf16[4,144,896]{2,1,0:T(8,128)(2,1)S(1)} async-done(((bf16[4,144,896]{2,1,0:T(8,128)(2,1)}), bf16[4,144,896]{2,1,0:T(8,128)(2,1)S(1)}, u32[]{:S(2)}, u32[]{:S(2)}) %all-to-all-start.2) | async-done | bytes 1032224 | tf_op jit(solution)/shard_map/all_to_all | solution.py:514
  68.3 0.0 copy-done
  68.3 2.0 %ssd_local.1 = (bf16[272,512]{1,0:T(8,128)(2,1)}, bf16[128,256]{1,0:T(8,128)(2,1)S(1)}, bf16[128,128]{1,0:T(8,128)(2,1)S(1)}, f32[8,128]{1,0:T(8,128)S(1)}, f32[128,8]{1,0:T(8,128)S(1)}) custom-call(s32[3]{0:T(128)S(1)} %pad_add_fusion.ids, f32[32]{0:T(128)S(1)} %copy-done.4, bf16[4,144,896]{2,1,0:T(8,128)(2,1)S(1)} %all-to-all-done.2.act_ref, ...), custom_call_target="tpu_custom_call" | custom-call | tf_op jit(solution)/shard_map/ssd_local/pallas_call | solution.py:241
  70.4 0.0 all-gather.3.cloned.1.call-update
  70.4 27.8 %all_gather.13.w_ref = bf16[512,896]{1,0:T(8,128)(2,1)S(1)} all-gather(bf16[32,896]{1,0:T(8,128)(2,1)S(1)} %copy-done.6), channel_id=1, replica_groups=mesh['sp'=16,'fs'=4,'tp'=8] {'sp'}, dimensions={0}, use_global_device_ids=true | all-gather | bytes 974848 | tf_op jit(solution)/shard_map/all_gather | solution.py:521
  98.2 1.4 project.2
  99.5 3.5 %all-to-all-start.1 = ((bf16[4,144,640]{2,1,0:T(8,128)(2,1)}), bf16[4,144,640]{2,1,0:T(8,128)(2,1)S(1)}, u32[]{:S(2)}, u32[]{:S(2)}) async-start(bf16[4,144,640]{2,1,0:T(8,128)(2,1)} %get-tuple-element.26), calls=%async_computation.1 | async-start | bytes 1474560 | tf_op jit(solution)/shard_map/all_to_all | solution.py:514
  103.1 3.3 %collective-permute-start.1 = (bf16[512,256]{1,0:T(8,128)(2,1)S(1)}, bf16[512,256]{1,0:T(8,128)(2,1)S(1)}, u32[]{:S(2)}, u32[]{:S(2)}) collective-permute-start(bf16[512,256]{1,0:T(8,128)(2,1)S(1)} %get-tuple-element.38.a0), channel_id=1, source_target_pairs={{0,8},{8,16},{16,24},{24,0},{1,9},{9,17},{17,25},{25,1},{2,10},{10... | collective-permute-start | bytes 786440 | tf_op jit(solution)/shard_map/ppermute | solution.py:492
  106.4 4.3 %collective-permute-start.2 = (bf16[512,256]{1,0:T(8,128)(2,1)S(1)}, bf16[512,256]{1,0:T(8,128)(2,1)S(1)}, u32[]{:S(2)}, u32[]{:S(2)}) collective-permute-start(bf16[512,256]{1,0:T(8,128)(2,1)S(1)} %get-tuple-element.38.a0), channel_id=1, source_target_pairs={{0,16},{8,24},{16,0},{24,8},{1,17},{9,25},{17,1},{25,9},{2,18},{10... | collective-permute-start | bytes 786440 | tf_op jit(solution)/shard_map/ppermute | solution.py:492
  110.7 3.1 %collective-permute-start.3 = (bf16[512,256]{1,0:T(8,128)(2,1)S(1)}, bf16[512,256]{1,0:T(8,128)(2,1)S(1)}, u32[]{:S(2)}, u32[]{:S(2)}) collective-permute-start(bf16[512,256]{1,0:T(8,128)(2,1)S(1)} %get-tuple-element.38.a0), channel_id=1, source_target_pairs={{0,24},{8,0},{16,8},{24,16},{1,25},{9,1},{17,9},{25,17},{2,26},{10... | collective-permute-start | bytes 786440 | tf_op jit(solution)/shard_map/ppermute | solution.py:492
  113.8 0.0 all-to-all-done.1.act_ref
  113.8 1.1 ssd_inner.1
  114.9 0.0 collective-permute-done.1.a1
  114.9 1.9 %collective-permute-done.2.a2 = bf16[512,256]{1,0:T(8,128)(2,1)S(1)} collective-permute-done((bf16[512,256]{1,0:T(8,128)(2,1)S(1)}, bf16[512,256]{1,0:T(8,128)(2,1)S(1)}, u32[]{:S(2)}, u32[]{:S(2)}) %collective-permute-start.2) | collective-permute-done | bytes 262176 | tf_op jit(solution)/shard_map/ppermute | solution.py:492
  116.8 1.4 collective-permute-done.3.a3
  118.2 31.8 %all-gather.3.cloned.1.call-done = bf16[4352,512]{1,0:T(8,128)(2,1)} async-done(((bf16[272,512]{1,0:T(8,128)(2,1)}), bf16[4352,512]{1,0:T(8,128)(2,1)}) %all-gather.3.cloned.1.call-update) | async-done | bytes 4456464 | tf_op jit(solution)/shard_map/all_gather | solution.py:520
  150.1 3.7 %attend.1 = bf16[128,2048]{1,0:T(8,128)(2,1)S(1)} custom-call(s32[3]{0:T(128)S(1)} %pad_add_fusion.ids, f32[16]{0:T(128)S(1)} %copy-done.5, bf16[128,256]{1,0:T(8,128)(2,1)S(1)} %get-tuple-element.33.q_ref, f32[128,256]{1,0:T(8,128)S(1)} %get-tuple-element.34.yin_ref, f32[128,256]{1,0:T(8,128)S(1)} %get-tuple-element.35.gate_ref, ...), custom_call_target="tpu_custom_call" | custom-call | tf_op jit(solution)/shard_map/attend/pallas_call | solution.py:460
  153.7 21.8 %all_to_all.20 = bf16[8,16,2048]{2,1,0:T(8,128)(2,1)S(1)} all-to-all(bf16[8,16,2048]{2,1,0:T(8,128)(2,1)S(1)} %bitcast.14), channel_id=1, replica_groups=mesh['sp'=16,'fs'=4,'tp'=8] {'tp'}, dimensions={0} | all-to-all | bytes 1048576 | tf_op jit(solution)/shard_map/all_to_all | solution.py:525
  175.5 0.7 reduce_sum.12
  (11 shorter events, 0.0 us)
Async XLA Ops:
  6.5 61.8 %copy-start.3 = (f32[1,128,4]{1,2,0:T(4,128)S(1)}, f32[1,128,4]{1,2,0:T(4,128)}, u32[]{:S(2)}) copy-start(f32[1,128,4]{1,2,0:T(4,128)} %param.26) | copy-start | bytes 6148
  6.5 61.8 %copy-start = (f32[4,4096]{1,0:T(4,128)S(1)}, f32[4,4096]{1,0:T(4,128)}, u32[]{:S(2)}) copy-start(f32[4,4096]{1,0:T(4,128)} %cc_ref.1) | copy-start | bytes 196612
  6.5 61.8 %copy-start.4 = (f32[32]{0:T(128)S(1)}, f32[32]{0:T(128)}, u32[]{:S(2)}) copy-start(f32[32]{0:T(128)} %rate.1) | copy-start | bytes 388
  10.2 58.2 %copy-start.1 = (f32[32,128]{1,0:T(8,128)S(1)}, f32[32,128]{1,0:T(8,128)}, u32[]{:S(2)}) copy-start(f32[32,128]{1,0:T(8,128)} %get-tuple-element.28.step_ref) | copy-start | bytes 49156
  10.2 60.3 %copy-start.6 = (bf16[32,896]{1,0:T(8,128)(2,1)S(1)}, bf16[32,896]{1,0:T(8,128)(2,1)}, u32[]{:S(2)}) copy-start(bf16[32,896]{1,0:T(8,128)(2,1)} %get-tuple-element.25) | copy-start | bytes 172036
  10.2 39.4 %all-to-all-start = ((bf16[4,144,512]{2,1,0:T(8,128)(2,1)}), bf16[4,144,512]{2,1,0:T(8,128)(2,1)S(1)}, u32[]{:S(2)}, u32[]{:S(2)}) async-start(bf16[4,144,512]{2,1,0:T(8,128)(2,1)} %get-tuple-element.22), calls=%async_computation | async-start | bytes 1179648 | tf_op jit(solution)/shard_map/all_to_all | solution.py:505
  49.6 3.0 %collective-permute-start = (bf16[4,16,512]{2,1,0:T(8,128)(2,1)S(1)}, bf16[4,16,512]{2,1,0:T(8,128)(2,1)S(1)}, u32[]{:S(2)}, u32[]{:S(2)}) collective-permute-start(bf16[4,16,512]{2,1,0:T(8,128)(2,1)S(1)} %slice.3), channel_id=1, source_target_pairs={{0,32},{32,64},{64,96},{96,128},{128,160},{160,192},{192,224},{224... | collective-permute-start | bytes 196616 | tf_op jit(solution)/shard_map/ppermute | solution.py:508
  54.1 95.9 %copy-start.2 = (f32[2048]{0:T(1024)S(1)}, f32[2048]{0:T(1024)}, u32[]{:S(2)}) copy-start(f32[2048]{0:T(1024)} %param.27) | copy-start | bytes 24580
  54.1 95.9 %copy-start.5 = (f32[16]{0:T(128)S(1)}, f32[16]{0:T(128)}, u32[]{:S(2)}) copy-start(f32[16]{0:T(128)} %bias.1) | copy-start | bytes 196
  54.1 14.2 %all-to-all-start.2 = ((bf16[4,144,896]{2,1,0:T(8,128)(2,1)}), bf16[4,144,896]{2,1,0:T(8,128)(2,1)S(1)}, u32[]{:S(2)}, u32[]{:S(2)}) async-start(bf16[4,144,896]{2,1,0:T(8,128)(2,1)} %project.3), calls=%async_computation.2 | async-start | bytes 2064384 | tf_op jit(solution)/shard_map/all_to_all | solution.py:514
  58.7 91.4 %all-gather.3.cloned.1.call-start = ((), (), s32[]{:S(2)}) async-start(), calls=%async_computation.4 | async-start | bytes 4734976 | tf_op jit(solution)/shard_map/all_gather | solution.py:520
  99.5 14.3 %all-to-all-start.1 = ((bf16[4,144,640]{2,1,0:T(8,128)(2,1)}), bf16[4,144,640]{2,1,0:T(8,128)(2,1)S(1)}, u32[]{:S(2)}, u32[]{:S(2)}) async-start(bf16[4,144,640]{2,1,0:T(8,128)(2,1)} %get-tuple-element.26), calls=%async_computation.1 | async-start | bytes 1474560 | tf_op jit(solution)/shard_map/all_to_all | solution.py:514
  103.1 11.9 %collective-permute-start.1 = (bf16[512,256]{1,0:T(8,128)(2,1)S(1)}, bf16[512,256]{1,0:T(8,128)(2,1)S(1)}, u32[]{:S(2)}, u32[]{:S(2)}) collective-permute-start(bf16[512,256]{1,0:T(8,128)(2,1)S(1)} %get-tuple-element.38.a0), channel_id=1, source_target_pairs={{0,8},{8,16},{16,24},{24,0},{1,9},{9,17},{17,25},{25,1},{2,10},{10... | collective-permute-start | bytes 786440 | tf_op jit(solution)/shard_map/ppermute | solution.py:492
  106.4 10.4 %collective-permute-start.2 = (bf16[512,256]{1,0:T(8,128)(2,1)S(1)}, bf16[512,256]{1,0:T(8,128)(2,1)S(1)}, u32[]{:S(2)}, u32[]{:S(2)}) collective-permute-start(bf16[512,256]{1,0:T(8,128)(2,1)S(1)} %get-tuple-element.38.a0), channel_id=1, source_target_pairs={{0,16},{8,24},{16,0},{24,8},{1,17},{9,25},{17,1},{25,9},{2,18},{10... | collective-permute-start | bytes 786440 | tf_op jit(solution)/shard_map/ppermute | solution.py:492
  110.7 7.5 %collective-permute-start.3 = (bf16[512,256]{1,0:T(8,128)(2,1)S(1)}, bf16[512,256]{1,0:T(8,128)(2,1)S(1)}, u32[]{:S(2)}, u32[]{:S(2)}) collective-permute-start(bf16[512,256]{1,0:T(8,128)(2,1)S(1)} %get-tuple-element.38.a0), channel_id=1, source_target_pairs={{0,24},{8,0},{16,8},{24,16},{1,25},{9,1},{17,9},{25,17},{2,26},{10... | collective-permute-start | bytes 786440 | tf_op jit(solution)/shard_map/ppermute | solution.py:492
Sparse Core Ops, SparseCore 0:
  70.5 79.4 all-gather.2
